TPU v7x, 512 devices: a whole 4x8x8 slice. The times are simulated.
512 devices in a mesh: sp: 128 (over z, y, core), tp: 4 (over x).
Axes of the slice: x: 4, y: 8, z: 8, core: 2. Of those that a mesh axis runs over, the one named last changes fastest.
Arguments:
- glu_value: bfloat16 [131072, 1024], P('sp', 'tp'), may hold values from -6 to 6
- glu_gate: bfloat16 [131072, 1024], P('sp', 'tp'), may hold values from -8 to 8
- conv_taps: float32 [31, 1024], P(None, 'tp'), may hold values from -1 to 1
- channel_gain: float32 [1024], P('tp'), may hold values from 0.1 to 1.9
- proj_weight: bfloat16 [1024, 1024], P('tp'), may hold values from -0.1875 to 0.1875
- out_grad: bfloat16 [131072, 1024], P('sp'), may hold values from -6 to 6
Outputs:
- value_grad: bfloat16 [131072, 1024], P('sp', 'tp')
- gate_grad: bfloat16 [131072, 1024], P('sp', 'tp')
- proj_grad: float32 [1024, 1024], P(('tp', 'sp'))
- taps_grad: float32 [31, 1024], P(None, 'tp')
- norm_gain_gradient: float32 [1024], P('tp')
All inputs are finite; a program needn't handle non-finite values.
Results may differ from a plain program's by a relative error of at most 0.0029.
Values may be sent and summed in bfloat16 or wider, within the bound.
No kernel may reach another device: no remote copies, remote signals or barrier semaphores. Data moves between devices by JAX's collectives and lax.ppermute only.
A program may use at most 64 MiB of HBM per device.

v0:
```python
import jax
import jax.numpy as jnp
from jax import lax
from jax.sharding import Mesh
from jax.sharding import PartitionSpec as P

SP = ("sp_0", "sp_1", "sp_2")
TP_SP = ("tp", "sp_0", "sp_1", "sp_2")


def from_behind(block, axis, distance):
    devices = range(lax.axis_size(axis))
    route = [(i - distance, i) for i in devices if i - distance in devices]
    return lax.ppermute(block, axis, route)


def sent_to_all(array, axis):
    peers = lax.axis_size(axis)
    return lax.all_to_all(
        jnp.broadcast_to(array[None], (peers, *array.shape)), axis, 0, 0, tiled=True
    )


def over_copies(array, axis):
    everything = sent_to_all(array, axis)
    return jnp.sum(everything, axis=0)


def together(arrays, axis):
    ends = [0]
    for a in arrays:
        ends.append(ends[-1] + a.size)
    so_far = over_copies(jnp.concatenate([a.ravel() for a in arrays]), axis)
    return tuple((so_far[b:e].reshape(a.shape) for a, b, e in zip(arrays, ends, ends[1:])))


def in_blocks(array, dim, peers):
    before, after = (array.shape[:dim], array.shape[dim + 1 :])
    return jnp.moveaxis(array.reshape(*before, peers, -1, *after), dim, 0)


def sent_and_summed(array, axis, dim):
    peers = lax.axis_size(axis)
    tiles = lax.all_to_all(in_blocks(array, dim, peers), axis, 0, 0, tiled=True)
    return jnp.sum(tiles, axis=0)


def sum_by_axis(array, axes, dim):
    far, near = axes
    own = sent_and_summed(in_blocks(array, dim, lax.axis_size(far)), near, dim + 1)
    return jnp.sum(lax.all_to_all(own, far, 0, 0, tiled=True), axis=0)


def rows_for(lines, peers):
    spare = -lines.shape[0] % peers
    if not spare:
        return lines
    return jnp.concatenate([lines, jnp.zeros((spare, *lines.shape[1:]), lines.dtype)])


def laid_out(tiles, dim):
    shape = list(tiles.shape[1:])
    shape[dim] *= tiles.shape[0]
    return jnp.moveaxis(tiles, 0, dim).reshape(shape)


def gathered_by_axis(array, axes, dim):
    far, near = axes
    initial = sent_to_all(array, far)
    tiles = jnp.swapaxes(sent_to_all(initial, near), 0, 1)
    return laid_out(tiles.reshape(-1, *array.shape), dim)


def nested_sum(array, axes):
    padded = rows_for(array, lax.axis_size(axes[0]) * lax.axis_size(axes[1]))
    whole = gathered_by_axis(sum_by_axis(padded, axes, 0), axes, 0)
    return lax.slice_in_dim(whole, 0, len(array)).reshape(array.shape)


def packed_total(arrays, axis):
    flat, at, done = (jnp.concatenate([a.reshape(-1) for a in arrays]), 0, [])
    so_far = nested_sum(flat, axis)
    for a in arrays:
        done.append(so_far[at : at + a.size].reshape(a.shape))
        at += a.size
    return tuple(done)


def per_device(glu_value, glu_gate, conv_taps, channel_gain, proj_weight, out_grad):
    kernel_len = conv_taps.shape[0]
    halo_rows = kernel_len - 1
    row_count = glu_value.shape[0]
    channel_width = channel_gain.shape[0] * lax.axis_size("tp")
    gradient_factor = 1.0 / jnp.sqrt(jnp.float32(row_count * lax.axis_size(SP)))
    prev_value, prev_gate = from_behind(
        (glu_value[row_count - halo_rows :], glu_gate[row_count - halo_rows :]), SP, 1
    )
    value_ext = jnp.concatenate([prev_value, glu_value], axis=0)
    gate_ext = jnp.concatenate([prev_gate, glu_gate], axis=0)
    glu_out = value_ext.astype(jnp.float32) * jax.nn.sigmoid(gate_ext.astype(jnp.float32))
    convolved_output = jnp.zeros((row_count, glu_out.shape[1]), jnp.float32)
    for tap in range(kernel_len):
        convolved_output = convolved_output + conv_taps[tap] * glu_out[tap : tap + row_count]
    row_sum, row_sq = together(
        (jnp.sum(convolved_output, axis=1), jnp.sum(convolved_output * convolved_output, axis=1)),
        "tp",
    )
    row_average = (row_sum / channel_width)[:, None]
    inverse_deviation = lax.rsqrt(
        (row_sq / channel_width)[:, None] - row_average * row_average + 1e-05
    )
    centered_scaled = (convolved_output - row_average) * inverse_deviation
    normalized_rows = centered_scaled * channel_gain
    activ = jax.nn.silu(normalized_rows).astype(jnp.bfloat16)
    act_grad = lax.dot_general(
        out_grad, proj_weight, (((1,), (1,)), ((), ())), preferred_element_type=jnp.float32
    )
    norm_sig = jax.nn.sigmoid(normalized_rows)
    normalized_gradient = act_grad * norm_sig * (1.0 + normalized_rows * (1.0 - norm_sig))
    centered_scaled_gradient = normalized_gradient * channel_gain
    backward_first, backward_second = together(
        (
            jnp.sum(centered_scaled_gradient, axis=1),
            jnp.sum(centered_scaled_gradient * centered_scaled, axis=1),
        ),
        "tp",
    )
    convolved_gradient = inverse_deviation * (
        centered_scaled_gradient
        - (backward_first / channel_width)[:, None]
        - centered_scaled * (backward_second / channel_width)[:, None]
    )
    gain_product = jnp.sum(normalized_gradient * centered_scaled, axis=0) * gradient_factor
    taps_term = (
        jnp.stack(
            [
                jnp.sum(convolved_gradient * glu_out[tap : tap + row_count], axis=0)
                for tap in range(kernel_len)
            ]
        )
        * gradient_factor
    )
    zero_rows = jnp.zeros((halo_rows, glu_out.shape[1]), jnp.float32)
    grad_pad = jnp.concatenate([zero_rows, convolved_gradient, zero_rows], axis=0)
    grad_ext = jnp.zeros((row_count + halo_rows, glu_out.shape[1]), jnp.float32)
    for tap in range(kernel_len):
        grad_ext = (
            grad_ext
            + conv_taps[tap] * grad_pad[halo_rows - tap : halo_rows - tap + row_count + halo_rows]
        )
    returned = from_behind(grad_ext[:halo_rows], SP, -1)
    own_part = grad_ext[halo_rows:]
    glu_grad = jnp.concatenate(
        [own_part[: row_count - halo_rows], own_part[row_count - halo_rows :] + returned], axis=0
    )
    value_f = glu_value.astype(jnp.float32)
    gate_sig = jax.nn.sigmoid(glu_gate.astype(jnp.float32))
    value_grad = (glu_grad * gate_sig).astype(jnp.bfloat16)
    gate_grad = (glu_grad * value_f * gate_sig * (1.0 - gate_sig)).astype(jnp.bfloat16)
    proj_grad = sum_by_axis(
        lax.dot_general(
            activ, out_grad, (((0,), (0,)), ((), ())), preferred_element_type=jnp.float32
        )
        * gradient_factor,
        (("sp_0", "sp_1"), "sp_2"),
        0,
    )
    taps_grad, norm_gain_gradient = packed_total(
        (taps_term, gain_product), (("sp_0", "sp_1"), "sp_2")
    )
    return (value_grad, gate_grad, proj_grad, taps_grad, norm_gain_gradient)


def solution(mesh):
    finer = Mesh(mesh.devices.reshape(8, 8, 2, mesh.shape["tp"]), ("sp_0", "sp_1", "sp_2", "tp"))
    return jax.shard_map(
        per_device,
        mesh=finer,
        in_specs=(P(SP, "tp"), P(SP, "tp"), P(None, "tp"), P("tp"), P("tp", None), P(SP, None)),
        out_specs=(P(SP, "tp"), P(SP, "tp"), P(TP_SP, None), P(None, "tp"), P("tp")),
        check_vma=False,
    )
```

profile of v0, /device:TPU:1, one launch (start us, length us, event | category | flops | bytes accessed | tf_op | source)
XLA Modules:
  0.0 134.5 jit_solution(9795917948837046299)
XLA Ops:
  1.5 4.6 %collective-permute-start = (bf16[30,256]{1,0:T(8,128)(2,1)S(1)}, bf16[30,256]{1,0:T(8,128)(2,1)S(1)}, u32[]{:S(2)}, u32[]{:S(2)}) collective-permute-start(bf16[30,256]{1,0:T(8,128)(2,1)S(1)} %slice.380), channel_id=1, source_target_pairs={{0,4},{4,8},{8,12},{12,16},{16,20},{20,24},{24,28},{28,32},{32,36}... | collective-permute-start | bytes 46088 | tf_op jit(solution)/shard_map/ppermute | solution.py:14
  6.8 1.9 %collective-permute-start.1 = (bf16[30,256]{1,0:T(8,128)(2,1)S(1)}, bf16[30,256]{1,0:T(8,128)(2,1)S(1)}, u32[]{:S(2)}, u32[]{:S(2)}) collective-permute-start(bf16[30,256]{1,0:T(8,128)(2,1)S(1)} %slice.381), channel_id=1, source_target_pairs={{0,4},{4,8},{8,12},{12,16},{16,20},{20,24},{24,28},{28,32},{32,36}... | collective-permute-start | bytes 46088 | tf_op jit(solution)/shard_map/ppermute | solution.py:14
  8.7 1.0 fusion.40
  9.8 1.0 fusion.41
  10.8 1.6 %collective-permute-done.1 = bf16[30,256]{1,0:T(8,128)(2,1)S(1)} collective-permute-done((bf16[30,256]{1,0:T(8,128)(2,1)S(1)}, bf16[30,256]{1,0:T(8,128)(2,1)S(1)}, u32[]{:S(2)}, u32[]{:S(2)}) %collective-permute-start.1) | collective-permute-done | bytes 15392 | tf_op jit(solution)/shard_map/ppermute | solution.py:14
  12.3 1.6 %divide_multiply_fusion = f32[1054,256]{1,0:T(8,128)S(1)} fusion(bf16[1024,256]{1,0:T(8,128)(2,1)} %param.6, bf16[30,256]{1,0:T(8,128)(2,1)S(1)} %collective-permute-done, bf16[1024,256]{1,0:T(8,128)(2,1)} %param.7, bf16[30,256]{1,0:T(8,128)(2,1)S(1)} %collective-permute-done.1), kind=kLoop, calls=%fused_computation.62 | loop fusion | flops 3237888 | bytes 2158592 | tf_op jit(solution)/shard_map/mul | solution.py:100
  13.9 5.1 %fusion.39 = (f32[1024]{0:T(1024)S(1)}, f32[1024]{0:T(1024)S(1)}, f32[1024,256]{1,0:T(8,128)}) fusion(f32[1054,256]{1,0:T(8,128)S(1)} %divide_multiply_fusion, f32[256]{0:T(256)S(1)} %bitcast.136, f32[256]{0:T(256)S(1)} %bitcast.138, f32[256]{0:T(256)S(1)} %bitcast.80, f32[256]{0:T(256)S(1)} %bitcast.82, f32[256]{0:T(256)S(1)} %bitcast.84, ...), kind=kLoop, calls=%fused_computation.126 | loop fusion | flops 16775168 | bytes 33594368 | tf_op jit(solution)/shard_map/reduce_sum | solution.py:105
  19.1 6.7 %all_to_all.47 = f32[4,1,2048]{2,1,0:T(1,128)S(1)} all-to-all(f32[4,1,2048]{2,1,0:T(1,128)S(1)} %broadcast_in_dim.12), channel_id=1, replica_groups=mesh['sp_0'=8,'sp_1'=8,'sp_2'=2,'tp'=4] {'tp'}, dimensions={0} | all-to-all | bytes 65536 | tf_op jit(solution)/shard_map/all_to_all | solution.py:19
  25.8 3.5 %multiply_reduce_fusion = (f32[256]{0:T(256)S(1)}, f32[1024]{0:T(1024)S(1)}, f32[1024]{0:T(1024)S(1)}, f32[1024,256]{1,0:T(8,128)}) fusion(f32[1024,256]{1,0:T(8,128)} %get-tuple-element.42, f32[1024]{0:T(1024)S(1)} %get-tuple-element.79, f32[1024]{0:T(1024)S(1)} %get-tuple-element.78, f32[256]{0:T(256)S(1)} %copy-done.5, ...), kind=kOutput, calls=%fused_computation.65 | convolution fusion | flops 541325056 | bytes 4737024 | tf_op jit(solution)/shard_map/dot_general | solution.py:115
  29.9 3.3 %all-to-all-start.1 = ((f32[4,1,2048]{2,1,0:T(1,128)}), f32[4,1,2048]{2,1,0:T(1,128)S(1)}, u32[]{:S(2)}, u32[]{:S(2)}) async-start(f32[4,1,2048]{2,1,0:T(1,128)} %broadcast_in_dim.13), calls=%async_computation.1 | async-start | bytes 65536 | tf_op jit(solution)/shard_map/all_to_all | solution.py:19
  33.2 4.3 %all-to-all-done.1 = f32[4,1,2048]{2,1,0:T(1,128)S(1)} async-done(((f32[4,1,2048]{2,1,0:T(1,128)}), f32[4,1,2048]{2,1,0:T(1,128)S(1)}, u32[]{:S(2)}, u32[]{:S(2)}) %all-to-all-start.1) | async-done | bytes 32800 | tf_op jit(solution)/shard_map/all_to_all | solution.py:19
  37.5 4.3 %multiply_reduce_fusion.1 = (f32[256]{0:T(256)S(1)}, f32[256]{0:T(256)S(1)}, f32[256]{0:T(256)S(1)}, f32[256]{0:T(256)S(1)}, f32[256]{0:T(256)S(1)}, /*index=5*/...) fusion(f32[1054,256]{1,0:T(8,128)S(1)} %divide_multiply_fusion,, ...), kind=kLoop, calls=%fused_computation.66 | loop fusion | flops 11267584 | bytes 22055936 | tf_op jit(solution)/shard_map/reduce_sum | solution.py:137
  41.8 1.7 %multiply_reduce_fusion.19 = (f32[256]{0:T(256)S(1)}, f32[256]{0:T(256)S(1)}, f32[256]{0:T(256)S(1)}, f32[256]{0:T(256)S(1)}, f32[256]{0:T(256)S(1)}, /*index=5*...) fusion(f32[1024,256]{1,0:T(8,128)S(1)} %get-tuple-element.41, ...), kind=kLoop, calls=%fused_computation.84 | loop fusion | flops 6812416 | bytes 14693376 | tf_op jit(solution)/shard_map/reduce_sum | solution.py:137
  43.9 7.1 %all_to_all.48 = f32[2,1,4096]{2,1,0:T(1,128)S(1)} all-to-all(f32[2,1,4096]{2,1,0:T(1,128)S(1)} %reshape.52), channel_id=1, replica_groups=mesh['sp_0'=8,'sp_1'=8,'sp_2'=2,'tp'=4] {'sp_2'}, dimensions={0} | all-to-all | bytes 65536 | tf_op jit(solution)/shard_map/all_to_all | solution.py:44
  53.0 16.3 %all-to-all-start.5 = ((f32[64,1,64]{2,1,0:T(1,128)}), f32[64,1,64]{2,1,0:T(1,128)S(1)}, u32[]{:S(2)}, u32[]{:S(2)}) async-start(f32[64,1,64]{2,1,0:T(1,128)} %bitcast.64), calls=%async_computation.5 | async-start | bytes 65536 | tf_op jit(solution)/shard_map/all_to_all | solution.py:51
  69.3 2.1 %convolution_multiply_fusion = f32[256,1024]{1,0:T(8,128)} fusion(bf16[1024,1024]{1,0:T(8,128)(2,1)S(1)} %copy-done, f32[1024,256]{1,0:T(8,128)S(1)} %copy-done.2, f32[256]{0:T(256)S(1)} %copy-done.5, f32[1024]{0:T(1024)S(1)} %get-tuple-element.79, f32[1024]{0:T(1024)S(1)} %get-tuple-element.78), kind=kOutput, calls=%fused_computation | convolution fusion | flops 539230208 | bytes 4203520 | tf_op jit(solution)/shard_map/dot_general | solution.py:161
  71.4 1.8 %reshape_reshape.7 = f32[64,2,2,1024]{3,2,1,0:T(2,128)S(1)} reshape(f32[256,1024]{1,0:T(8,128)} %convolution_multiply_fusion) | data formatting | bytes 2097152 | tf_op jit(solution)/shard_map/reshape;reshape | solution.py:39
  73.2 1.1 copy.35
  74.4 5.7 %all-to-all-done.5 = f32[64,1,64]{2,1,0:T(1,128)S(1)} async-done(((f32[64,1,64]{2,1,0:T(1,128)}), f32[64,1,64]{2,1,0:T(1,128)S(1)}, u32[]{:S(2)}, u32[]{:S(2)}) %all-to-all-start.5) | async-done | bytes 16416 | tf_op jit(solution)/shard_map/all_to_all | solution.py:51
  80.0 5.3 %all-to-all-start.2 = ((f32[2,64,2,1024]{3,2,1,0:T(2,128)}), f32[2,64,2,1024]{3,2,1,0:T(2,128)S(1)}, u32[]{:S(2)}, u32[]{:S(2)}) async-start(f32[2,64,2,1024]{3,2,1,0:T(2,128)} %bitcast.73), calls=%async_computation.2 | async-start | bytes 2097152 | tf_op jit(solution)/shard_map/all_to_all | solution.py:44
  85.5 1.7 %all-to-all-done.2 = f32[2,64,2,1024]{3,2,1,0:T(2,128)S(1)} async-done(((f32[2,64,2,1024]{3,2,1,0:T(2,128)}), f32[2,64,2,1024]{3,2,1,0:T(2,128)S(1)}, u32[]{:S(2)}, u32[]{:S(2)}) %all-to-all-start.2) | async-done | bytes 1048608 | tf_op jit(solution)/shard_map/all_to_all | solution.py:44
  87.8 5.8 %all-to-all-start.6 = ((f32[64,1,64]{2,1,0:T(1,128)}), f32[64,1,64]{2,1,0:T(1,128)S(1)}, u32[]{:S(2)}, u32[]{:S(2)}) async-start(f32[64,1,64]{2,1,0:T(1,128)} %broadcast_in_dim.15), calls=%async_computation.6 | async-start | bytes 65536 | tf_op jit(solution)/shard_map/all_to_all | solution.py:19
  93.5 1.8 %reduce_sum.384 = f32[64,2,1024]{2,1,0:T(2,128)} reduce(f32[2,64,2,1024]{3,2,1,0:T(2,128)S(1)} %all-to-all-done.2, f32[]{:T(128)} %constant.6.clone.1), dimensions={0}, to_apply=%region_6.7 | reduce | flops 131072 | bytes 1572868 | tf_op jit(solution)/shard_map/reduce_sum | solution.py:45
  95.3 3.2 %concatenate.32 = f32[1084,256]{1,0:T(8,128)S(1)} concatenate(f32[30,256]{1,0:T(8,128)S(1)} %broadcast_in_dim.14, f32[1024,256]{1,0:T(8,128)} %copy-done.1, f32[30,256]{1,0:T(8,128)S(1)} %broadcast_in_dim.14), dimensions={0} | concatenate | bytes 2220032 | tf_op jit(solution)/shard_map/concatenate | solution.py:144
  98.5 5.7 %all-to-all-done.6 = f32[64,1,64]{2,1,0:T(1,128)S(1)} async-done(((f32[64,1,64]{2,1,0:T(1,128)}), f32[64,1,64]{2,1,0:T(1,128)S(1)}, u32[]{:S(2)}, u32[]{:S(2)}) %all-to-all-start.6) | async-done | bytes 16416 | tf_op jit(solution)/shard_map/all_to_all | solution.py:19
  104.3 5.2 %all_to_all.49 = f32[2,1,4096]{2,1,0:T(1,128)S(1)} all-to-all(f32[2,1,4096]{2,1,0:T(1,128)S(1)} %reshape.54), channel_id=1, replica_groups=mesh['sp_0'=8,'sp_1'=8,'sp_2'=2,'tp'=4] {'sp_2'}, dimensions={0} | all-to-all | bytes 65536 | tf_op jit(solution)/shard_map/all_to_all | solution.py:19
  109.5 5.7 %all-to-all-start.3 = ((f32[64,2,1024]{2,1,0:T(2,128)}), f32[64,2,1024]{2,1,0:T(2,128)}, u32[]{:S(2)}, u32[]{:S(2)}) async-start(f32[64,2,1024]{2,1,0:T(2,128)} %reduce_sum.384), calls=%async_computation.3 | async-start | bytes 1048576 | tf_op jit(solution)/shard_map/all_to_all | solution.py:51
  115.2 5.4 %fusion.2 = f32[1054,256]{1,0:T(8,128)S(1)} fusion(f32[1084,256]{1,0:T(8,128)S(1)} %concatenate.32, f32[1024,256]{1,0:T(8,128)} %copy-done.1, f32[256]{0:T(256)S(1)} %bitcast.137, f32[256]{0:T(256)S(1)} %bitcast.139, f32[256]{0:T(256)S(1)} %bitcast.81, f32[256]{0:T(256)S(1)} %bitcast.83, f32[256]{0:T(256)S(1)} %bitcast.85, f32[256]{0:T(256)S(1)} %bitcast.87, ...), kind=kLoop, calls=%fused_computation.5 | loop fusion | flops 16459264 | bytes 33459200 | tf_op jit(solution)/shard_map/add | solution.py:148
  120.6 2.7 %collective-permute-start.2 = (f32[30,256]{1,0:T(8,128)S(1)}, f32[30,256]{1,0:T(8,128)S(1)}, u32[]{:S(2)}, u32[]{:S(2)}) collective-permute-start(f32[30,256]{1,0:T(8,128)S(1)} %slice.548), channel_id=1, source_target_pairs={{4,0},{8,4},{12,8},{16,12},{20,16},{24,20},{28,24},{32,28},{36,32}... | collective-permute-start | bytes 92168 | tf_op jit(solution)/shard_map/ppermute | solution.py:14
  123.4 5.4 %collective-permute-done.2 = f32[30,256]{1,0:T(8,128)S(1)} collective-permute-done((f32[30,256]{1,0:T(8,128)S(1)}, f32[30,256]{1,0:T(8,128)S(1)}, u32[]{:S(2)}, u32[]{:S(2)}) %collective-permute-start.2) | collective-permute-done | bytes 30752 | tf_op jit(solution)/shard_map/ppermute | solution.py:14
  128.7 1.4 %multiply_convert_fusion.1 = (bf16[1024,256]{1,0:T(8,128)(2,1)}, bf16[1024,256]{1,0:T(8,128)(2,1)}) fusion(bf16[1024,256]{1,0:T(8,128)(2,1)S(1)} %copy-done.3, f32[30,256]{1,0:T(8,128)S(1)} %slice_add_fusion, f32[994,256]{1,0:T(8,128)S(1)} %slice.546, bf16[1024,256]{1,0:T(8,128)(2,1)S(1)} %copy-done.4), kind=kLoop, calls=%fused_computation.98 | loop fusion | flops 3407872 | bytes 3145728 | tf_op jit(solution)/shard_map/convert_element_type | solution.py:159
  132.7 1.8 %reduce_sum.385 = f32[2,1024]{1,0:T(2,128)} reduce(f32[64,2,1024]{2,1,0:T(2,128)} %all-to-all-done.3, f32[]{:T(128)} %constant.6.clone.1), dimensions={0}, to_apply=%region_7.8 | reduce | flops 129024 | bytes 532484 | tf_op jit(solution)/shard_map/reduce_sum | solution.py:51
  (51 shorter events, 8.1 us)
Async XLA Ops:
  0.6 25.1 %copy-start = (bf16[1024,1024]{1,0:T(8,128)(2,1)S(1)}, bf16[1024,1024]{1,0:T(8,128)(2,1)}, u32[]{:S(2)}) copy-start(bf16[1024,1024]{1,0:T(8,128)(2,1)} %param.11) | copy-start | bytes 6291460
  1.5 9.2 %collective-permute-start = (bf16[30,256]{1,0:T(8,128)(2,1)S(1)}, bf16[30,256]{1,0:T(8,128)(2,1)S(1)}, u32[]{:S(2)}, u32[]{:S(2)}) collective-permute-start(bf16[30,256]{1,0:T(8,128)(2,1)S(1)} %slice.380), channel_id=1, source_target_pairs={{0,4},{4,8},{8,12},{12,16},{16,20},{20,24},{24,28},{28,32},{32,36}... | collective-permute-start | bytes 46088 | tf_op jit(solution)/shard_map/ppermute | solution.py:14
  6.8 5.5 %collective-permute-start.1 = (bf16[30,256]{1,0:T(8,128)(2,1)S(1)}, bf16[30,256]{1,0:T(8,128)(2,1)S(1)}, u32[]{:S(2)}, u32[]{:S(2)}) collective-permute-start(bf16[30,256]{1,0:T(8,128)(2,1)S(1)} %slice.381), channel_id=1, source_target_pairs={{0,4},{4,8},{8,12},{12,16},{16,20},{20,24},{24,28},{28,32},{32,36}... | collective-permute-start | bytes 46088 | tf_op jit(solution)/shard_map/ppermute | solution.py:14
  13.9 11.9 %copy-start.5 = (f32[256]{0:T(256)S(1)}, f32[256]{0:T(256)}, u32[]{:S(2)}) copy-start(f32[256]{0:T(256)} %param.9) | copy-start | bytes 3076
  29.9 7.5 %all-to-all-start.1 = ((f32[4,1,2048]{2,1,0:T(1,128)}), f32[4,1,2048]{2,1,0:T(1,128)S(1)}, u32[]{:S(2)}, u32[]{:S(2)}) async-start(f32[4,1,2048]{2,1,0:T(1,128)} %broadcast_in_dim.13), calls=%async_computation.1 | async-start | bytes 65536 | tf_op jit(solution)/shard_map/all_to_all | solution.py:19
  41.8 1.7 %copy-start.1 = (f32[1024,256]{1,0:T(8,128)}, f32[1024,256]{1,0:T(8,128)S(1)}, u32[]{:S(2)}) copy-start(f32[1024,256]{1,0:T(8,128)S(1)} %get-tuple-element.41) | copy-start | bytes 3145732
  43.5 25.7 %copy-start.2 = (f32[1024,256]{1,0:T(8,128)S(1)}, f32[1024,256]{1,0:T(8,128)}, u32[]{:S(2)}) copy-start(f32[1024,256]{1,0:T(8,128)} %get-tuple-element.42) | copy-start | bytes 3145732
  53.0 27.1 %all-to-all-start.5 = ((f32[64,1,64]{2,1,0:T(1,128)}), f32[64,1,64]{2,1,0:T(1,128)S(1)}, u32[]{:S(2)}, u32[]{:S(2)}) async-start(f32[64,1,64]{2,1,0:T(1,128)} %bitcast.64), calls=%async_computation.5 | async-start | bytes 65536 | tf_op jit(solution)/shard_map/all_to_all | solution.py:51
  80.0 7.1 %all-to-all-start.2 = ((f32[2,64,2,1024]{3,2,1,0:T(2,128)}), f32[2,64,2,1024]{3,2,1,0:T(2,128)S(1)}, u32[]{:S(2)}, u32[]{:S(2)}) async-start(f32[2,64,2,1024]{3,2,1,0:T(2,128)} %bitcast.73), calls=%async_computation.2 | async-start | bytes 2097152 | tf_op jit(solution)/shard_map/all_to_all | solution.py:44
  87.8 16.4 %all-to-all-start.6 = ((f32[64,1,64]{2,1,0:T(1,128)}), f32[64,1,64]{2,1,0:T(1,128)S(1)}, u32[]{:S(2)}, u32[]{:S(2)}) async-start(f32[64,1,64]{2,1,0:T(1,128)} %broadcast_in_dim.15), calls=%async_computation.6 | async-start | bytes 65536 | tf_op jit(solution)/shard_map/all_to_all | solution.py:19
  109.5 23.2 %all-to-all-start.3 = ((f32[64,2,1024]{2,1,0:T(2,128)}), f32[64,2,1024]{2,1,0:T(2,128)}, u32[]{:S(2)}, u32[]{:S(2)}) async-start(f32[64,2,1024]{2,1,0:T(2,128)} %reduce_sum.384), calls=%async_computation.3 | async-start | bytes 1048576 | tf_op jit(solution)/shard_map/all_to_all | solution.py:51
  120.6 8.1 %copy-start.3 = (bf16[1024,256]{1,0:T(8,128)(2,1)S(1)}, bf16[1024,256]{1,0:T(8,128)(2,1)}, u32[]{:S(2)}) copy-start(bf16[1024,256]{1,0:T(8,128)(2,1)} %param.6) | copy-start | bytes 1572868
  120.6 8.1 %copy-start.4 = (bf16[1024,256]{1,0:T(8,128)(2,1)S(1)}, bf16[1024,256]{1,0:T(8,128)(2,1)}, u32[]{:S(2)}) copy-start(bf16[1024,256]{1,0:T(8,128)(2,1)} %param.7) | copy-start | bytes 1572868
  120.6 8.1 %collective-permute-start.2 = (f32[30,256]{1,0:T(8,128)S(1)}, f32[30,256]{1,0:T(8,128)S(1)}, u32[]{:S(2)}, u32[]{:S(2)}) collective-permute-start(f32[30,256]{1,0:T(8,128)S(1)} %slice.548), channel_id=1, source_target_pairs={{4,0},{8,4},{12,8},{16,12},{20,16},{24,20},{28,24},{32,28},{36,32}... | collective-permute-start | bytes 92168 | tf_op jit(solution)/shard_map/ppermute | solution.py:14
where the time goes:
time: 137 us; the launch traced here: 134 us
  starting transfers between devices  45.5 us (33%)
  other arithmetic  25.4 us (19%)
  waiting for transfers between devices  24.4 us (18%)
  blocking collectives  18.9 us (14%)
  local copies, waits for them, and re-layouts  13.7 us (10%)
  matrix products  5.6 us (4%)
    all_to_all x2, starting transfers between devices, sum_by_axis(): return jnp.sum(lax.all_to_all(own, far, 0, 0, tiled=True), axis=0)  22 us
    all_to_all x2, blocking collectives, sent_to_all(): lax.all_to_all(jnp.broadcast_to(array[None], (peers, *array.shape)), axis...  11.9 us
    all_to_all x2, waiting for transfers between devices, sent_to_all(): lax.all_to_all(jnp.broadcast_to(array[None], (peers, *array.shape)), axis...  9.93 us
    ppermute x3, starting transfers between devices, from_behind(): return lax.ppermute(block, axis, route)  9.14 us
    all_to_all x2, starting transfers between devices, sent_to_all(): lax.all_to_all(jnp.broadcast_to(array[None], (peers, *array.shape)), axis...  9.03 us
    all_to_all x1, blocking collectives, sent_and_summed(): tiles = lax.all_to_all(in_blocks(array, dim, peers), axis, 0, 0, tiled=True)  7.08 us
    ppermute x3, waiting for transfers between devices, from_behind(): return lax.ppermute(block, axis, route)  6.91 us
    reduce_sum x2, other arithmetic, per_device(): jnp.sum(convolved_gradient * glu_out[tap:tap + row_count], axis=0)  6.03 us
  transfers between devices with their start and end apart: 8, of which 7 were waited for; matrix products, arithmetic and copies ran while one was open for 16% of the time, Pallas kernels for 0%

commit v1 on v0

v1 whole, which is shorter than its diff:
```python
import jax
import jax.numpy as jnp
from jax import lax
from jax.sharding import Mesh
from jax.sharding import PartitionSpec as P

SP = ("z", "y", "core")
F32, BF16 = jnp.float32, jnp.bfloat16


def shifted(block, distance):
    devices = range(lax.axis_size(SP))
    route = [(i - distance, i) for i in devices if i - distance in devices]
    return lax.ppermute(block, SP, route)


def swapped(block):
    return lax.ppermute(block, "core", [(0, 1), (1, 0)])


def over_tp(array):
    peers = lax.axis_size("tp")
    sent = jnp.broadcast_to(array[None], (peers, *array.shape))
    return jnp.sum(lax.all_to_all(sent, "tp", 0, 0, tiled=True), axis=0)


def per_device(glu_value, glu_gate, conv_taps, channel_gain, proj_weight, out_grad):
    taps = conv_taps.shape[0]
    halo = taps - 1
    rows, width = glu_value.shape
    channels = width * lax.axis_size("tp")
    factor = 1.0 / jnp.sqrt(F32(rows * lax.axis_size(SP)))
    edge = jnp.concatenate([glu_value[rows - 32 :], glu_gate[rows - 32 :]], axis=0)
    edge = shifted(edge, 1)
    value_ext = jnp.concatenate([edge[32 - halo : 32], glu_value], axis=0)
    gate_ext = jnp.concatenate([edge[64 - halo :], glu_gate], axis=0)
    glu_out = value_ext.astype(F32) * jax.nn.sigmoid(gate_ext.astype(F32))
    conv = jnp.zeros((rows, width), F32)
    for tap in range(taps):
        conv = conv + conv_taps[tap] * glu_out[tap : tap + rows]
    sums = over_tp(jnp.stack([jnp.sum(conv, axis=1), jnp.sum(conv * conv, axis=1)]))
    mean = (sums[0] / channels)[:, None]
    rstd = lax.rsqrt((sums[1] / channels)[:, None] - mean * mean + 1e-05)
    xhat = (conv - mean) * rstd
    normed = xhat * channel_gain
    sig = jax.nn.sigmoid(normed)
    activ = (normed * sig).astype(BF16)
    act_grad = lax.dot_general(
        out_grad, proj_weight, (((1,), (1,)), ((), ())), preferred_element_type=F32
    )
    norm_grad = act_grad * sig * (1.0 + normed * (1.0 - sig))
    xhat_grad = norm_grad * channel_gain
    sums2 = over_tp(jnp.stack([jnp.sum(xhat_grad, axis=1), jnp.sum(xhat_grad * xhat, axis=1)]))
    conv_grad = rstd * (
        xhat_grad - (sums2[0] / channels)[:, None] - xhat * (sums2[1] / channels)[:, None]
    )
    z, y, i = 8, 8, 2
    me = lax.axis_index("core")
    row = lax.broadcasted_iota(jnp.int32, (width, width), 0)
    col = lax.broadcasted_iota(jnp.int32, (width, width), 1)
    half = width // 2
    source = (col % half) // i * (2 * i) + ((col // half) ^ me) * i + col % i
    order = (row == source).astype(BF16)
    activ = jnp.dot(activ, order, preferred_element_type=F32).astype(BF16)
    proj = lax.dot_general(
        activ, out_grad, (((0,), (0,)), ((), ())), preferred_element_type=F32
    )
    proj = proj[:half] + swapped(proj[half:])
    small = jnp.concatenate(
        [
            jnp.sum(conv_grad * glu_out[tap : tap + rows], axis=0)[None]
            for tap in range(taps)
        ]
        + [jnp.sum(norm_grad * xhat, axis=0)[None]],
        axis=0,
    )
    small = small + swapped(small)
    outs = channels
    first = jnp.concatenate(
        [
            proj.reshape(z, y * i, outs).astype(BF16),
            jnp.broadcast_to(
                jnp.concatenate([small[:16], small[16:]], axis=1).astype(BF16)[None], (z, 16, 512)
            ),
        ],
        axis=2,
    )
    first = jnp.sum(lax.all_to_all(first, "z", 0, 0, tiled=True).astype(F32), axis=0)
    proj = first[:, :outs].reshape(y, i * outs)
    small = first[:, outs:].reshape(1, 16 * 512)
    second = jnp.concatenate([proj, jnp.broadcast_to(small, (y, 16 * 512))], axis=1)[:, None]
    second = jnp.sum(lax.all_to_all(second, "y", 0, 0, tiled=True), axis=0)[0] * factor
    proj_grad = second[: i * outs].reshape(i, outs)
    small = second[i * outs :].reshape(16, 2, width).swapaxes(0, 1).reshape(32, width)
    taps_grad, gain_grad = small[:taps], small[taps]
    returned = shifted(conv_grad[:32], -1)
    grad_ext = jnp.concatenate([conv_grad, returned[:halo]], axis=0)
    glu_grad = jnp.zeros((rows, width), F32)
    for tap in range(taps):
        glu_grad = glu_grad + conv_taps[tap] * grad_ext[halo - tap : halo - tap + rows]
    value_f = glu_value.astype(F32)
    gate_sig = jax.nn.sigmoid(glu_gate.astype(F32))
    value_grad = (glu_grad * gate_sig).astype(BF16)
    gate_grad = (glu_grad * value_f * gate_sig * (1.0 - gate_sig)).astype(BF16)
    return (value_grad, gate_grad, proj_grad, taps_grad, gain_grad)


def solution(mesh):
    finer = Mesh(mesh.devices.reshape(8, 8, 2, mesh.shape["tp"]), (*SP, "tp"))
    return jax.shard_map(
        per_device,
        mesh=finer,
        in_specs=(P(SP, "tp"), P(SP, "tp"), P(None, "tp"), P("tp"), P("tp", None), P(SP, None)),
        out_specs=(P(SP, "tp"), P(SP, "tp"), P(("tp", *SP), None), P(None, "tp"), P("tp")),
        check_vma=False,
    )
```

time: 137 us -> 107 us (0.78); the launches traced: 134 us -> 106 us
  blocking collectives: 18.9 us -> 0 us
  starting transfers between devices: 45.5 us -> 36.6 us
  local copies, waits for them, and re-layouts: 13.7 us -> 8.04 us
  other arithmetic: 25.4 us -> 29.3 us
    all_to_all x3 -> x0, blocking collectives: 18.9 us -> none  [the longest x2 11.9 us: sent_to_all(): lax.all_to_all(jnp.broadcast_to(array[None], (peers, *array.shape)), axis...]
    all_to_all x5 -> x4, starting transfers between devices: 36.3 us -> 21.9 us  [the longest x1 10.6 us: per_device(): lax.all_to_all(first, 'z', 0, 0, tiled=True).astype(F32)]
    convert_element_type x1 -> x3, other arithmetic: 1.41 us -> 15.3 us  [the longest x1 14.1 us: per_device(): gate_grad = (glu_grad * value_f * gate_sig * (1.0 - gate_sig)).astype(BF16)]
    ppermute x3 -> x4, starting transfers between devices: 9.14 us -> 14.7 us  [the longest x2 7.78 us: swapped(): return lax.ppermute(block, 'core', [(0, 1), (1, 0)])]
    add x2 -> x1, other arithmetic: 5.38 us -> 0.01 us  [per_device(): source = col % half // i * (2 * i) + (col // half ^ me) * i + col % i]
    reduce_sum x9 -> x7, other arithmetic: 15.5 us -> 11.5 us  [the longest x2 6.03 us: per_device(): jnp.sum(conv_grad * glu_out[tap:tap + rows], axis=0)[None]]
    all_to_all x5 -> x4, waiting for transfers between devices: 17.5 us -> 20.7 us  [the longest x1 12.2 us: per_device(): lax.all_to_all(first, 'z', 0, 0, tiled=True).astype(F32)]
    ppermute x3 -> x4, waiting for transfers between devices: 6.91 us -> 3.74 us  [the longest x2 1.91 us: shifted(): return lax.ppermute(block, SP, route)]
  transfers between devices with their start and end apart: 8 -> 8, of which waited for: 7 -> 5; matrix products, arithmetic and copies ran while one was open for 16% -> 20% of each run, Pallas kernels for 0% -> 0%
where the time goes in v1:
time: 107 us; the launch traced here: 106 us
  starting transfers between devices  36.6 us (34%)
  other arithmetic  29.3 us (27%)
  waiting for transfers between devices  24.5 us (23%)
  local copies, waits for them, and re-layouts  8.04 us (8%)
  matrix products  5.93 us (6%)
  between operations  1.71 us (2%)
    convert_element_type x1, other arithmetic, per_device(): gate_grad = (glu_grad * value_f * gate_sig * (1.0 - gate_sig)).astype(BF16)  14.1 us
    all_to_all x1, waiting for transfers between devices, per_device(): lax.all_to_all(first, 'z', 0, 0, tiled=True).astype(F32)  12.2 us
    all_to_all x1, starting transfers between devices, per_device(): lax.all_to_all(first, 'z', 0, 0, tiled=True).astype(F32)  10.6 us
    all_to_all x2, waiting for transfers between devices, over_tp(): return jnp.sum(lax.all_to_all(sent, 'tp', 0, 0, tiled=True), axis=0)  8.5 us
    ppermute x2, starting transfers between devices, swapped(): return lax.ppermute(block, 'core', [(0, 1), (1, 0)])  7.78 us
    ppermute x2, starting transfers between devices, shifted(): return lax.ppermute(block, SP, route)  6.89 us
    all_to_all x2, starting transfers between devices, over_tp(): return jnp.sum(lax.all_to_all(sent, 'tp', 0, 0, tiled=True), axis=0)  6.53 us
    reduce_sum x2, other arithmetic, per_device(): jnp.sum(conv_grad * glu_out[tap:tap + rows], axis=0)[None]  6.03 us
  transfers between devices with their start and end apart: 8, of which 5 were waited for; matrix products, arithmetic and copies ran while one was open for 20% of the time, Pallas kernels for 0%

profile of v1, /device:TPU:1, one launch (start us, length us, event | category | flops | bytes accessed | tf_op | source)
XLA Modules:
  0.0 106.0 jit_solution(12450380515493822043)
XLA Ops:
  0.6 0.9 slice.409
  1.5 0.7 slice.410
  2.2 4.6 %collective-permute-start = (bf16[64,256]{1,0:T(8,128)(2,1)S(1)}, bf16[64,256]{1,0:T(8,128)(2,1)S(1)}, u32[]{:S(2)}, u32[]{:S(2)}) collective-permute-start(bf16[64,256]{1,0:T(8,128)(2,1)S(1)} %pad_maximum_fusion.3), channel_id=1, source_target_pairs={{0,4},{4,8},{8,12},{12,16},{16,20},{20,24},{24,28},{28,32},{32,36}... | collective-permute-start | bytes 98312 | tf_op jit(solution)/shard_map/ppermute | solution.py:14
  6.8 1.0 fusion.163
  7.9 1.0 fusion.162
  9.1 1.9 %collective-permute-done = bf16[64,256]{1,0:T(8,128)(2,1)S(1)} collective-permute-done((bf16[64,256]{1,0:T(8,128)(2,1)S(1)}, bf16[64,256]{1,0:T(8,128)(2,1)S(1)}, u32[]{:S(2)}, u32[]{:S(2)}) %collective-permute-start) | collective-permute-done | bytes 32800 | tf_op jit(solution)/shard_map/ppermute | solution.py:14
  11.1 1.6 %divide_multiply_fusion = f32[1054,256]{1,0:T(8,128)S(1)} fusion(bf16[1024,256]{1,0:T(8,128)(2,1)} %param.6, bf16[30,256]{1,0:T(8,128)(2,1)S(1)} %get-tuple-element.77, bf16[1024,256]{1,0:T(8,128)(2,1)} %param.7, bf16[30,256]{1,0:T(8,128)(2,1)S(1)} %get-tuple-element.76), kind=kLoop, calls=%fused_computation.33 | loop fusion | flops 3237888 | bytes 2158592 | tf_op jit(solution)/shard_map/mul | solution.py:37
  12.9 5.1 %fusion.160 = (f32[1024]{0:T(1024)S(1)}, f32[1024]{0:T(1024)S(1)}, f32[1024,256]{1,0:T(8,128)}) fusion(f32[1054,256]{1,0:T(8,128)S(1)} %divide_multiply_fusion, f32[256]{0:T(256)S(1)} %bitcast.117, f32[256]{0:T(256)S(1)} %bitcast.119, f32[256]{0:T(256)S(1)} %bitcast.123, f32[256]{0:T(256)S(1)} %bitcast.125, f32[256]{0:T(256)S(1)} %bitcast.127, ...), kind=kLoop, calls=%fused_computation.247 | loop fusion | flops 16775168 | bytes 33594368 | tf_op jit(solution)/shard_map/reduce_sum | solution.py:41
  18.1 0.6 broadcast_in_dim.130
  18.7 3.3 %all-to-all-start = ((f32[4,2,1024]{2,1,0:T(2,128)}), f32[4,2,1024]{2,1,0:T(2,128)S(1)}, u32[]{:S(2)}, u32[]{:S(2)}) async-start(f32[4,2,1024]{2,1,0:T(2,128)} %broadcast_in_dim.130), calls=%async_computation | async-start | bytes 65536 | tf_op jit(solution)/shard_map/all_to_all | solution.py:24
  22.0 4.3 %all-to-all-done = f32[4,2,1024]{2,1,0:T(2,128)S(1)} async-done(((f32[4,2,1024]{2,1,0:T(2,128)}), f32[4,2,1024]{2,1,0:T(2,128)S(1)}, u32[]{:S(2)}, u32[]{:S(2)}) %all-to-all-start) | async-done | bytes 32800 | tf_op jit(solution)/shard_map/all_to_all | solution.py:24
  26.3 3.5 %multiply_reduce_fusion = (f32[256]{0:T(256)S(1)}, f32[1024]{0:T(1024)S(1)}, f32[1024]{0:T(1024)S(1)}, f32[1024,256]{1,0:T(8,128)}) fusion(f32[1024,256]{1,0:T(8,128)} %get-tuple-element.44, f32[1024]{0:T(1024)S(1)} %bitcast.87, f32[1024]{0:T(1024)S(1)} %add_rsqrt_fusion, f32[256]{0:T(256)S(1)} %copy-done.48, bf16[1024,1024]{1,0:T(8,128)(2,1)S(1)} %copy-done, ...), kind=kOutput, calls=%fused_computation.135 | convolution fusion | flops 541325056 | bytes 4737024 | tf_op jit(solution)/shard_map/dot_general | solution.py:48
  29.9 0.6 broadcast_in_dim.131
  30.5 3.3 %all-to-all-start.1 = ((f32[4,2,1024]{2,1,0:T(2,128)}), f32[4,2,1024]{2,1,0:T(2,128)S(1)}, u32[]{:S(2)}, u32[]{:S(2)}) async-start(f32[4,2,1024]{2,1,0:T(2,128)} %broadcast_in_dim.131), calls=%async_computation.1 | async-start | bytes 65536 | tf_op jit(solution)/shard_map/all_to_all | solution.py:24
  33.8 4.2 %all-to-all-done.1 = f32[4,2,1024]{2,1,0:T(2,128)S(1)} async-done(((f32[4,2,1024]{2,1,0:T(2,128)}), f32[4,2,1024]{2,1,0:T(2,128)S(1)}, u32[]{:S(2)}, u32[]{:S(2)}) %all-to-all-start.1) | async-done | bytes 32800 | tf_op jit(solution)/shard_map/all_to_all | solution.py:24
  38.1 4.3 %multiply_reduce_fusion.1 = (f32[256]{0:T(256)S(1)}, f32[256]{0:T(256)S(1)}, f32[256]{0:T(256)S(1)}, f32[256]{0:T(256)S(1)}, f32[256]{0:T(256)S(1)}, /*index=5*/...) fusion(f32[1054,256]{1,0:T(8,128)S(1)} %divide_multiply_fusion,, ...), kind=kLoop, calls=%fused_computation.136 | loop fusion | flops 11267584 | bytes 22055936 | tf_op jit(solution)/shard_map/reduce_sum | solution.py:71
  42.4 1.7 %multiply_reduce_fusion.19 = (f32[256]{0:T(256)S(1)}, f32[256]{0:T(256)S(1)}, f32[256]{0:T(256)S(1)}, f32[256]{0:T(256)S(1)}, f32[256]{0:T(256)S(1)}, /*index=5*...) fusion(f32[1024,256]{1,0:T(8,128)S(1)} %get-tuple-element.41, ...), kind=kLoop, calls=%fused_computation.154 | loop fusion | flops 6812416 | bytes 14693376 | tf_op jit(solution)/shard_map/reduce_sum | solution.py:71
  44.2 5.9 %collective-permute-start.3 = (f32[32,256]{1,0:T(8,128)S(1)}, f32[32,256]{1,0:T(8,128)S(1)}, u32[]{:S(2)}, u32[]{:S(2)}) collective-permute-start(f32[32,256]{1,0:T(8,128)S(1)} %concatenate.33), channel_id=1, source_target_pairs={{0,4},{4,0},{1,5},{5,1},{2,6},{6,2},{3,7},{7,3},{8,12},{12,8},{9,1... | collective-permute-start | bytes 98312 | tf_op jit(solution)/shard_map/ppermute | solution.py:18
  50.1 2.4 %fusion.1 = f32[256,1024]{1,0:T(8,128)S(1)} fusion(bf16[1024,1024]{1,0:T(8,128)(2,1)S(1)} %copy-done, f32[1024,256]{1,0:T(8,128)} %get-tuple-element.44, f32[256]{0:T(256)S(1)} %copy-done.48, f32[1024]{0:T(1024)S(1)} %bitcast.89, f32[1024]{0:T(1024)S(1)} %add_rsqrt_fusion, s32[256]{0:T(256)S(1)} %get-tuple-element.88, s32[256]{0:T(256)S(1)} %get-tuple-element.91, ...), kind=kOutput, calls=%fused_computation.32 | convolution fusion | flops 675020800 | bytes 4210436 | tf_op jit(solution)/shard_map/dot_general | solution.py:65
  52.6 1.9 %collective-permute-start.2 = (f32[128,1024]{1,0:T(8,128)S(1)}, f32[128,1024]{1,0:T(8,128)S(1)}, u32[]{:S(2)}, u32[]{:S(2)}) collective-permute-start(f32[128,1024]{1,0:T(8,128)S(1)} %slice.620), channel_id=1, source_target_pairs={{0,4},{4,0},{1,5},{5,1},{2,6},{6,2},{3,7},{7,3},{8,12},{12,8},{9,1... | collective-permute-start | bytes 1572872 | tf_op jit(solution)/shard_map/ppermute | solution.py:18
  54.5 1.8 %collective-permute-done.2 = f32[128,1024]{1,0:T(8,128)S(1)} collective-permute-done((f32[128,1024]{1,0:T(8,128)S(1)}, f32[128,1024]{1,0:T(8,128)S(1)}, u32[]{:S(2)}, u32[]{:S(2)}) %collective-permute-start.2) | collective-permute-done | bytes 524320 | tf_op jit(solution)/shard_map/ppermute | solution.py:18
  56.5 0.8 pad_maximum_fusion.1
  57.2 10.6 %all-to-all-start.2 = ((bf16[8,16,1536]{2,1,0:T(8,128)(2,1)}), bf16[8,16,1536]{2,1,0:T(8,128)(2,1)S(1)}, u32[]{:S(2)}, u32[]{:S(2)}) async-start(bf16[8,16,1536]{2,1,0:T(8,128)(2,1)} %pad_maximum_fusion.1), calls=%async_computation.2 | async-start | bytes 786432 | tf_op jit(solution)/shard_map/all_to_all | solution.py:88
  67.9 0.6 slice.559
  68.5 2.3 %collective-permute-start.1 = (f32[32,256]{1,0:T(8,128)}, f32[32,256]{1,0:T(8,128)}, u32[]{:S(2)}, u32[]{:S(2)}) collective-permute-start(f32[32,256]{1,0:T(8,128)} %slice.559), channel_id=1, source_target_pairs={{4,0},{8,4},{12,8},{16,12},{20,16},{24,20},{28,24},{32,28},{36,32}... | collective-permute-start | bytes 98312 | tf_op jit(solution)/shard_map/ppermute | solution.py:14
  70.8 12.2 %all-to-all-done.2 = bf16[8,16,1536]{2,1,0:T(8,128)(2,1)S(1)} async-done(((bf16[8,16,1536]{2,1,0:T(8,128)(2,1)}), bf16[8,16,1536]{2,1,0:T(8,128)(2,1)S(1)}, u32[]{:S(2)}, u32[]{:S(2)}) %all-to-all-start.2) | async-done | bytes 393248 | tf_op jit(solution)/shard_map/all_to_all | solution.py:88
  83.4 0.9 broadcast_in_dim.167
  84.3 4.7 %all-to-all-start.3 = ((f32[8,1,10240]{2,1,0:T(1,128)}), f32[8,1,10240]{2,1,0:T(1,128)S(1)}, u32[]{:S(2)}, u32[]{:S(2)}) async-start(f32[8,1,10240]{2,1,0:T(1,128)} %broadcast_in_dim.167), calls=%async_computation.3 | async-start | bytes 655360 | tf_op jit(solution)/shard_map/all_to_all | solution.py:92
  89.3 14.1 %multiply_convert_fusion.1 = (bf16[1024,256]{1,0:T(8,128)(2,1)}, f32[1024,256]{1,0:T(8,128)S(1)}) fusion(bf16[1024,256]{1,0:T(8,128)(2,1)} %param.6, bf16[1024,256]{1,0:T(8,128)(2,1)} %param.7, f32[1024,256]{1,0:T(8,128)S(1)} %copy-done.2, f32[256]{0:T(256)S(1)} %bitcast.118, f32[30,256]{1,0:T(8,128)} %bitcast.81, f32[256]{0:T(256)S(1)} %bitcast.120, ...), kind=kLoop, calls=%fused_computation.168 | loop fusion | flops 26476544 | bytes 3732480 | tf_op jit(solution)/shard_map/convert_element_type | solution.py:104
  103.4 1.1 %multiply_convert_fusion.2 = bf16[1024,256]{1,0:T(8,128)(2,1)} fusion(f32[1024,256]{1,0:T(8,128)S(1)} %get-tuple-element.43, bf16[1024,256]{1,0:T(8,128)(2,1)S(1)} %copy-done.3), kind=kLoop, calls=%fused_computation.169 | loop fusion | flops 1572864 | bytes 2097152 | tf_op jit(solution)/shard_map/convert_element_type | solution.py:103
  104.8 0.6 slice.517
  105.4 0.6 slice.628
  (135 shorter events, 1.0 us)
Async XLA Ops:
  0.6 25.7 %copy-start = (bf16[1024,1024]{1,0:T(8,128)(2,1)S(1)}, bf16[1024,1024]{1,0:T(8,128)(2,1)}, u32[]{:S(2)}) copy-start(bf16[1024,1024]{1,0:T(8,128)(2,1)} %param.11) | copy-start | bytes 6291460
  2.2 8.8 %collective-permute-start = (bf16[64,256]{1,0:T(8,128)(2,1)S(1)}, bf16[64,256]{1,0:T(8,128)(2,1)S(1)}, u32[]{:S(2)}, u32[]{:S(2)}) collective-permute-start(bf16[64,256]{1,0:T(8,128)(2,1)S(1)} %pad_maximum_fusion.3), channel_id=1, source_target_pairs={{0,4},{4,8},{8,12},{12,16},{16,20},{20,24},{24,28},{28,32},{32,36}... | collective-permute-start | bytes 98312 | tf_op jit(solution)/shard_map/ppermute | solution.py:14
  7.8 4.8 %copy-start.5 = (f32[1,256]{1,0:T(1,128)}, f32[1,256]{1,0:T(1,128)S(1)}, u32[]{:S(2)}) copy-start(f32[1,256]{1,0:T(1,128)S(1)} %get-tuple-element.68) | copy-start | bytes 3076
  7.8 4.8 %copy-start.7 = (f32[1,256]{1,0:T(1,128)}, f32[1,256]{1,0:T(1,128)S(1)}, u32[]{:S(2)}) copy-start(f32[1,256]{1,0:T(1,128)S(1)} %get-tuple-element.69) | copy-start | bytes 3076
  7.8 4.8 %copy-start.9 = (f32[1,256]{1,0:T(1,128)}, f32[1,256]{1,0:T(1,128)S(1)}, u32[]{:S(2)}) copy-start(f32[1,256]{1,0:T(1,128)S(1)} %get-tuple-element.70) | copy-start | bytes 3076
  7.9 4.8 %copy-start.11 = (f32[1,256]{1,0:T(1,128)}, f32[1,256]{1,0:T(1,128)S(1)}, u32[]{:S(2)}) copy-start(f32[1,256]{1,0:T(1,128)S(1)} %get-tuple-element.71) | copy-start | bytes 3076
  12.9 13.4 %copy-start.48 = (f32[256]{0:T(256)S(1)}, f32[256]{0:T(256)}, u32[]{:S(2)}) copy-start(f32[256]{0:T(256)} %param.9) | copy-start | bytes 3076
  18.7 7.5 %all-to-all-start = ((f32[4,2,1024]{2,1,0:T(2,128)}), f32[4,2,1024]{2,1,0:T(2,128)S(1)}, u32[]{:S(2)}, u32[]{:S(2)}) async-start(f32[4,2,1024]{2,1,0:T(2,128)} %broadcast_in_dim.130), calls=%async_computation | async-start | bytes 65536 | tf_op jit(solution)/shard_map/all_to_all | solution.py:24
  30.5 7.5 %all-to-all-start.1 = ((f32[4,2,1024]{2,1,0:T(2,128)}), f32[4,2,1024]{2,1,0:T(2,128)S(1)}, u32[]{:S(2)}, u32[]{:S(2)}) async-start(f32[4,2,1024]{2,1,0:T(2,128)} %broadcast_in_dim.131), calls=%async_computation.1 | async-start | bytes 65536 | tf_op jit(solution)/shard_map/all_to_all | solution.py:24
  44.2 10.3 %collective-permute-start.3 = (f32[32,256]{1,0:T(8,128)S(1)}, f32[32,256]{1,0:T(8,128)S(1)}, u32[]{:S(2)}, u32[]{:S(2)}) collective-permute-start(f32[32,256]{1,0:T(8,128)S(1)} %concatenate.33), channel_id=1, source_target_pairs={{0,4},{4,0},{1,5},{5,1},{2,6},{6,2},{3,7},{7,3},{8,12},{12,8},{9,1... | collective-permute-start | bytes 98312 | tf_op jit(solution)/shard_map/ppermute | solution.py:18
  52.6 3.8 %collective-permute-start.2 = (f32[128,1024]{1,0:T(8,128)S(1)}, f32[128,1024]{1,0:T(8,128)S(1)}, u32[]{:S(2)}, u32[]{:S(2)}) collective-permute-start(f32[128,1024]{1,0:T(8,128)S(1)} %slice.620), channel_id=1, source_target_pairs={{0,4},{4,0},{1,5},{5,1},{2,6},{6,2},{3,7},{7,3},{8,12},{12,8},{9,1... | collective-permute-start | bytes 1572872 | tf_op jit(solution)/shard_map/ppermute | solution.py:18
  56.4 11.4 %copy-start.2 = (f32[1024,256]{1,0:T(8,128)S(1)}, f32[1024,256]{1,0:T(8,128)}, u32[]{:S(2)}) copy-start(f32[1024,256]{1,0:T(8,128)} %copy-done.1) | copy-start | bytes 3145732
  57.2 25.8 %all-to-all-start.2 = ((bf16[8,16,1536]{2,1,0:T(8,128)(2,1)}), bf16[8,16,1536]{2,1,0:T(8,128)(2,1)S(1)}, u32[]{:S(2)}, u32[]{:S(2)}) async-start(bf16[8,16,1536]{2,1,0:T(8,128)(2,1)} %pad_maximum_fusion.1), calls=%async_computation.2 | async-start | bytes 786432 | tf_op jit(solution)/shard_map/all_to_all | solution.py:88
  68.5 20.6 %collective-permute-start.1 = (f32[32,256]{1,0:T(8,128)}, f32[32,256]{1,0:T(8,128)}, u32[]{:S(2)}, u32[]{:S(2)}) collective-permute-start(f32[32,256]{1,0:T(8,128)} %slice.559), channel_id=1, source_target_pairs={{4,0},{8,4},{12,8},{16,12},{20,16},{24,20},{28,24},{32,28},{36,32}... | collective-permute-start | bytes 98312 | tf_op jit(solution)/shard_map/ppermute | solution.py:14
  83.1 6.0 %copy-start.6 = (f32[1,256]{1,0:T(1,128)S(1)}, f32[1,256]{1,0:T(1,128)}, u32[]{:S(2)}) copy-start(f32[1,256]{1,0:T(1,128)} %copy-done.5) | copy-start | bytes 3076
  83.1 6.0 %copy-start.8 = (f32[1,256]{1,0:T(1,128)S(1)}, f32[1,256]{1,0:T(1,128)}, u32[]{:S(2)}) copy-start(f32[1,256]{1,0:T(1,128)} %copy-done.7) | copy-start | bytes 3076
  83.1 6.0 %copy-start.10 = (f32[1,256]{1,0:T(1,128)S(1)}, f32[1,256]{1,0:T(1,128)}, u32[]{:S(2)}) copy-start(f32[1,256]{1,0:T(1,128)} %copy-done.9) | copy-start | bytes 3076
  83.2 6.0 %copy-start.12 = (f32[1,256]{1,0:T(1,128)S(1)}, f32[1,256]{1,0:T(1,128)}, u32[]{:S(2)}) copy-start(f32[1,256]{1,0:T(1,128)} %copy-done.11) | copy-start | bytes 3076
  83.2 6.0 %copy-start.14 = (f32[1,256]{1,0:T(1,128)S(1)}, f32[1,256]{1,0:T(1,128)}, u32[]{:S(2)}) copy-start(f32[1,256]{1,0:T(1,128)} %copy-done.13) | copy-start | bytes 3076
  83.2 6.0 %copy-start.16 = (f32[1,256]{1,0:T(1,128)S(1)}, f32[1,256]{1,0:T(1,128)}, u32[]{:S(2)}) copy-start(f32[1,256]{1,0:T(1,128)} %copy-done.15) | copy-start | bytes 3076
  83.2 6.0 %copy-start.18 = (f32[1,256]{1,0:T(1,128)S(1)}, f32[1,256]{1,0:T(1,128)}, u32[]{:S(2)}) copy-start(f32[1,256]{1,0:T(1,128)} %copy-done.17) | copy-start | bytes 3076
  83.2 6.0 %copy-start.20 = (f32[1,256]{1,0:T(1,128)S(1)}, f32[1,256]{1,0:T(1,128)}, u32[]{:S(2)}) copy-start(f32[1,256]{1,0:T(1,128)} %copy-done.19) | copy-start | bytes 3076
  83.2 6.0 %copy-start.22 = (f32[1,256]{1,0:T(1,128)S(1)}, f32[1,256]{1,0:T(1,128)}, u32[]{:S(2)}) copy-start(f32[1,256]{1,0:T(1,128)} %copy-done.21) | copy-start | bytes 3076
  83.2 6.0 %copy-start.24 = (f32[1,256]{1,0:T(1,128)S(1)}, f32[1,256]{1,0:T(1,128)}, u32[]{:S(2)}) copy-start(f32[1,256]{1,0:T(1,128)} %copy-done.23) | copy-start | bytes 3076
  83.2 6.0 %copy-start.26 = (f32[1,256]{1,0:T(1,128)S(1)}, f32[1,256]{1,0:T(1,128)}, u32[]{:S(2)}) copy-start(f32[1,256]{1,0:T(1,128)} %copy-done.25) | copy-start | bytes 3076
  83.2 6.0 %copy-start.28 = (f32[1,256]{1,0:T(1,128)S(1)}, f32[1,256]{1,0:T(1,128)}, u32[]{:S(2)}) copy-start(f32[1,256]{1,0:T(1,128)} %copy-done.27) | copy-start | bytes 3076
  83.2 6.0 %copy-start.30 = (f32[1,256]{1,0:T(1,128)S(1)}, f32[1,256]{1,0:T(1,128)}, u32[]{:S(2)}) copy-start(f32[1,256]{1,0:T(1,128)} %copy-done.29) | copy-start | bytes 3076
  83.3 6.0 %copy-start.32 = (f32[1,256]{1,0:T(1,128)S(1)}, f32[1,256]{1,0:T(1,128)}, u32[]{:S(2)}) copy-start(f32[1,256]{1,0:T(1,128)} %copy-done.31) | copy-start | bytes 3076
  83.3 6.0 %copy-start.34 = (f32[1,256]{1,0:T(1,128)S(1)}, f32[1,256]{1,0:T(1,128)}, u32[]{:S(2)}) copy-start(f32[1,256]{1,0:T(1,128)} %copy-done.33) | copy-start | bytes 3076
  83.3 6.0 %copy-start.36 = (f32[1,256]{1,0:T(1,128)S(1)}, f32[1,256]{1,0:T(1,128)}, u32[]{:S(2)}) copy-start(f32[1,256]{1,0:T(1,128)} %copy-done.35) | copy-start | bytes 3076
  84.3 20.2 %all-to-all-start.3 = ((f32[8,1,10240]{2,1,0:T(1,128)}), f32[8,1,10240]{2,1,0:T(1,128)S(1)}, u32[]{:S(2)}, u32[]{:S(2)}) async-start(f32[8,1,10240]{2,1,0:T(1,128)} %broadcast_in_dim.167), calls=%async_computation.3 | async-start | bytes 655360 | tf_op jit(solution)/shard_map/all_to_all | solution.py:92
  89.2 14.2 %copy-start.3 = (bf16[1024,256]{1,0:T(8,128)(2,1)S(1)}, bf16[1024,256]{1,0:T(8,128)(2,1)}, u32[]{:S(2)}) copy-start(bf16[1024,256]{1,0:T(8,128)(2,1)} %param.7) | copy-start | bytes 1572868
  (25 other events, 94.5 us)

commit v2 on v1

v2 whole, which is shorter than its diff:
```python
import math

import jax
import jax.numpy as jnp
from jax import lax
from jax.experimental import pallas as pl
from jax.experimental.pallas import tpu as pltpu
from jax.sharding import Mesh
from jax.sharding import PartitionSpec as P

SP = ("z", "y", "core")
F32, BF16 = jnp.float32, jnp.bfloat16
LANES = 128
PAD = 32
NT = (((1,), (1,)), ((), ()))
TN = (((0,), (0,)), ((), ()))


def shifted(block, distance):
    devices = range(lax.axis_size(SP))
    route = [(i - distance, i) for i in devices if i - distance in devices]
    return lax.ppermute(block, SP, route)


def swapped(block):
    return lax.ppermute(block, "core", [(0, 1), (1, 0)])


def near(array):
    return pltpu.with_memory_space_constraint(array, pltpu.VMEM)


def kernel(body, outs, args, scratch=(), aliases=None, name=None, limit=16, smem=0):
    space = pl.BlockSpec(memory_space=pltpu.VMEM)
    return pl.pallas_call(
        body,
        out_shape=[
            pltpu.VMEM(s, d) if where == "near" else jax.ShapeDtypeStruct(s, d) for s, d, where in outs
        ],
        in_specs=[pl.BlockSpec(memory_space=pltpu.SMEM)] * smem + [space] * (len(args) - smem),
        out_specs=[space] * len(outs),
        scratch_shapes=[pltpu.VMEM(s, d) for s, d in scratch],
        input_output_aliases=aliases or {},
        compiler_params=pltpu.CompilerParams(vmem_limit_bytes=limit << 20),
        name=name,
    )(*args)


def lanes(h):
    return slice(h * LANES, (h + 1) * LANES)


def glu_body(value, gate, glu, edge):
    rows = value.shape[0]

    def step(i, carry):
        r = pl.multiple_of(i * 64, 64)
        for h in range(2):
            v = value[pl.ds(r, 64), lanes(h)].astype(F32)
            g = gate[pl.ds(r, 64), lanes(h)].astype(F32)
            glu[h, pl.ds(PAD + r, 64), :] = v * jax.nn.sigmoid(g)
        return carry

    lax.fori_loop(0, rows // 64, step, 0)
    for h in range(2):
        edge[h] = glu[h, rows : rows + PAD, :]


def conv_rows(glu, taps, conv, start, count):
    n = taps.shape[0]
    for h in range(2):
        weights = [jnp.broadcast_to(taps[k : k + 1, lanes(h)], (8, LANES)) for k in range(n)]

        def step(i, carry, h=h, weights=weights):
            for u in range(2):
                r = start + i * 16 + u * 8
                parts = [None, None]
                for k in range(n):
                    term = weights[k] * glu[h, pl.ds(r + PAD + 1 - n + k, 8), :]
                    parts[k % 2] = term if parts[k % 2] is None else parts[k % 2] + term
                conv[h, pl.ds(pl.multiple_of(r, 8), 8), :] = parts[0] + parts[1]
            return carry

        lax.fori_loop(0, count // 16, step, 0)


def split(x):
    high = x.astype(BF16)
    return high, (x - high.astype(F32)).astype(BF16)


def selector(row):
    sub = lax.broadcasted_iota(jnp.int32, (8, LANES), 0)
    return (sub == row).astype(F32).astype(BF16)


def row_sums(pairs):
    total = None
    for row, x in pairs:
        pick = selector(row)
        for part in split(x):
            term = lax.dot_general(pick, part, NT, preferred_element_type=F32)
            total = term if total is None else total + term
    return total


def conv_stats(conv, stats, start, count):
    def step(i, carry):
        r = pl.multiple_of(start + i * 256, 256)
        pairs = []
        for h in range(2):
            c = conv[h, pl.ds(r, 256), :]
            pairs += [(0, c), (1, c * c)]
        stats[:, pl.ds(r, 256)] = row_sums(pairs)
        return carry

    lax.fori_loop(0, count // 256, step, 0)


def conv_body(glu, taps, conv, stats):
    rows = conv.shape[1]
    conv_rows(glu, taps, conv, 256, rows - 256)
    conv_stats(conv, stats, 256, rows - 256)


def head_body(edge, glu_in, taps, conv_in, stats_in, glu, conv, sent, stats):
    for h in range(2):
        glu[h, 0:PAD, :] = edge[h]
    conv_rows(glu, taps, conv, 0, 256)
    conv_stats(conv, stats, 0, 256)
    rows = conv.shape[1]
    for p in range(sent.shape[0]):
        sent[p, :, 0:256] = stats[0:2]
        sent[p, :, 256:rows] = stats_in[0:2, 256:rows]


def column(row):
    return jnp.broadcast_to(row, (LANES, LANES)).T


def norm_body(stats, conv, act_grad, gain, activ, xhat_out, scaled, sums, rstd_out, gain_sum, rows_in):
    peers = stats.shape[0]
    channels = 2 * LANES * peers
    total = stats[0]
    for p in range(1, peers):
        total = total + stats[p]
    mean = total[0:1] * (1.0 / channels)
    rstd = lax.rsqrt(total[1:2] * (1.0 / channels) - mean * mean + 1e-05)
    rstd_out[...] = rstd
    rows_in[0:1, :] = rstd
    rows_in[1:2, :] = mean
    for h in range(2):
        gain_sum[h] = jnp.zeros((8, LANES), F32)

    def step(i, carry):
        r = pl.multiple_of(i * LANES, LANES)
        rs = column(rows_in[0:1, pl.ds(r, LANES)])
        mu = column(rows_in[1:2, pl.ds(r, LANES)])
        pairs = []
        for h in range(2):
            g = gain[0:1, lanes(h)]
            xhat = (conv[h, pl.ds(r, LANES), :] - mu) * rs
            normed = xhat * g
            sig = jax.nn.sigmoid(normed)
            activ[pl.ds(r, LANES), lanes(h)] = (normed * sig).astype(BF16)
            ng = act_grad[pl.ds(r, LANES), lanes(h)] * (sig * (1.0 + normed * (1.0 - sig)))
            gain_sum[h] += jnp.sum((ng * xhat).reshape(16, 8, LANES), axis=0)
            xg = ng * g
            xhat_out[h, pl.ds(r, LANES), :] = xhat
            scaled[h, pl.ds(r, LANES), :] = xg * rs
            pairs += [(0, xg), (1, xg * xhat)]
        out = row_sums(pairs)
        for p in range(peers):
            sums[p, :, pl.ds(r, LANES)] = out[0:2]
        return carry

    lax.fori_loop(0, conv.shape[1] // LANES, step, 0)


def taps_body(sums, rstd, xhat, scaled, glu, gain_sum, grad, small, rows_in):
    peers = sums.shape[0]
    channels = 2 * LANES * peers
    n = small.shape[0] - 1
    rows = grad.shape[1]
    total = sums[0]
    for p in range(1, peers):
        total = total + sums[p]
    rows_in[...] = total * (rstd[...] * (1.0 / channels))

    def step(i, carry):
        r = pl.multiple_of(i * LANES, LANES)
        first = column(rows_in[0:1, pl.ds(r, LANES)])
        second = column(rows_in[1:2, pl.ds(r, LANES)])
        for h in range(2):
            at = pl.ds(r, LANES)
            grad[h, at, :] = scaled[h, at, :] - first - xhat[h, at, :] * second
        return carry

    lax.fori_loop(0, rows // LANES, step, 0)
    for h in range(2):

        def tile(i, acc, h=h):
            r = pl.multiple_of(i * 8, 8)
            c = grad[h, pl.ds(r, 8), :]
            return tuple(
                acc[k] + c * glu[h, pl.ds(r + PAD + 1 - n + k, 8), :] for k in range(n)
            )

        acc = lax.fori_loop(0, rows // 8, tile, tuple(jnp.zeros((8, LANES), F32) for _ in range(n)))
        for k in range(n):
            small[k : k + 1, lanes(h)] = jnp.sum(acc[k], axis=0, keepdims=True)
        small[n : n + 1, lanes(h)] = jnp.sum(gain_sum[h], axis=0, keepdims=True)


def pack_body(kept, received, small, other, out):
    outs = kept.shape[1]
    total = small[...] + other[...]
    low, high = total[0:16].astype(BF16), total[16:32].astype(BF16)
    for p in range(out.shape[0]):
        at = slice(p * 16, (p + 1) * 16)
        out[p, :, 0:outs] = (kept[at] + received[at]).astype(BF16)
        out[p, :, outs : outs + 256] = low
        out[p, :, outs + 256 : outs + 512] = high


def relay_body(got, out, held):
    outs = got.shape[2] - 512
    total = got[0].astype(F32)
    for p in range(1, got.shape[0]):
        total = total + got[p].astype(F32)
    held[...] = total[:, 0:outs]
    for p in range(out.shape[0]):
        out[p, :, 0:512] = total[0:8, outs:]
        out[p, :, 512:1024] = total[8:16, outs:]
        for i in range(2):
            for j in range(4):
                out[p, 4 * i + j : 4 * i + j + 1, 1024:1280] = held[
                    2 * p + i : 2 * p + i + 1, 256 * j : 256 * j + 256
                ]


def final_body(factor, got, proj, taps, gain):
    total = got[0]
    for p in range(1, got.shape[0]):
        total = total + got[p]
    total = total * factor
    taps[0:8] = total[:, 0:256]
    taps[16:24] = total[:, 256:512]
    taps[8:16] = total[:, 512:768]
    taps[24:31] = total[0:7, 768:1024]
    gain[...] = total[7:8, 768:1024]
    for i in range(2):
        for j in range(4):
            proj[i : i + 1, 256 * j : 256 * j + 256] = total[4 * i + j : 4 * i + j + 1, 1024:1280]


def glu_grad_body(grad, after, taps, value, gate, value_grad, gate_grad, ext):
    rows = grad.shape[1]
    n = taps.shape[0]

    def fill(i, carry):
        r = pl.multiple_of(i * 64, 64)
        for h in range(2):
            ext[h, pl.ds(r, 64), :] = grad[h, pl.ds(r, 64), :]
        return carry

    lax.fori_loop(0, rows // 64, fill, 0)
    for h in range(2):
        ext[h, rows : rows + PAD, :] = after[h]
        weights = [jnp.broadcast_to(taps[k : k + 1, lanes(h)], (8, LANES)) for k in range(n)]

        def step(i, carry, h=h, weights=weights):
            tiles = []
            for u in range(2):
                r = i * 16 + u * 8
                parts = [None, None]
                for k in range(n):
                    term = weights[k] * ext[h, pl.ds(r + n - 1 - k, 8), :]
                    parts[k % 2] = term if parts[k % 2] is None else parts[k % 2] + term
                tiles.append(parts[0] + parts[1])
            at = pl.ds(pl.multiple_of(i * 16, 16), 16)
            dglu = jnp.concatenate(tiles, axis=0)
            sig = jax.nn.sigmoid(gate[at, lanes(h)].astype(F32))
            got = dglu * sig
            value_grad[at, lanes(h)] = got.astype(BF16)
            gate_grad[at, lanes(h)] = (got * value[at, lanes(h)].astype(F32) * (1.0 - sig)).astype(BF16)
            return carry

        lax.fori_loop(0, rows // 16, step, 0)


def act_body(out_grad, weight, act):
    act[...] = lax.dot_general(out_grad[...], weight[...], NT, preferred_element_type=F32)


def proj_body(me, activ, out_grad, kept, sent):
    width = activ.shape[1]
    half, i = width // 2, 2
    row = lax.broadcasted_iota(jnp.int32, (width, width), 0)
    col = lax.broadcasted_iota(jnp.int32, (width, width), 1)
    low = jnp.bitwise_and(col, half - 1)
    high = jnp.bitwise_xor(jnp.right_shift(col, 7), me[0])
    source = jnp.left_shift(jnp.right_shift(low, 1), 2) + 2 * high + jnp.bitwise_and(col, 1)
    order = (row == source).astype(F32).astype(BF16)
    placed = jnp.dot(activ[...], order, preferred_element_type=F32).astype(BF16)
    kept[...] = lax.dot_general(placed[:, :half], out_grad[...], TN, preferred_element_type=F32)
    sent[...] = lax.dot_general(placed[:, half:], out_grad[...], TN, preferred_element_type=F32)


def over_tp(array):
    return lax.all_to_all(array, "tp", 0, 0, tiled=True)


def per_device(glu_value, glu_gate, conv_taps, channel_gain, proj_weight, out_grad):
    n = conv_taps.shape[0]
    rows, width = glu_value.shape
    peers = lax.axis_size("tp")
    outs = out_grad.shape[1]
    factor = 1.0 / math.sqrt(rows * lax.axis_size(SP))
    def wide(length):
        return ((2, length, LANES), F32, "near")

    stat = ((peers, 2, rows), F32, "far")
    glu, edge = kernel(glu_body, [wide(rows + PAD), wide(PAD)], (glu_value, glu_gate), name="glu")
    edge = shifted(edge, 1)
    conv, stats = kernel(
        conv_body, [wide(rows), ((8, rows), F32, "near")], (near(glu), conv_taps), name="conv"
    )
    glu, conv, stats = kernel(
        head_body,
        [wide(rows + PAD), wide(rows), stat],
        (near(edge), near(glu), conv_taps, near(conv), near(stats)),
        aliases={1: 0, 3: 1},
        scratch=[((8, 256), F32)],
        name="head",
    )
    stats = over_tp(stats)
    (act_grad,) = kernel(
        act_body, [((rows, width), F32, "near")], (out_grad, proj_weight), name="act"
    )
    stats, act_grad = lax.optimization_barrier((stats, act_grad))
    activ, xhat, scaled, sums, rstd, gain_sum = kernel(
        norm_body,
        [
            ((rows, width), BF16, "near"),
            wide(rows),
            wide(rows),
            stat,
            ((1, rows), F32, "near"),
            wide(8),
        ],
        (near(stats), near(conv), near(act_grad), channel_gain[None]),
        scratch=[((2, rows), F32)],
        name="norm",
    )
    sums = over_tp(sums)
    kept, sent = kernel(
        proj_body,
        [((width // 2, outs), F32, "near")] * 2,
        (lax.axis_index("core")[None], activ, out_grad),
        name="proj",
        smem=1,
    )
    sums, sent = lax.optimization_barrier((sums, sent))
    received = swapped(sent)
    grad, small = kernel(
        taps_body,
        [wide(rows), ((n + 1, width), F32, "near")],
        (near(sums), near(rstd), near(xhat), near(scaled), near(glu), near(gain_sum)),
        scratch=[((2, rows), F32)],
        name="taps",
    )
    other = swapped(small)
    (first,) = kernel(
        pack_body,
        [((8, 16, outs + 512), BF16, "far")],
        (near(kept), near(received), near(small), near(other)),
        name="pack",
    )
    first = lax.all_to_all(first, "z", 0, 0, tiled=True)
    after = shifted(grad[:, :PAD], -1)
    first, after = lax.optimization_barrier((first, after))
    (second,) = kernel(
        relay_body,
        [((8, 8, 1280), F32, "far")],
        (near(first),),
        scratch=[((16, outs), F32)],
        name="relay",
    )
    second = lax.all_to_all(second, "y", 0, 0, tiled=True)
    value_grad, gate_grad = kernel(
        glu_grad_body,
        [((rows, width), BF16, "far")] * 2,
        (near(grad), near(after), conv_taps, glu_value, glu_gate),
        scratch=[((2, rows + PAD, LANES), F32)],
        name="glu_grad",
    )
    second, value_grad, gate_grad = lax.optimization_barrier((second, value_grad, gate_grad))
    proj_grad, taps_grad, gain_grad = kernel(
        lambda *refs: final_body(factor, *refs),
        [((2, outs), F32, "far"), ((n, width), F32, "far"), ((1, width), F32, "far")],
        (near(second),),
        name="final",
    )
    return (value_grad, gate_grad, proj_grad, taps_grad, gain_grad.reshape(width))


def solution(mesh):
    finer = Mesh(mesh.devices.reshape(8, 8, 2, mesh.shape["tp"]), (*SP, "tp"))
    return jax.shard_map(
        per_device,
        mesh=finer,
        in_specs=(P(SP, "tp"), P(SP, "tp"), P(None, "tp"), P("tp"), P("tp", None), P(SP, None)),
        out_specs=(P(SP, "tp"), P(SP, "tp"), P(("tp", *SP), None), P(None, "tp"), P("tp")),
        check_vma=False,
    )
```

time: 107 us -> 103 us (0.963)
  other arithmetic: 29.3 us -> 0 us
  Pallas kernels: 0 us -> 24.2 us
  local copies, waits for them, and re-layouts: 8.04 us -> 16.1 us
  matrix products: 5.93 us -> 0 us
    pallas_call x0 -> x11, Pallas kernels: none -> 24.2 us  [kernel(): pl.pallas_call(body, out_shape=[pltpu.VMEM(s, d) if where == 'near' else...]
    unnamed x100 -> x44, local copies, waits for them, and re-layouts: 0.24 us -> 16.1 us
    convert_element_type x3 -> x0, other arithmetic: 15.3 us -> none  [the longest x1 14.1 us: per_device(): gate_grad = (glu_grad * value_f * gate_sig * (1.0 - gate_sig)).astype(BF16)]
    reduce_sum x7 -> x0, other arithmetic: 11.5 us -> none  [the longest x2 6.03 us: per_device(): jnp.sum(conv_grad * glu_out[tap:tap + rows], axis=0)[None]]
    dot_general x2 -> x0, matrix products: 5.93 us -> none  [the longest x1 3.51 us: per_device(): lax.dot_general(out_grad, proj_weight, (((1,), (1,)), ((), ())), preferre...]
    slice x14 -> x1, local copies, waits for them, and re-layouts: 5.47 us -> 0.01 us  [per_device(): after = shifted(grad[:, :PAD], -1)]
    broadcast_in_dim x4 -> x0, local copies, waits for them, and re-layouts: 2.19 us -> none  [the longest x2 1.25 us: over_tp(): sent = jnp.broadcast_to(array[None], (peers, *array.shape))]
    mul x2 -> x0, other arithmetic: 1.6 us -> none  [the longest x1 1.59 us: per_device(): glu_out = value_ext.astype(F32) * jax.nn.sigmoid(gate_ext.astype(F32))]
  transfers between devices with their start and end apart: 8 -> 8, of which waited for: 5 -> 7; matrix products, arithmetic and copies ran while one was open for 20% -> 0% of each run, Pallas kernels for 0% -> 16%
where the time goes in v2:
time: 103 us; the launch traced here: 102 us
  starting transfers between devices  36.7 us (36%)
  Pallas kernels  24.2 us (23%)
  waiting for transfers between devices  24.2 us (23%)
  local copies, waits for them, and re-layouts  16.1 us (16%)
    pallas_call x11, Pallas kernels, kernel(): pl.pallas_call(body, out_shape=[pltpu.VMEM(s, d) if where == 'near' else...  24.2 us
    unnamed x44, local copies, waits for them, and re-layouts  16.1 us
    all_to_all x1, waiting for transfers between devices, per_device(): first = lax.all_to_all(first, 'z', 0, 0, tiled=True)  9.62 us
    all_to_all x1, starting transfers between devices, per_device(): first = lax.all_to_all(first, 'z', 0, 0, tiled=True)  9.08 us
    ppermute x2, starting transfers between devices, swapped(): return lax.ppermute(block, 'core', [(0, 1), (1, 0)])  8.89 us
    all_to_all x1, waiting for transfers between devices, per_device(): second = lax.all_to_all(second, 'y', 0, 0, tiled=True)  8.05 us
    all_to_all x2, starting transfers between devices, over_tp(): return lax.all_to_all(array, 'tp', 0, 0, tiled=True)  7.08 us
    ppermute x2, starting transfers between devices, shifted(): return lax.ppermute(block, SP, route)  6.93 us
  transfers between devices with their start and end apart: 8, of which 7 were waited for; matrix products, arithmetic and copies ran while one was open for 0% of the time, Pallas kernels for 16%

profile of v2, /device:TPU:1, one launch (start us, length us, event | category | flops | bytes accessed | tf_op | source)
XLA Modules:
  0.0 102.0 jit_solution(17181424066801993142)
XLA Ops:
  0.6 1.0 %copy-done.5 = bf16[1024,256]{1,0:T(8,128)(2,1)S(1)} copy-done((bf16[1024,256]{1,0:T(8,128)(2,1)S(1)}, bf16[1024,256]{1,0:T(8,128)(2,1)}, u32[]{:S(2)}) %copy-start.5) | copy-done | bytes 524312
  1.7 1.0 %copy-done.7 = bf16[1024,256]{1,0:T(8,128)(2,1)S(1)} copy-done((bf16[1024,256]{1,0:T(8,128)(2,1)S(1)}, bf16[1024,256]{1,0:T(8,128)(2,1)}, u32[]{:S(2)}) %copy-start.7) | copy-done | bytes 524312
  3.0 4.6 %collective-permute-start = (f32[2,32,128]{2,1,0:T(8,128)S(1)}, f32[2,32,128]{2,1,0:T(8,128)S(1)}, u32[]{:S(2)}, u32[]{:S(2)}) collective-permute-start(f32[2,32,128]{2,1,0:T(8,128)S(1)} %get-tuple-element.36), channel_id=1, source_target_pairs={{0,4},{4,8},{8,12},{12,16},{16,20},{20,24},{24,28},{28,32},{32,36}... | collective-permute-start | bytes 98312 | tf_op jit(solution)/shard_map/ppermute | solution.py:22
  8.4 3.2 %conv.1 = (f32[2,1024,128]{2,1,0:T(8,128)S(1)}, f32[8,1024]{1,0:T(8,128)S(1)}) custom-call(f32[2,1056,128]{2,1,0:T(8,128)S(1)} %get-tuple-element.37.glu.glu_in, f32[31,256]{1,0:T(8,128)S(1)} %copy-done.18), custom_call_target="tpu_custom_call" | custom-call | tf_op jit(solution)/shard_map/conv/pallas_call | solution.py:35
  11.8 1.7 %head.1 = (f32[2,1056,128]{2,1,0:T(8,128)S(1)}, f32[2,1024,128]{2,1,0:T(8,128)S(1)}, f32[4,2,1024]{2,1,0:T(2,128)}) custom-call(f32[2,32,128]{2,1,0:T(8,128)S(1)} %collective-permute-done.edge, f32[2,1056,128]{2,1,0:T(8,128)S(1)} %get-tuple-element.37.glu.glu_in, f32[31,256]{1,0:T(8,128)S(1)} %copy-done.18, ...), custom_call_target="tpu_custom_call", output_to_operand_aliasing={{0}: (1, {}), {1}: (3, {})} | custom-call | tf_op jit(solution)/shard_map/head/pallas_call | solution.py:35
  13.6 1.0 copy-done.3
  14.5 3.8 %all-to-all-start = ((f32[4,2,1024]{2,1,0:T(2,128)}), f32[4,2,1024]{2,1,0:T(2,128)S(1)}, u32[]{:S(2)}, u32[]{:S(2)}) async-start(f32[4,2,1024]{2,1,0:T(2,128)} %get-tuple-element.40), calls=%async_computation | async-start | bytes 65536 | tf_op jit(solution)/shard_map/all_to_all | solution.py:311
  18.4 1.0 %copy-done.13 = bf16[256,1024]{1,0:T(8,128)(2,1)S(1)} copy-done((bf16[256,1024]{1,0:T(8,128)(2,1)S(1)}, bf16[256,1024]{1,0:T(8,128)(2,1)}, u32[]{:S(2)}) %copy-start.13) | copy-done | bytes 524312
  20.2 1.0 copy-done.1
  21.1 1.5 %all-to-all-done.stats = f32[4,2,1024]{2,1,0:T(2,128)S(1)} async-done(((f32[4,2,1024]{2,1,0:T(2,128)}), f32[4,2,1024]{2,1,0:T(2,128)S(1)}, u32[]{:S(2)}, u32[]{:S(2)}) %all-to-all-start) | async-done | bytes 32800 | tf_op jit(solution)/shard_map/all_to_all | solution.py:311
  22.7 1.2 %copy-done.2 = f32[1024,256]{1,0:T(8,128)S(1)} copy-done((f32[1024,256]{1,0:T(8,128)S(1)}, f32[1024,256]{1,0:T(8,128)}, u32[]{:S(2)}) %copy-start.2) | copy-done | bytes 1048600
  23.9 1.2 %copy-done.4 = f32[2,1024,128]{2,1,0:T(8,128)S(1)} copy-done((f32[2,1024,128]{2,1,0:T(8,128)S(1)}, f32[2,1024,128]{2,1,0:T(8,128)}, u32[]{:S(2)}) %copy-start.4) | copy-done | bytes 1048600
  25.1 3.7 %norm.1 = (bf16[1024,256]{1,0:T(8,128)(2,1)S(1)}, f32[2,1024,128]{2,1,0:T(8,128)S(1)}, f32[2,1024,128]{2,1,0:T(8,128)S(1)}, f32[4,2,1024]{2,1,0:T(2,128)}, f32[1...) custom-call(f32[4,2,1024]{2,1,0:T(2,128)S(1)} %all-to-all-done.stats, f32[2,1024,128]{2,1,0:T(8,128)S(1)} %copy-done.4, ...), custom_call_target="tpu_custom_call" | custom-call | tf_op jit(solution)/shard_map/norm/pallas_call | solution.py:35
  28.8 1.0 copy-done.9
  29.8 1.0 copy-done.11
  31.6 3.3 %all-to-all-start.1 = ((f32[4,2,1024]{2,1,0:T(2,128)}), f32[4,2,1024]{2,1,0:T(2,128)S(1)}, u32[]{:S(2)}, u32[]{:S(2)}) async-start(f32[4,2,1024]{2,1,0:T(2,128)} %get-tuple-element.46), calls=%async_computation.1 | async-start | bytes 65536 | tf_op jit(solution)/shard_map/all_to_all | solution.py:311
  34.9 1.0 %copy-done.17 = bf16[1024,256]{1,0:T(8,128)(2,1)S(1)} copy-done((bf16[1024,256]{1,0:T(8,128)(2,1)S(1)}, bf16[1024,256]{1,0:T(8,128)(2,1)}, u32[]{:S(2)}) %copy-start.17) | copy-done | bytes 524312
  35.9 1.2 %proj.1 = (f32[128,1024]{1,0:T(8,128)S(1)}, f32[128,1024]{1,0:T(8,128)S(1)}) custom-call(s32[1]{0:T(128)} %bitcast.me, bf16[1024,256]{1,0:T(8,128)(2,1)S(1)} %copy-done.17, bf16[1024,1024]{1,0:T(8,128)(2,1)S(1)} %copy-done), custom_call_target="tpu_custom_call" | custom-call | tf_op jit(solution)/shard_map/proj/pallas_call | solution.py:35
  39.1 7.0 %collective-permute-start.1 = (f32[128,1024]{1,0:T(8,128)}, f32[128,1024]{1,0:T(8,128)S(1)}, u32[]{:S(2)}, u32[]{:S(2)}) collective-permute-start(f32[128,1024]{1,0:T(8,128)} %copy-done.21), channel_id=1, source_target_pairs={{0,4},{4,0},{1,5},{5,1},{2,6},{6,2},{3,7},{7,3},{8,12},{12,8},{9,1... | collective-permute-start | bytes 1572872 | tf_op jit(solution)/shard_map/ppermute | solution.py:26
  46.1 1.2 %copy-done.10 = f32[2,1024,128]{2,1,0:T(8,128)S(1)} copy-done((f32[2,1024,128]{2,1,0:T(8,128)S(1)}, f32[2,1024,128]{2,1,0:T(8,128)}, u32[]{:S(2)}) %copy-start.10) | copy-done | bytes 1048600
  47.3 1.2 %copy-done.12 = f32[2,1024,128]{2,1,0:T(8,128)S(1)} copy-done((f32[2,1024,128]{2,1,0:T(8,128)S(1)}, f32[2,1024,128]{2,1,0:T(8,128)}, u32[]{:S(2)}) %copy-start.12) | copy-done | bytes 1048600
  48.5 6.1 %taps.6 = (f32[2,1024,128]{2,1,0:T(8,128)S(1)}, f32[32,256]{1,0:T(8,128)S(1)}) custom-call(f32[4,2,1024]{2,1,0:T(2,128)S(1)} %all-to-all-done.1.sums, f32[1,1024]{1,0:T(1,128)S(1)} %get-tuple-element.50.rstd, f32[2,1024,128]{2,1,0:T(8,128)S(1)} %copy-done.10, f32[2,1024,128]{2,1,0:T(8,128)S(1)} %copy-done.12, f32[2,1056,128]{2,1,0:T(8,128)S(1)} %get-tuple-element.53.glu, ...), custom_call_target="tpu_custom_call" | custom-call | tf_op jit(solution)/shard_map/taps/pallas_call | solution.py:35
  54.7 1.9 %collective-permute-start.2 = (f32[32,256]{1,0:T(8,128)S(1)}, f32[32,256]{1,0:T(8,128)S(1)}, u32[]{:S(2)}, u32[]{:S(2)}) collective-permute-start(f32[32,256]{1,0:T(8,128)S(1)} %get-tuple-element.55.small), channel_id=1, source_target_pairs={{0,4},{4,0},{1,5},{5,1},{2,6},{6,2},{3,7},{7,3},{8,12},{12,8},{9,1... | collective-permute-start | bytes 98312 | tf_op jit(solution)/shard_map/ppermute | solution.py:26
  56.6 1.2 %collective-permute-done.2.other = f32[32,256]{1,0:T(8,128)S(1)} collective-permute-done((f32[32,256]{1,0:T(8,128)S(1)}, f32[32,256]{1,0:T(8,128)S(1)}, u32[]{:S(2)}, u32[]{:S(2)}) %collective-permute-start.2) | collective-permute-done | bytes 32800 | tf_op jit(solution)/shard_map/ppermute | solution.py:26
  58.6 9.1 %all-to-all-start.2 = ((bf16[8,16,1536]{2,1,0:T(8,128)(2,1)}), bf16[8,16,1536]{2,1,0:T(8,128)(2,1)S(1)}, u32[]{:S(2)}, u32[]{:S(2)}) async-start(bf16[8,16,1536]{2,1,0:T(8,128)(2,1)} %pack.1), calls=%async_computation.2 | async-start | bytes 786432 | tf_op jit(solution)/shard_map/all_to_all | solution.py:380
  67.7 2.4 %collective-permute-start.3 = (f32[2,32,128]{2,1,0:T(8,128)S(1)}, f32[2,32,128]{2,1,0:T(8,128)S(1)}, u32[]{:S(2)}, u32[]{:S(2)}) collective-permute-start(f32[2,32,128]{2,1,0:T(8,128)S(1)} %slice.3), channel_id=1, source_target_pairs={{4,0},{8,4},{12,8},{16,12},{20,16},{24,20},{28,24},{32,28},{36,32}... | collective-permute-start | bytes 98312 | tf_op jit(solution)/shard_map/ppermute | solution.py:22
  70.0 3.2 %collective-permute-done.3.after = f32[2,32,128]{2,1,0:T(8,128)S(1)} collective-permute-done((f32[2,32,128]{2,1,0:T(8,128)S(1)}, f32[2,32,128]{2,1,0:T(8,128)S(1)}, u32[]{:S(2)}, u32[]{:S(2)}) %collective-permute-start.3) | collective-permute-done | bytes 32800 | tf_op jit(solution)/shard_map/ppermute | solution.py:22
  73.2 9.6 %all-to-all-done.2.got = bf16[8,16,1536]{2,1,0:T(8,128)(2,1)S(1)} async-done(((bf16[8,16,1536]{2,1,0:T(8,128)(2,1)}), bf16[8,16,1536]{2,1,0:T(8,128)(2,1)S(1)}, u32[]{:S(2)}, u32[]{:S(2)}) %all-to-all-start.2) | async-done | bytes 393248 | tf_op jit(solution)/shard_map/all_to_all | solution.py:380
  82.8 0.8 relay.1
  83.6 4.7 %all-to-all-start.3 = ((f32[8,8,1280]{2,1,0:T(8,128)}), f32[8,8,1280]{2,1,0:T(8,128)S(1)}, u32[]{:S(2)}, u32[]{:S(2)}) async-start(f32[8,8,1280]{2,1,0:T(8,128)} %relay.1), calls=%async_computation.3 | async-start | bytes 655360 | tf_op jit(solution)/shard_map/all_to_all | solution.py:390
  88.4 4.9 %glu_grad.1 = (bf16[1024,256]{1,0:T(8,128)(2,1)}, bf16[1024,256]{1,0:T(8,128)(2,1)}) custom-call(f32[2,1024,128]{2,1,0:T(8,128)S(1)} %get-tuple-element.56.grad, f32[2,32,128]{2,1,0:T(8,128)S(1)} %collective-permute-done.3.after, f32[31,256]{1,0:T(8,128)S(1)} %copy-done.19, bf16[1024,256]{1,0:T(8,128)(2,1)S(1)} %copy-done.6, bf16[1024,256]{1,0:T(8,128)(2,1)S(1)} %copy-done.8), custom_call_target="tpu_custom_call" | custom-call | tf_op jit(solution)/shard_map/glu_grad/pallas_call | solution.py:35
  93.3 8.1 %all-to-all-done.3.refs_0_ = f32[8,8,1280]{2,1,0:T(8,128)S(1)} async-done(((f32[8,8,1280]{2,1,0:T(8,128)}), f32[8,8,1280]{2,1,0:T(8,128)S(1)}, u32[]{:S(2)}, u32[]{:S(2)}) %all-to-all-start.3) | async-done | bytes 327712 | tf_op jit(solution)/shard_map/all_to_all | solution.py:390
  (40 shorter events, 6.3 us)
Async XLA Ops:
  0.6 1.0 %copy-start.5 = (bf16[1024,256]{1,0:T(8,128)(2,1)S(1)}, bf16[1024,256]{1,0:T(8,128)(2,1)}, u32[]{:S(2)}) copy-start(bf16[1024,256]{1,0:T(8,128)(2,1)} %value.3) | copy-start | bytes 1572868
  1.7 1.0 %copy-start.7 = (bf16[1024,256]{1,0:T(8,128)(2,1)S(1)}, bf16[1024,256]{1,0:T(8,128)(2,1)}, u32[]{:S(2)}) copy-start(bf16[1024,256]{1,0:T(8,128)(2,1)} %gate.3) | copy-start | bytes 1572868
  3.0 8.8 %collective-permute-start = (f32[2,32,128]{2,1,0:T(8,128)S(1)}, f32[2,32,128]{2,1,0:T(8,128)S(1)}, u32[]{:S(2)}, u32[]{:S(2)}) collective-permute-start(f32[2,32,128]{2,1,0:T(8,128)S(1)} %get-tuple-element.36), channel_id=1, source_target_pairs={{0,4},{4,8},{8,12},{12,16},{16,20},{20,24},{24,28},{28,32},{32,36}... | collective-permute-start | bytes 98312 | tf_op jit(solution)/shard_map/ppermute | solution.py:22
  7.6 0.8 copy-start.18
  11.8 6.5 %copy-start = (bf16[1024,1024]{1,0:T(8,128)(2,1)S(1)}, bf16[1024,1024]{1,0:T(8,128)(2,1)}, u32[]{:S(2)}) copy-start(bf16[1024,1024]{1,0:T(8,128)(2,1)} %out_grad.3) | copy-start | bytes 6291460
  13.6 1.0 copy-start.3
  14.5 8.1 %all-to-all-start = ((f32[4,2,1024]{2,1,0:T(2,128)}), f32[4,2,1024]{2,1,0:T(2,128)S(1)}, u32[]{:S(2)}, u32[]{:S(2)}) async-start(f32[4,2,1024]{2,1,0:T(2,128)} %get-tuple-element.40), calls=%async_computation | async-start | bytes 65536 | tf_op jit(solution)/shard_map/all_to_all | solution.py:311
  18.4 1.0 %copy-start.13 = (bf16[256,1024]{1,0:T(8,128)(2,1)S(1)}, bf16[256,1024]{1,0:T(8,128)(2,1)}, u32[]{:S(2)}) copy-start(bf16[256,1024]{1,0:T(8,128)(2,1)} %weight.1) | copy-start | bytes 1572868
  19.4 3.3 %copy-start.20 = (f32[256]{0:T(256)S(1)}, f32[256]{0:T(256)}, u32[]{:S(2)}) copy-start(f32[256]{0:T(256)} %param.9) | copy-start | bytes 3076
  20.2 1.0 copy-start.1
  22.7 1.2 %copy-start.2 = (f32[1024,256]{1,0:T(8,128)S(1)}, f32[1024,256]{1,0:T(8,128)}, u32[]{:S(2)}) copy-start(f32[1024,256]{1,0:T(8,128)} %copy-done.1) | copy-start | bytes 3145732
  23.9 1.2 %copy-start.4 = (f32[2,1024,128]{2,1,0:T(8,128)S(1)}, f32[2,1024,128]{2,1,0:T(8,128)}, u32[]{:S(2)}) copy-start(f32[2,1024,128]{2,1,0:T(8,128)} %copy-done.3) | copy-start | bytes 3145732
  28.8 1.0 copy-start.9
  29.8 1.0 copy-start.11
  30.8 0.8 copy-start.16
  31.6 7.5 %all-to-all-start.1 = ((f32[4,2,1024]{2,1,0:T(2,128)}), f32[4,2,1024]{2,1,0:T(2,128)S(1)}, u32[]{:S(2)}, u32[]{:S(2)}) async-start(f32[4,2,1024]{2,1,0:T(2,128)} %get-tuple-element.46), calls=%async_computation.1 | async-start | bytes 65536 | tf_op jit(solution)/shard_map/all_to_all | solution.py:311
  34.8 1.0 %copy-start.17 = (bf16[1024,256]{1,0:T(8,128)(2,1)S(1)}, bf16[1024,256]{1,0:T(8,128)(2,1)}, u32[]{:S(2)}) copy-start(bf16[1024,256]{1,0:T(8,128)(2,1)} %copy-done.16) | copy-start | bytes 1572868
  37.1 0.8 copy-start.14
  37.9 0.8 copy-start.21
  39.1 18.7 %collective-permute-start.1 = (f32[128,1024]{1,0:T(8,128)}, f32[128,1024]{1,0:T(8,128)S(1)}, u32[]{:S(2)}, u32[]{:S(2)}) collective-permute-start(f32[128,1024]{1,0:T(8,128)} %copy-done.21), channel_id=1, source_target_pairs={{0,4},{4,0},{1,5},{5,1},{2,6},{6,2},{3,7},{7,3},{8,12},{12,8},{9,1... | collective-permute-start | bytes 1572872 | tf_op jit(solution)/shard_map/ppermute | solution.py:26
  46.1 1.2 %copy-start.10 = (f32[2,1024,128]{2,1,0:T(8,128)S(1)}, f32[2,1024,128]{2,1,0:T(8,128)}, u32[]{:S(2)}) copy-start(f32[2,1024,128]{2,1,0:T(8,128)} %copy-done.9) | copy-start | bytes 3145732
  47.3 1.2 %copy-start.12 = (f32[2,1024,128]{2,1,0:T(8,128)S(1)}, f32[2,1024,128]{2,1,0:T(8,128)}, u32[]{:S(2)}) copy-start(f32[2,1024,128]{2,1,0:T(8,128)} %copy-done.11) | copy-start | bytes 3145732
  48.5 9.2 %copy-start.15 = (f32[128,1024]{1,0:T(8,128)S(1)}, f32[128,1024]{1,0:T(8,128)}, u32[]{:S(2)}) copy-start(f32[128,1024]{1,0:T(8,128)} %copy-done.14) | copy-start | bytes 1572868
  54.7 3.1 %collective-permute-start.2 = (f32[32,256]{1,0:T(8,128)S(1)}, f32[32,256]{1,0:T(8,128)S(1)}, u32[]{:S(2)}, u32[]{:S(2)}) collective-permute-start(f32[32,256]{1,0:T(8,128)S(1)} %get-tuple-element.55.small), channel_id=1, source_target_pairs={{0,4},{4,0},{1,5},{5,1},{2,6},{6,2},{3,7},{7,3},{8,12},{12,8},{9,1... | collective-permute-start | bytes 98312 | tf_op jit(solution)/shard_map/ppermute | solution.py:26
  58.6 29.8 %copy-start.6 = (bf16[1024,256]{1,0:T(8,128)(2,1)S(1)}, bf16[1024,256]{1,0:T(8,128)(2,1)}, u32[]{:S(2)}) copy-start(bf16[1024,256]{1,0:T(8,128)(2,1)} %value.3) | copy-start | bytes 1572868
  58.6 29.8 %copy-start.8 = (bf16[1024,256]{1,0:T(8,128)(2,1)S(1)}, bf16[1024,256]{1,0:T(8,128)(2,1)}, u32[]{:S(2)}) copy-start(bf16[1024,256]{1,0:T(8,128)(2,1)} %gate.3) | copy-start | bytes 1572868
  58.6 29.8 %copy-start.19 = (f32[31,256]{1,0:T(8,128)S(1)}, f32[31,256]{1,0:T(8,128)}, u32[]{:S(2)}) copy-start(f32[31,256]{1,0:T(8,128)} %taps.7) | copy-start | bytes 95236
  58.6 24.2 %all-to-all-start.2 = ((bf16[8,16,1536]{2,1,0:T(8,128)(2,1)}), bf16[8,16,1536]{2,1,0:T(8,128)(2,1)S(1)}, u32[]{:S(2)}, u32[]{:S(2)}) async-start(bf16[8,16,1536]{2,1,0:T(8,128)(2,1)} %pack.1), calls=%async_computation.2 | async-start | bytes 786432 | tf_op jit(solution)/shard_map/all_to_all | solution.py:380
  67.7 5.5 %collective-permute-start.3 = (f32[2,32,128]{2,1,0:T(8,128)S(1)}, f32[2,32,128]{2,1,0:T(8,128)S(1)}, u32[]{:S(2)}, u32[]{:S(2)}) collective-permute-start(f32[2,32,128]{2,1,0:T(8,128)S(1)} %slice.3), channel_id=1, source_target_pairs={{4,0},{8,4},{12,8},{16,12},{20,16},{24,20},{28,24},{32,28},{36,32}... | collective-permute-start | bytes 98312 | tf_op jit(solution)/shard_map/ppermute | solution.py:22
  83.6 17.7 %all-to-all-start.3 = ((f32[8,8,1280]{2,1,0:T(8,128)}), f32[8,8,1280]{2,1,0:T(8,128)S(1)}, u32[]{:S(2)}, u32[]{:S(2)}) async-start(f32[8,8,1280]{2,1,0:T(8,128)} %relay.1), calls=%async_computation.3 | async-start | bytes 655360 | tf_op jit(solution)/shard_map/all_to_all | solution.py:390

commit v3 on v2

v3 whole, which is shorter than its diff:
```python
import math

import jax
import jax.numpy as jnp
from jax import lax
from jax.experimental import pallas as pl
from jax.experimental.pallas import tpu as pltpu
from jax.sharding import Mesh
from jax.sharding import PartitionSpec as P


SP = ("z", "y", "core")
F32, BF16 = jnp.float32, jnp.bfloat16
LANES = 128
PAD = 32
NT = (((1,), (1,)), ((), ()))
TN = (((0,), (0,)), ((), ()))


def shifted(block, distance):
    devices = range(lax.axis_size(SP))
    route = [(i - distance, i) for i in devices if i - distance in devices]
    return lax.ppermute(block, SP, route)


def swapped(block):
    return lax.ppermute(block, "core", [(0, 1), (1, 0)])


def near(array):
    return pltpu.with_memory_space_constraint(array, pltpu.VMEM)


def far(array):
    return pltpu.with_memory_space_constraint(array, pltpu.HBM)


VMEM, HBM, SMEM = (pl.BlockSpec(memory_space=m) for m in (pltpu.VMEM, pltpu.HBM, pltpu.SMEM))


def kernel(body, outs, args, ins=(), out_specs=None, scratch=(), aliases=None, limit=16):
    shapes = {
        "near": pltpu.VMEM,
        "far": pltpu.HBM,
        "any": jax.ShapeDtypeStruct,
    }
    return pl.pallas_call(
        body,
        out_shape=[shapes[where](s, d) for s, d, where in outs],
        in_specs=list(ins) + [VMEM] * (len(args) - len(ins)),
        out_specs=out_specs or [VMEM] * len(outs),
        scratch_shapes=[pltpu.VMEM(*x) if isinstance(x, tuple) else x for x in scratch],
        input_output_aliases=aliases or {},
        compiler_params=pltpu.CompilerParams(vmem_limit_bytes=limit << 20),
    )(*args)


def lanes(h):
    return slice(h * LANES, (h + 1) * LANES)


def glu_body(value_in, gate_in, taps_in, glu, edge, taps, value, gate, sems):
    rows = value.shape[0]
    chunks = sems.shape[1] - 1
    size = rows // chunks
    load_taps = pltpu.make_async_copy(taps_in, taps, sems.at[0, chunks])
    loads = []
    for c in range(chunks):
        at = pl.ds(c * size, size)
        loads.append(pltpu.make_async_copy(value_in.at[at], value.at[at], sems.at[0, c]))
        loads.append(pltpu.make_async_copy(gate_in.at[at], gate.at[at], sems.at[1, c]))
    for load in loads:
        load.start()
    load_taps.start()
    for c in range(chunks):
        loads[2 * c].wait()
        loads[2 * c + 1].wait()

        def step(i, carry, c=c):
            r = pl.multiple_of(c * size + i * 64, 64)
            for h in range(2):
                v = value[pl.ds(r, 64), lanes(h)].astype(F32)
                g = gate[pl.ds(r, 64), lanes(h)].astype(F32)
                glu[h, pl.ds(PAD + r, 64), :] = v * jax.nn.sigmoid(g)
            return carry

        lax.fori_loop(0, size // 64, step, 0)
    for h in range(2):
        edge[h] = glu[h, rows : rows + PAD, :]
    load_taps.wait()


def conv_rows(glu, taps, conv, start, count):
    n = taps.shape[0]
    for h in range(2):
        weights = [jnp.broadcast_to(taps[k : k + 1, lanes(h)], (8, LANES)) for k in range(n)]

        def step(i, carry, h=h, weights=weights):
            for u in range(4):
                r = start + i * 32 + u * 8
                parts = [None, None]
                for k in range(n):
                    term = weights[k] * glu[h, pl.ds(r + PAD + 1 - n + k, 8), :]
                    parts[k % 2] = term if parts[k % 2] is None else parts[k % 2] + term
                conv[h, pl.ds(pl.multiple_of(r, 8), 8), :] = parts[0] + parts[1]
            return carry

        lax.fori_loop(0, count // 32, step, 0)


def split(x):
    high = x.astype(BF16)
    return high, (x - high.astype(F32)).astype(BF16)


def selector(row):
    sub = lax.broadcasted_iota(jnp.int32, (8, LANES), 0)
    return (sub == row).astype(F32).astype(BF16)


def row_sums(pairs):
    total = None
    for row, x in pairs:
        pick = selector(row)
        for part in split(x):
            term = lax.dot_general(pick, part, NT, preferred_element_type=F32)
            total = term if total is None else total + term
    return total


def conv_stats(conv, stats, start, count):
    def step(i, carry):
        r = pl.multiple_of(start + i * 256, 256)
        pairs = []
        for h in range(2):
            c = conv[h, pl.ds(r, 256), :]
            pairs += [(0, c), (1, c * c)]
        stats[:, pl.ds(r, 256)] = row_sums(pairs)
        return carry

    lax.fori_loop(0, count // 256, step, 0)


def conv_body(glu, taps, conv, stats, saved, sem):
    rows = conv.shape[1]
    store = pltpu.make_async_copy(
        glu.at[:, pl.ds(PAD, rows)], saved.at[:, pl.ds(PAD, rows)], sem
    )
    store.start()
    conv_rows(glu, taps, conv, 256, rows - 256)
    conv_stats(conv, stats, 256, rows - 256)
    store.wait()


def head_body(saved_in, edge, glu_in, taps, conv_in, stats_in, saved, glu, conv, sent, stats, sem):
    store = pltpu.make_async_copy(edge, saved.at[:, pl.ds(0, PAD)], sem)
    store.start()
    for h in range(2):
        glu[h, 0:PAD, :] = edge[h]
    conv_rows(glu, taps, conv, 0, 256)
    conv_stats(conv, stats, 0, 256)
    rows = conv.shape[1]
    for p in range(sent.shape[0]):
        sent[p, :, 0:256] = stats[0:2]
        sent[p, :, 256:rows] = stats_in[0:2, 256:rows]
    store.wait()


def column(row):
    return jnp.broadcast_to(row, (LANES, LANES)).T


def norm_body(
    stats, conv, act_grad, gain, activ_out, xhat_out, scaled, sums, rstd_out, gain_sum,
    rows_in, activ, xhats, sems,
):
    peers = stats.shape[0]
    channels = 2 * LANES * peers
    total = stats[0]
    for p in range(1, peers):
        total = total + stats[p]
    mean = total[0:1] * (1.0 / channels)
    rstd = lax.rsqrt(total[1:2] * (1.0 / channels) - mean * mean + 1e-05)
    rstd_out[...] = rstd
    rows_in[0:1, :] = rstd
    rows_in[1:2, :] = mean
    for h in range(2):
        gain_sum[h] = jnp.zeros((8, LANES), F32)

    def store(i):
        at = pl.ds(pl.multiple_of(i * LANES, LANES), LANES)
        return (
            pltpu.make_async_copy(activ.at[at], activ_out.at[at], sems.at[0, i]),
            pltpu.make_async_copy(xhats.at[:, at], xhat_out.at[:, at], sems.at[1, i]),
        )

    def step(i, carry):
        r = pl.multiple_of(i * LANES, LANES)
        rs = column(rows_in[0:1, pl.ds(r, LANES)])
        mu = column(rows_in[1:2, pl.ds(r, LANES)])
        pairs = []
        for h in range(2):
            g = gain[0:1, lanes(h)]
            xhat = (conv[h, pl.ds(r, LANES), :] - mu) * rs
            normed = xhat * g
            sig = jax.nn.sigmoid(normed)
            activ[pl.ds(r, LANES), lanes(h)] = (normed * sig).astype(BF16)
            ng = act_grad[pl.ds(r, LANES), lanes(h)] * (sig * (1.0 + normed * (1.0 - sig)))
            gain_sum[h] += jnp.sum((ng * xhat).reshape(16, 8, LANES), axis=0)
            xg = ng * g
            xhats[h, pl.ds(r, LANES), :] = xhat
            scaled[h, pl.ds(r, LANES), :] = xg * rs
            pairs += [(0, xg), (1, xg * xhat)]
        out = row_sums(pairs)
        for p in range(peers):
            sums[p, :, pl.ds(r, LANES)] = out[0:2]
        for copy in store(i):
            copy.start()
        return carry

    blocks = conv.shape[1] // LANES
    lax.fori_loop(0, blocks, step, 0)
    for i in range(blocks):
        for copy in store(i):
            copy.wait()


def taps_body(
    kept_in, xhat_in, glu_in, received, sums, rstd, scaled, gain_sum, grad, small, packed,
    rows_in, columns, kept, xhat, glu, joined, sems,
):
    rows = grad.shape[1]
    load_xhat = pltpu.make_async_copy(xhat_in, xhat, sems.at[0])
    load_kept = pltpu.make_async_copy(kept_in, kept, sems.at[1])
    load_glu = pltpu.make_async_copy(glu_in, glu, sems.at[2])
    load_xhat.start()
    load_kept.start()
    load_glu.start()
    peers = sums.shape[0]
    channels = 2 * LANES * peers
    n = small.shape[0] - 1
    total = sums[0]
    for p in range(1, peers):
        total = total + sums[p]
    rows_in[...] = total * (rstd[...] * (1.0 / channels))
    for b in range(rows // LANES):
        at = slice(b * LANES, (b + 1) * LANES)
        columns[0, at] = column(rows_in[0:1, at])
        columns[1, at] = column(rows_in[1:2, at])
    load_xhat.wait()

    def step(i, carry):
        at = pl.ds(pl.multiple_of(i * 64, 64), 64)
        for h in range(2):
            grad[h, at, :] = scaled[h, at, :] - columns[0, at] - xhat[h, at, :] * columns[1, at]
        return carry

    lax.fori_loop(0, rows // 64, step, 0)
    load_kept.wait()
    for p in range(joined.shape[0]):
        at = slice(p * 16, (p + 1) * 16)
        joined[p] = (kept[at] + received[at]).astype(BF16)
    store = pltpu.make_async_copy(joined, packed.at[:, :, pl.ds(0, joined.shape[2])], sems.at[3])
    store.start()
    load_glu.wait()
    for h in range(2):
        for lo, hi in ((0, 16), (16, n)):

            def tile(i, acc, h=h, lo=lo, hi=hi):
                acc = list(acc)
                for u in range(4):
                    r = pl.multiple_of(i * 32 + u * 8, 8)
                    c = grad[h, pl.ds(r, 8), :]
                    for k in range(lo, hi):
                        acc[k - lo] = acc[k - lo] + c * glu[h, pl.ds(r + PAD + 1 - n + k, 8), :]
                return tuple(acc)

            zero = tuple(jnp.zeros((8, LANES), F32) for _ in range(lo, hi))
            acc = lax.fori_loop(0, rows // 32, tile, zero)
            for k in range(lo, hi):
                small[k : k + 1, lanes(h)] = jnp.sum(acc[k - lo], axis=0, keepdims=True)
        small[n : n + 1, lanes(h)] = jnp.sum(gain_sum[h], axis=0, keepdims=True)
    store.wait()


def pack_body(packed_in, small, other, packed, piece, sem):
    total = small[...] + other[...]
    low, high = total[0:16].astype(BF16), total[16:32].astype(BF16)
    for p in range(piece.shape[0]):
        piece[p, :, 0:256] = low
        piece[p, :, 256:512] = high
    outs = packed.shape[2] - 512
    store = pltpu.make_async_copy(piece, packed.at[:, :, pl.ds(outs, 512)], sem)
    store.start()
    store.wait()


def relay_body(got, out, held):
    outs = got.shape[2] - 512
    total = got[0].astype(F32)
    for p in range(1, got.shape[0]):
        total = total + got[p].astype(F32)
    held[...] = total[:, 0:outs]
    for p in range(out.shape[0]):
        out[p, :, 0:512] = total[0:8, outs:]
        out[p, :, 512:1024] = total[8:16, outs:]
        for i in range(2):
            for j in range(4):
                out[p, 4 * i + j : 4 * i + j + 1, 1024:1280] = held[
                    2 * p + i : 2 * p + i + 1, 256 * j : 256 * j + 256
                ]


def final_body(factor, got, proj, taps, gain):
    total = got[0]
    for p in range(1, got.shape[0]):
        total = total + got[p]
    total = total * factor
    taps[0:8] = total[:, 0:256]
    taps[16:24] = total[:, 256:512]
    taps[8:16] = total[:, 512:768]
    taps[24:31] = total[0:7, 768:1024]
    gain[...] = total[7:8, 768:1024]
    for i in range(2):
        for j in range(4):
            proj[i : i + 1, 256 * j : 256 * j + 256] = total[4 * i + j : 4 * i + j + 1, 1024:1280]


def glu_grad_body(grad, after, taps, value, gate, value_grad, gate_grad, ext):
    rows = grad.shape[1]
    n = taps.shape[0]

    def fill(i, carry):
        r = pl.multiple_of(i * 64, 64)
        for h in range(2):
            ext[h, pl.ds(r, 64), :] = grad[h, pl.ds(r, 64), :]
        return carry

    lax.fori_loop(0, rows // 64, fill, 0)
    for h in range(2):
        ext[h, rows : rows + PAD, :] = after[h]
        weights = [jnp.broadcast_to(taps[k : k + 1, lanes(h)], (8, LANES)) for k in range(n)]

        def step(i, carry, h=h, weights=weights):
            tiles = []
            for u in range(2):
                r = i * 16 + u * 8
                parts = [None, None]
                for k in range(n):
                    term = weights[k] * ext[h, pl.ds(r + n - 1 - k, 8), :]
                    parts[k % 2] = term if parts[k % 2] is None else parts[k % 2] + term
                tiles.append(parts[0] + parts[1])
            at = pl.ds(pl.multiple_of(i * 16, 16), 16)
            dglu = jnp.concatenate(tiles, axis=0)
            sig = jax.nn.sigmoid(gate[at, lanes(h)].astype(F32))
            got = dglu * sig
            value_grad[at, lanes(h)] = got.astype(BF16)
            gate_grad[at, lanes(h)] = (got * value[at, lanes(h)].astype(F32) * (1.0 - sig)).astype(BF16)
            return carry

        lax.fori_loop(0, rows // 16, step, 0)


def act_body(grad_in, weight_in, act, out_grad, weight, sems):
    rows = out_grad.shape[0]
    size = rows // 4
    load_weight = pltpu.make_async_copy(weight_in, weight, sems.at[4])
    load_weight.start()
    loads = []
    for c in range(4):
        at = pl.ds(c * size, size)
        loads.append(pltpu.make_async_copy(grad_in.at[at], out_grad.at[at], sems.at[c]))
        loads[c].start()
    load_weight.wait()
    for c in range(4):
        loads[c].wait()
        at = pl.ds(c * size, size)
        act[at] = lax.dot_general(out_grad[at], weight[...], NT, preferred_element_type=F32)


def proj_body(me, activ_in, grad_in, kept, sent, activ, out_grad, sems):
    load_activ = pltpu.make_async_copy(activ_in, activ, sems.at[0])
    load_grad = pltpu.make_async_copy(grad_in, out_grad, sems.at[1])
    load_activ.start()
    load_grad.start()
    width = activ.shape[1]
    half = width // 2
    row = lax.broadcasted_iota(jnp.int32, (width, width), 0)
    col = lax.broadcasted_iota(jnp.int32, (width, width), 1)
    low = jnp.bitwise_and(col, half - 1)
    high = jnp.bitwise_xor(jnp.right_shift(col, 7), me[0])
    source = jnp.left_shift(jnp.right_shift(low, 1), 2) + 2 * high + jnp.bitwise_and(col, 1)
    order = (row == source).astype(F32).astype(BF16)
    load_activ.wait()
    placed = jnp.dot(activ[...], order, preferred_element_type=F32).astype(BF16)
    load_grad.wait()
    sent[...] = lax.dot_general(placed[:, half:], out_grad[...], TN, preferred_element_type=F32)
    kept[...] = lax.dot_general(placed[:, :half], out_grad[...], TN, preferred_element_type=F32)


def over_tp(array):
    return lax.all_to_all(array, "tp", 0, 0, tiled=True)


def per_device(glu_value, glu_gate, conv_taps, channel_gain, proj_weight, out_grad):
    n = conv_taps.shape[0]
    rows, width = glu_value.shape
    peers = lax.axis_size("tp")
    outs = out_grad.shape[1]
    factor = 1.0 / math.sqrt(rows * lax.axis_size(SP))

    def wide(length):
        return ((2, length, LANES), F32, "near")

    def kept_wide(length):
        return ((2, length, LANES), F32, "far")

    stat = ((peers, 2, rows), F32, "any")
    dma = pltpu.SemaphoreType.DMA
    tall = ((rows, width), BF16)
    glu, edge, taps = kernel(
        glu_body,
        [wide(rows + PAD), wide(PAD), ((n, width), F32, "near")],
        (far(glu_value), far(glu_gate), far(conv_taps)),
        ins=[HBM] * 3,
        scratch=[tall, tall, dma((2, 5))],
    )
    edge = shifted(edge, 1)
    conv, stats, saved = kernel(
        conv_body,
        [wide(rows), ((8, rows), F32, "near"), kept_wide(rows + PAD)],
        (near(glu), near(taps)),
        out_specs=[VMEM, VMEM, HBM],
        scratch=[dma],
    )
    saved, _, conv, stats = kernel(
        head_body,
        [kept_wide(rows + PAD), wide(rows + PAD), wide(rows), stat],
        (far(saved), near(edge), near(glu), near(taps), near(conv), near(stats)),
        ins=[HBM],
        out_specs=[HBM, VMEM, VMEM, VMEM],
        aliases={0: 0, 2: 1, 4: 2},
        scratch=[((8, 256), F32), dma],
    )
    stats = over_tp(stats)
    (act_grad,) = kernel(
        act_body,
        [((rows, width), F32, "near")],
        (far(out_grad), far(proj_weight)),
        ins=[HBM] * 2,
        scratch=[((rows, outs), BF16), ((width, outs), BF16), dma((5,))],
    )
    stats, act_grad = lax.optimization_barrier((stats, act_grad))
    activ, xhat, scaled, sums, rstd, gain_sum = kernel(
        norm_body,
        [
            (*tall, "far"),
            kept_wide(rows),
            wide(rows),
            stat,
            ((1, rows), F32, "near"),
            wide(8),
        ],
        (near(stats), near(conv), near(act_grad), channel_gain[None]),
        out_specs=[HBM] * 2 + [VMEM] * 4,
        scratch=[((2, rows), F32), tall, wide(rows)[:2], dma((2, rows // LANES))],
    )
    sums = over_tp(sums)
    kept, sent = kernel(
        proj_body,
        [((width // 2, outs), F32, "far")] * 2,
        (lax.axis_index("core")[None], far(activ), far(out_grad)),
        ins=[SMEM, HBM, HBM],
        scratch=[tall, ((rows, outs), BF16), dma((2,))],
    )
    received = swapped(sent)
    sums, received = lax.optimization_barrier((sums, received))
    payload = ((8, 16, outs + 512), BF16, "far")
    share = ((width // 2, outs), F32)
    grad, small, first = kernel(
        taps_body,
        [wide(rows), ((n + 1, width), F32, "near"), payload],
        (
            far(kept), far(xhat), far(saved), near(received), near(sums), near(rstd),
            near(scaled), near(gain_sum),
        ),
        ins=[HBM] * 3,
        out_specs=[VMEM, VMEM, HBM],
        scratch=[
            ((2, rows), F32),
            ((2, rows, LANES), F32),
            share,
            wide(rows)[:2],
            wide(rows + PAD)[:2],
            ((8, 16, outs), BF16),
            dma((4,)),
        ],
    )
    other = swapped(small)
    (first,) = kernel(
        pack_body,
        [payload],
        (far(first), near(small), near(other)),
        ins=[HBM],
        out_specs=[HBM],
        aliases={0: 0},
        scratch=[((8, 16, 512), BF16), dma],
    )
    first = lax.all_to_all(first, "z", 0, 0, tiled=True)
    after = shifted(grad[:, :PAD], -1)
    first, after = lax.optimization_barrier((first, after))
    (second,) = kernel(
        relay_body, [((8, 8, 1280), F32, "any")], (near(first),), scratch=[((16, outs), F32)]
    )
    second = lax.all_to_all(second, "y", 0, 0, tiled=True)
    value_grad, gate_grad = kernel(
        glu_grad_body,
        [((rows, width), BF16, "any")] * 2,
        (near(grad), near(after), conv_taps, glu_value, glu_gate),
        scratch=[((2, rows + PAD, LANES), F32)],
    )
    second, value_grad, gate_grad = lax.optimization_barrier((second, value_grad, gate_grad))
    proj_grad, taps_grad, gain_grad = kernel(
        lambda *refs: final_body(factor, *refs),
        [((2, outs), F32, "any"), ((n, width), F32, "any"), ((1, width), F32, "any")],
        (near(second),),
    )
    return (value_grad, gate_grad, proj_grad, taps_grad, gain_grad.reshape(width))


def solution(mesh):
    finer = Mesh(mesh.devices.reshape(8, 8, 2, mesh.shape["tp"]), (*SP, "tp"))
    return jax.shard_map(
        per_device,
        mesh=finer,
        in_specs=(P(SP, "tp"), P(SP, "tp"), P(None, "tp"), P("tp"), P("tp", None), P(SP, None)),
        out_specs=(P(SP, "tp"), P(SP, "tp"), P(("tp", *SP), None), P(None, "tp"), P("tp")),
        check_vma=False,
    )
```

time: 103 us -> 93.7 us (0.910)
  local copies, waits for them, and re-layouts: 16.1 us -> 0.03 us
  blocking collectives: 0 us -> 6.65 us
  Pallas kernels: 24.2 us -> 28 us
  starting transfers between devices: 36.7 us -> 33.7 us
    unnamed x44 -> x8, local copies, waits for them, and re-layouts: 16.1 us -> 0.03 us
    all_to_all x0 -> x1, blocking collectives: none -> 6.65 us  [over_tp(): return lax.all_to_all(array, 'tp', 0, 0, tiled=True)]
    pallas_call x11, Pallas kernels: 24.2 us -> 28 us  [kernel(): pl.pallas_call(body, out_shape=[shapes[where](s, d) for s, d, where in ou...]
    all_to_all x2 -> x1, starting transfers between devices: 7.08 us -> 3.28 us  [over_tp(): return lax.all_to_all(array, 'tp', 0, 0, tiled=True)]
  transfers between devices with their start and end apart: 8 -> 7, of which waited for: 7 -> 6; matrix products, arithmetic and copies ran while one was open for 0% -> 0% of each run, Pallas kernels for 16% -> 12%
where the time goes in v3:
time: 93.7 us; the launch traced here: 93.1 us
  starting transfers between devices  33.7 us (36%)
  Pallas kernels  28 us (30%)
  waiting for transfers between devices  23.9 us (26%)
  blocking collectives  6.65 us (7%)
    pallas_call x11, Pallas kernels, kernel(): pl.pallas_call(body, out_shape=[shapes[where](s, d) for s, d, where in ou...  28 us
    all_to_all x1, starting transfers between devices, per_device(): first = lax.all_to_all(first, 'z', 0, 0, tiled=True)  10.1 us
    all_to_all x1, waiting for transfers between devices, per_device(): first = lax.all_to_all(first, 'z', 0, 0, tiled=True)  9.61 us
    ppermute x2, starting transfers between devices, swapped(): return lax.ppermute(block, 'core', [(0, 1), (1, 0)])  8.47 us
    all_to_all x1, waiting for transfers between devices, per_device(): second = lax.all_to_all(second, 'y', 0, 0, tiled=True)  8.03 us
    ppermute x2, starting transfers between devices, shifted(): return lax.ppermute(block, SP, route)  7.12 us
    all_to_all x1, blocking collectives, over_tp(): return lax.all_to_all(array, 'tp', 0, 0, tiled=True)  6.65 us
    all_to_all x1, starting transfers between devices, per_device(): second = lax.all_to_all(second, 'y', 0, 0, tiled=True)  4.75 us
  transfers between devices with their start and end apart: 7, of which 6 were waited for; matrix products, arithmetic and copies ran while one was open for 0% of the time, Pallas kernels for 12%

profile of v3, /device:TPU:1, one launch (start us, length us, event | category | flops | bytes accessed | tf_op | source)
XLA Modules:
  0.0 93.1 jit_solution(3262367559198015864)
XLA Ops:
  0.6 1.5 %shard_map.101 = (f32[2,1056,128]{2,1,0:T(8,128)S(1)}, f32[2,32,128]{2,1,0:T(8,128)S(1)}, f32[31,256]{1,0:T(8,128)S(1)}) custom-call(bf16[1024,256]{1,0:T(8,128)(2,1)} %value.1, bf16[1024,256]{1,0:T(8,128)(2,1)} %gate.1, f32[31,256]{1,0:T(8,128)} %taps.1), custom_call_target="tpu_custom_call" | custom-call | tf_op jit(solution)/shard_map/pallas_call | solution.py:47
  2.1 4.6 %collective-permute-start = (f32[2,32,128]{2,1,0:T(8,128)S(1)}, f32[2,32,128]{2,1,0:T(8,128)S(1)}, u32[]{:S(2)}, u32[]{:S(2)}) collective-permute-start(f32[2,32,128]{2,1,0:T(8,128)S(1)} %get-tuple-element.42), channel_id=1, source_target_pairs={{0,4},{4,8},{8,12},{12,16},{16,20},{20,24},{24,28},{28,32},{32,36}... | collective-permute-start | bytes 98312 | tf_op jit(solution)/shard_map/ppermute | solution.py:23
  6.7 3.0 %shard_map.102 = (f32[2,1024,128]{2,1,0:T(8,128)S(1)}, f32[8,1024]{1,0:T(8,128)S(1)}, f32[2,1056,128]{2,1,0:T(8,128)}) custom-call(f32[2,1056,128]{2,1,0:T(8,128)S(1)} %get-tuple-element.39.glu.glu_in, f32[31,256]{1,0:T(8,128)S(1)} %get-tuple-element.40.taps), custom_call_target="tpu_custom_call" | custom-call | tf_op jit(solution)/shard_map/pallas_call | solution.py:47
  9.7 1.2 %collective-permute-done.edge = f32[2,32,128]{2,1,0:T(8,128)S(1)} collective-permute-done((f32[2,32,128]{2,1,0:T(8,128)S(1)}, f32[2,32,128]{2,1,0:T(8,128)S(1)}, u32[]{:S(2)}, u32[]{:S(2)}) %collective-permute-start) | collective-permute-done | bytes 32800 | tf_op jit(solution)/shard_map/ppermute | solution.py:23
  10.9 1.6 %shard_map.103 = (f32[2,1056,128]{2,1,0:T(8,128)}, f32[2,1056,128]{2,1,0:T(8,128)S(1)}, f32[2,1024,128]{2,1,0:T(8,128)S(1)}, f32[4,2,1024]{2,1,0:T(2,128)}) custom-call(f32[2,1056,128]{2,1,0:T(8,128)} %get-tuple-element.41.saved_in, f32[2,32,128]{2,1,0:T(8,128)S(1)} %collective-permute-done.edge, ...), custom_call_target="tpu_custom_call", output_to_operand_aliasing={{0}: (0, {}), {1}: (2, {}), {2}: (4, {})} | custom-call | tf_op jit(solution)/shard_map/pallas_call | solution.py:47
  12.6 3.3 %all-to-all-start = ((f32[4,2,1024]{2,1,0:T(2,128)}), f32[4,2,1024]{2,1,0:T(2,128)S(1)}, u32[]{:S(2)}, u32[]{:S(2)}) async-start(f32[4,2,1024]{2,1,0:T(2,128)} %get-tuple-element.45), calls=%async_computation | async-start | bytes 65536 | tf_op jit(solution)/shard_map/all_to_all | solution.py:402
  15.8 0.0 copy-start.3
  15.9 3.1 %shard_map.104.act_grad = f32[1024,256]{1,0:T(8,128)S(1)} custom-call(bf16[1024,1024]{1,0:T(8,128)(2,1)} %grad_in.3, bf16[256,1024]{1,0:T(8,128)(2,1)} %weight_in.1), custom_call_target="tpu_custom_call" | custom-call | tf_op jit(solution)/shard_map/pallas_call | solution.py:47
  18.9 1.2 %all-to-all-done.stats = f32[4,2,1024]{2,1,0:T(2,128)S(1)} async-done(((f32[4,2,1024]{2,1,0:T(2,128)}), f32[4,2,1024]{2,1,0:T(2,128)S(1)}, u32[]{:S(2)}, u32[]{:S(2)}) %all-to-all-start) | async-done | bytes 32800 | tf_op jit(solution)/shard_map/all_to_all | solution.py:402
  20.1 3.7 %shard_map.105 = (bf16[1024,256]{1,0:T(8,128)(2,1)}, f32[2,1024,128]{2,1,0:T(8,128)}, f32[2,1024,128]{2,1,0:T(8,128)S(1)}, f32[4,2,1024]{2,1,0:T(2,128)S(1)}, f3...) custom-call(f32[4,2,1024]{2,1,0:T(2,128)S(1)} %all-to-all-done.stats, f32[2,1024,128]{2,1,0:T(8,128)S(1)} %get-tuple-element.47.conv, ...), custom_call_target="tpu_custom_call" | custom-call | tf_op jit(solution)/shard_map/pallas_call | solution.py:47
  23.8 3.5 %shard_map.106 = (f32[128,1024]{1,0:T(8,128)}, f32[128,1024]{1,0:T(8,128)}) custom-call(s32[1]{0:T(128)} %bitcast.me, bf16[1024,256]{1,0:T(8,128)(2,1)} %get-tuple-element.49.activ_in, bf16[1024,1024]{1,0:T(8,128)(2,1)} %grad_in.3), custom_call_target="tpu_custom_call" | custom-call | tf_op jit(solution)/shard_map/pallas_call | solution.py:47
  27.3 5.4 %collective-permute-start.1 = (f32[128,1024]{1,0:T(8,128)}, f32[128,1024]{1,0:T(8,128)S(1)}, u32[]{:S(2)}, u32[]{:S(2)}) collective-permute-start(f32[128,1024]{1,0:T(8,128)} %get-tuple-element.54), channel_id=1, source_target_pairs={{0,4},{4,0},{1,5},{5,1},{2,6},{6,2},{3,7},{7,3},{8,12},{12,8},{9,1... | collective-permute-start | bytes 1572872 | tf_op jit(solution)/shard_map/ppermute | solution.py:27
  32.7 6.7 %all_to_all.20.sums = f32[4,2,1024]{2,1,0:T(2,128)S(1)} all-to-all(f32[4,2,1024]{2,1,0:T(2,128)S(1)} %get-tuple-element.53), channel_id=1, replica_groups=mesh['z'=8,'y'=8,'core'=2,'tp'=4] {'tp'}, dimensions={0} | all-to-all | bytes 65536 | tf_op jit(solution)/shard_map/all_to_all | solution.py:402
  39.3 0.0 collective-permute-done.1.received
  39.3 4.7 %shard_map.107 = (f32[2,1024,128]{2,1,0:T(8,128)S(1)}, f32[32,256]{1,0:T(8,128)S(1)}, bf16[8,16,1536]{2,1,0:T(8,128)(2,1)}) custom-call(f32[128,1024]{1,0:T(8,128)} %get-tuple-element.50.kept_in, f32[2,1024,128]{2,1,0:T(8,128)} %get-tuple-element.51.xhat_in, f32[2,1056,128]{2,1,0:T(8,128)} %get-tuple-element.52.glu_in, ...), custom_call_target="tpu_custom_call" | custom-call | tf_op jit(solution)/shard_map/pallas_call | solution.py:47
  44.0 3.1 %collective-permute-start.2 = (f32[32,256]{1,0:T(8,128)S(1)}, f32[32,256]{1,0:T(8,128)S(1)}, u32[]{:S(2)}, u32[]{:S(2)}) collective-permute-start(f32[32,256]{1,0:T(8,128)S(1)} %get-tuple-element.61.small), channel_id=1, source_target_pairs={{0,4},{4,0},{1,5},{5,1},{2,6},{6,2},{3,7},{7,3},{8,12},{12,8},{9,1... | collective-permute-start | bytes 98312 | tf_op jit(solution)/shard_map/ppermute | solution.py:27
  47.1 0.8 collective-permute-done.2.other
  47.9 0.7 shard_map.108
  48.6 0.0 copy-start
  48.6 0.0 copy-start.1
  48.6 0.0 copy-start.2
  48.6 10.1 %all-to-all-start.2 = ((bf16[8,16,1536]{2,1,0:T(8,128)(2,1)}), bf16[8,16,1536]{2,1,0:T(8,128)(2,1)S(1)}, u32[]{:S(2)}, u32[]{:S(2)}) async-start(bf16[8,16,1536]{2,1,0:T(8,128)(2,1)} %shard_map.108), calls=%async_computation.2 | async-start | bytes 786432 | tf_op jit(solution)/shard_map/all_to_all | solution.py:509
  58.7 2.5 %collective-permute-start.3 = (f32[2,32,128]{2,1,0:T(8,128)S(1)}, f32[2,32,128]{2,1,0:T(8,128)S(1)}, u32[]{:S(2)}, u32[]{:S(2)}) collective-permute-start(f32[2,32,128]{2,1,0:T(8,128)S(1)} %slice.3), channel_id=1, source_target_pairs={{4,0},{8,4},{12,8},{16,12},{20,16},{24,20},{28,24},{32,28},{36,32}... | collective-permute-start | bytes 98312 | tf_op jit(solution)/shard_map/ppermute | solution.py:23
  61.3 3.0 %collective-permute-done.3.after = f32[2,32,128]{2,1,0:T(8,128)S(1)} collective-permute-done((f32[2,32,128]{2,1,0:T(8,128)S(1)}, f32[2,32,128]{2,1,0:T(8,128)S(1)}, u32[]{:S(2)}, u32[]{:S(2)}) %collective-permute-start.3) | collective-permute-done | bytes 32800 | tf_op jit(solution)/shard_map/ppermute | solution.py:23
  64.3 9.6 %all-to-all-done.2.got = bf16[8,16,1536]{2,1,0:T(8,128)(2,1)S(1)} async-done(((bf16[8,16,1536]{2,1,0:T(8,128)(2,1)}), bf16[8,16,1536]{2,1,0:T(8,128)(2,1)S(1)}, u32[]{:S(2)}, u32[]{:S(2)}) %all-to-all-start.2) | async-done | bytes 393248 | tf_op jit(solution)/shard_map/all_to_all | solution.py:509
  73.9 0.8 shard_map.109
  74.7 4.8 %all-to-all-start.3 = ((f32[8,8,1280]{2,1,0:T(8,128)}), f32[8,8,1280]{2,1,0:T(8,128)S(1)}, u32[]{:S(2)}, u32[]{:S(2)}) async-start(f32[8,8,1280]{2,1,0:T(8,128)} %shard_map.109), calls=%async_computation.3 | async-start | bytes 655360 | tf_op jit(solution)/shard_map/all_to_all | solution.py:515
  79.5 0.0 copy-done.1
  79.5 0.0 copy-done.2
  79.5 4.9 %shard_map.110 = (bf16[1024,256]{1,0:T(8,128)(2,1)}, bf16[1024,256]{1,0:T(8,128)(2,1)}) custom-call(f32[2,1024,128]{2,1,0:T(8,128)S(1)} %get-tuple-element.62.grad, f32[2,32,128]{2,1,0:T(8,128)S(1)} %collective-permute-done.3.after, f32[31,256]{1,0:T(8,128)S(1)} %copy-done.2, bf16[1024,256]{1,0:T(8,128)(2,1)S(1)} %copy-done, bf16[1024,256]{1,0:T(8,128)(2,1)S(1)} %copy-done.1), custom_call_target="tpu_custom_call" | custom-call | tf_op jit(solution)/shard_map/pallas_call | solution.py:47
  84.4 8.0 %all-to-all-done.3.refs_0_ = f32[8,8,1280]{2,1,0:T(8,128)S(1)} async-done(((f32[8,8,1280]{2,1,0:T(8,128)}), f32[8,8,1280]{2,1,0:T(8,128)S(1)}, u32[]{:S(2)}, u32[]{:S(2)}) %all-to-all-start.3) | async-done | bytes 327712 | tf_op jit(solution)/shard_map/all_to_all | solution.py:515
  92.4 0.6 shard_map.111
  (3 shorter events, 0.0 us)
Async XLA Ops:
  2.1 8.8 %collective-permute-start = (f32[2,32,128]{2,1,0:T(8,128)S(1)}, f32[2,32,128]{2,1,0:T(8,128)S(1)}, u32[]{:S(2)}, u32[]{:S(2)}) collective-permute-start(f32[2,32,128]{2,1,0:T(8,128)S(1)} %get-tuple-element.42), channel_id=1, source_target_pairs={{0,4},{4,8},{8,12},{12,16},{16,20},{20,24},{24,28},{28,32},{32,36}... | collective-permute-start | bytes 98312 | tf_op jit(solution)/shard_map/ppermute | solution.py:23
  12.6 7.5 %all-to-all-start = ((f32[4,2,1024]{2,1,0:T(2,128)}), f32[4,2,1024]{2,1,0:T(2,128)S(1)}, u32[]{:S(2)}, u32[]{:S(2)}) async-start(f32[4,2,1024]{2,1,0:T(2,128)} %get-tuple-element.45), calls=%async_computation | async-start | bytes 65536 | tf_op jit(solution)/shard_map/all_to_all | solution.py:402
  15.8 4.3 %copy-start.3 = (f32[256]{0:T(256)S(1)}, f32[256]{0:T(256)}, u32[]{:S(2)}) copy-start(f32[256]{0:T(256)} %param.9) | copy-start | bytes 3076
  27.3 12.1 %collective-permute-start.1 = (f32[128,1024]{1,0:T(8,128)}, f32[128,1024]{1,0:T(8,128)S(1)}, u32[]{:S(2)}, u32[]{:S(2)}) collective-permute-start(f32[128,1024]{1,0:T(8,128)} %get-tuple-element.54), channel_id=1, source_target_pairs={{0,4},{4,0},{1,5},{5,1},{2,6},{6,2},{3,7},{7,3},{8,12},{12,8},{9,1... | collective-permute-start | bytes 1572872 | tf_op jit(solution)/shard_map/ppermute | solution.py:27
  44.0 3.9 %collective-permute-start.2 = (f32[32,256]{1,0:T(8,128)S(1)}, f32[32,256]{1,0:T(8,128)S(1)}, u32[]{:S(2)}, u32[]{:S(2)}) collective-permute-start(f32[32,256]{1,0:T(8,128)S(1)} %get-tuple-element.61.small), channel_id=1, source_target_pairs={{0,4},{4,0},{1,5},{5,1},{2,6},{6,2},{3,7},{7,3},{8,12},{12,8},{9,1... | collective-permute-start | bytes 98312 | tf_op jit(solution)/shard_map/ppermute | solution.py:27
  48.6 30.9 %copy-start = (bf16[1024,256]{1,0:T(8,128)(2,1)S(1)}, bf16[1024,256]{1,0:T(8,128)(2,1)}, u32[]{:S(2)}) copy-start(bf16[1024,256]{1,0:T(8,128)(2,1)} %value.1) | copy-start | bytes 1572868
  48.6 30.8 %copy-start.1 = (bf16[1024,256]{1,0:T(8,128)(2,1)S(1)}, bf16[1024,256]{1,0:T(8,128)(2,1)}, u32[]{:S(2)}) copy-start(bf16[1024,256]{1,0:T(8,128)(2,1)} %gate.1) | copy-start | bytes 1572868
  48.6 30.8 %copy-start.2 = (f32[31,256]{1,0:T(8,128)S(1)}, f32[31,256]{1,0:T(8,128)}, u32[]{:S(2)}) copy-start(f32[31,256]{1,0:T(8,128)} %taps.1) | copy-start | bytes 95236
  48.6 25.2 %all-to-all-start.2 = ((bf16[8,16,1536]{2,1,0:T(8,128)(2,1)}), bf16[8,16,1536]{2,1,0:T(8,128)(2,1)S(1)}, u32[]{:S(2)}, u32[]{:S(2)}) async-start(bf16[8,16,1536]{2,1,0:T(8,128)(2,1)} %shard_map.108), calls=%async_computation.2 | async-start | bytes 786432 | tf_op jit(solution)/shard_map/all_to_all | solution.py:509
  58.7 5.5 %collective-permute-start.3 = (f32[2,32,128]{2,1,0:T(8,128)S(1)}, f32[2,32,128]{2,1,0:T(8,128)S(1)}, u32[]{:S(2)}, u32[]{:S(2)}) collective-permute-start(f32[2,32,128]{2,1,0:T(8,128)S(1)} %slice.3), channel_id=1, source_target_pairs={{4,0},{8,4},{12,8},{16,12},{20,16},{24,20},{28,24},{32,28},{36,32}... | collective-permute-start | bytes 98312 | tf_op jit(solution)/shard_map/ppermute | solution.py:23
  74.7 17.7 %all-to-all-start.3 = ((f32[8,8,1280]{2,1,0:T(8,128)}), f32[8,8,1280]{2,1,0:T(8,128)S(1)}, u32[]{:S(2)}, u32[]{:S(2)}) async-start(f32[8,8,1280]{2,1,0:T(8,128)} %shard_map.109), calls=%async_computation.3 | async-start | bytes 655360 | tf_op jit(solution)/shard_map/all_to_all | solution.py:515

commit v4 on v3

--- a/solution.py
+++ b/solution.py
@@ -14,7 +14,6 @@
 LANES = 128
 PAD = 32
 NT = (((1,), (1,)), ((), ()))
-TN = (((0,), (0,)), ((), ()))
 
 
 def shifted(block, distance):
@@ -166,102 +165,113 @@
     store.wait()
 
 
-def column(row):
-    return jnp.broadcast_to(row, (LANES, LANES)).T
+def spread(rows, stack, columns):
+    stats, length = rows.shape
+    blocks = length // LANES
+    stack[...] = jnp.zeros(stack.shape, F32)
+    for s in range(stats):
+        for b in range(blocks):
+            stack[s * blocks + b : s * blocks + b + 1, :] = rows[s : s + 1, b * LANES : (b + 1) * LANES]
+    turned = stack[...].T
+    for s in range(stats):
+        for b in range(blocks):
+            j = s * blocks + b
+            columns[s, b * LANES : (b + 1) * LANES] = jnp.broadcast_to(
+                turned[:, j : j + 1], (LANES, LANES)
+            )
 
 
 def norm_body(
-    stats, conv, act_grad, gain, activ_out, xhat_out, scaled, sums, rstd_out, gain_sum,
-    rows_in, activ, xhats, sems,
+    stats, conv, act_grad, gain, activ_out, xhat_out, scaled, sums, gain_sum,
+    rows_in, stack, columns, activ, xhats, sems,
 ):
     peers = stats.shape[0]
+    rows = conv.shape[1]
     channels = 2 * LANES * peers
     total = stats[0]
     for p in range(1, peers):
         total = total + stats[p]
     mean = total[0:1] * (1.0 / channels)
-    rstd = lax.rsqrt(total[1:2] * (1.0 / channels) - mean * mean + 1e-05)
-    rstd_out[...] = rstd
-    rows_in[0:1, :] = rstd
+    rows_in[0:1, :] = lax.rsqrt(total[1:2] * (1.0 / channels) - mean * mean + 1e-05)
     rows_in[1:2, :] = mean
+    spread(rows_in, stack, columns)
     for h in range(2):
         gain_sum[h] = jnp.zeros((8, LANES), F32)
+    size = 256
 
     def store(i):
-        at = pl.ds(pl.multiple_of(i * LANES, LANES), LANES)
+        at = pl.ds(pl.multiple_of(i * size, size), size)
         return (
             pltpu.make_async_copy(activ.at[at], activ_out.at[at], sems.at[0, i]),
             pltpu.make_async_copy(xhats.at[:, at], xhat_out.at[:, at], sems.at[1, i]),
         )
 
-    def step(i, carry):
-        r = pl.multiple_of(i * LANES, LANES)
-        rs = column(rows_in[0:1, pl.ds(r, LANES)])
-        mu = column(rows_in[1:2, pl.ds(r, LANES)])
+    def block(i, carry):
+        def step(j, carry):
+            at = pl.ds(pl.multiple_of(i * size + j * 32, 32), 32)
+            rs, mu = columns[0, at], columns[1, at]
+            for h in range(2):
+                g = gain[0:1, lanes(h)]
+                xhat = (conv[h, at, :] - mu) * rs
+                normed = xhat * g
+                sig = jax.nn.sigmoid(normed)
+                act = normed * sig
+                activ[at, lanes(h)] = act.astype(BF16)
+                ng = act_grad[at, lanes(h)] * (sig + act * (1.0 - sig))
+                gain_sum[h] += jnp.sum((ng * xhat).reshape(4, 8, LANES), axis=0)
+                xhats[h, at, :] = xhat
+                scaled[h, at, :] = ng * g * rs
+            return carry
+
+        lax.fori_loop(0, size // 32, step, 0)
+        for copy in store(i):
+            copy.start()
+        at = pl.ds(pl.multiple_of(i * size, size), size)
         pairs = []
         for h in range(2):
-            g = gain[0:1, lanes(h)]
-            xhat = (conv[h, pl.ds(r, LANES), :] - mu) * rs
-            normed = xhat * g
-            sig = jax.nn.sigmoid(normed)
-            activ[pl.ds(r, LANES), lanes(h)] = (normed * sig).astype(BF16)
-            ng = act_grad[pl.ds(r, LANES), lanes(h)] * (sig * (1.0 + normed * (1.0 - sig)))
-            gain_sum[h] += jnp.sum((ng * xhat).reshape(16, 8, LANES), axis=0)
-            xg = ng * g
-            xhats[h, pl.ds(r, LANES), :] = xhat
-            scaled[h, pl.ds(r, LANES), :] = xg * rs
-            pairs += [(0, xg), (1, xg * xhat)]
+            x = scaled[h, at, :]
+            pairs += [(0, x), (1, x * xhats[h, at, :])]
         out = row_sums(pairs)
         for p in range(peers):
-            sums[p, :, pl.ds(r, LANES)] = out[0:2]
-        for copy in store(i):
-            copy.start()
+            sums[p, :, at] = out[0:2]
         return carry
 
-    blocks = conv.shape[1] // LANES
-    lax.fori_loop(0, blocks, step, 0)
-    for i in range(blocks):
+    lax.fori_loop(0, rows // size, block, 0)
+    for i in range(rows // size):
         for copy in store(i):
             copy.wait()
 
 
 def taps_body(
-    kept_in, xhat_in, glu_in, received, sums, rstd, scaled, gain_sum, grad, small, packed,
-    rows_in, columns, kept, xhat, glu, joined, sems,
+    xhat_in, glu_in, sums, scaled, gain_sum, grad, small,
+    rows_in, stack, columns, xhat, glu, sems,
 ):
     rows = grad.shape[1]
-    load_xhat = pltpu.make_async_copy(xhat_in, xhat, sems.at[0])
-    load_kept = pltpu.make_async_copy(kept_in, kept, sems.at[1])
-    load_glu = pltpu.make_async_copy(glu_in, glu, sems.at[2])
-    load_xhat.start()
-    load_kept.start()
+    size = 256
+    loads = []
+    for i in range(rows // size):
+        at = pl.ds(i * size, size)
+        loads.append(pltpu.make_async_copy(xhat_in.at[:, at], xhat.at[:, at], sems.at[i]))
+        loads[i].start()
+    load_glu = pltpu.make_async_copy(glu_in, glu, sems.at[rows // size])
     load_glu.start()
     peers = sums.shape[0]
-    channels = 2 * LANES * peers
     n = small.shape[0] - 1
     total = sums[0]
     for p in range(1, peers):
         total = total + sums[p]
-    rows_in[...] = total * (rstd[...] * (1.0 / channels))
-    for b in range(rows // LANES):
-        at = slice(b * LANES, (b + 1) * LANES)
-        columns[0, at] = column(rows_in[0:1, at])
-        columns[1, at] = column(rows_in[1:2, at])
-    load_xhat.wait()
-
-    def step(i, carry):
-        at = pl.ds(pl.multiple_of(i * 64, 64), 64)
-        for h in range(2):
-            grad[h, at, :] = scaled[h, at, :] - columns[0, at] - xhat[h, at, :] * columns[1, at]
-        return carry
-
-    lax.fori_loop(0, rows // 64, step, 0)
-    load_kept.wait()
-    for p in range(joined.shape[0]):
-        at = slice(p * 16, (p + 1) * 16)
-        joined[p] = (kept[at] + received[at]).astype(BF16)
-    store = pltpu.make_async_copy(joined, packed.at[:, :, pl.ds(0, joined.shape[2])], sems.at[3])
-    store.start()
+    rows_in[...] = total * (1.0 / (2 * LANES * peers))
+    spread(rows_in, stack, columns)
+    for i in range(rows // size):
+        loads[i].wait()
+
+        def step(j, carry, i=i):
+            at = pl.ds(pl.multiple_of(i * size + j * 64, 64), 64)
+            for h in range(2):
+                grad[h, at, :] = scaled[h, at, :] - columns[0, at] - xhat[h, at, :] * columns[1, at]
+            return carry
+
+        lax.fori_loop(0, size // 64, step, 0)
     load_glu.wait()
     for h in range(2):
         for lo, hi in ((0, 16), (16, n)):
@@ -280,19 +290,17 @@
             for k in range(lo, hi):
                 small[k : k + 1, lanes(h)] = jnp.sum(acc[k - lo], axis=0, keepdims=True)
         small[n : n + 1, lanes(h)] = jnp.sum(gain_sum[h], axis=0, keepdims=True)
-    store.wait()
-
-
-def pack_body(packed_in, small, other, packed, piece, sem):
+
+
+def pack_body(kept, received, small, other, out):
+    outs = kept.shape[1]
     total = small[...] + other[...]
     low, high = total[0:16].astype(BF16), total[16:32].astype(BF16)
-    for p in range(piece.shape[0]):
-        piece[p, :, 0:256] = low
-        piece[p, :, 256:512] = high
-    outs = packed.shape[2] - 512
-    store = pltpu.make_async_copy(piece, packed.at[:, :, pl.ds(outs, 512)], sem)
-    store.start()
-    store.wait()
+    for p in range(out.shape[0]):
+        at = slice(p * 16, (p + 1) * 16)
+        out[p, :, 0:outs] = (kept[at] + received[at]).astype(BF16)
+        out[p, :, outs : outs + 256] = low
+        out[p, :, outs + 256 : outs + 512] = high
 
 
 def relay_body(got, out, held):
@@ -326,39 +334,66 @@
             proj[i : i + 1, 256 * j : 256 * j + 256] = total[4 * i + j : 4 * i + j + 1, 1024:1280]
 
 
-def glu_grad_body(grad, after, taps, value, gate, value_grad, gate_grad, ext):
-    rows = grad.shape[1]
+def moves(pairs, sems):
+    copies = [pltpu.make_async_copy(x, y, sems.at[k]) for k, (x, y) in enumerate(pairs)]
+    for copy in copies:
+        copy.start()
+    return copies
+
+
+def glu_grad_rows(source, offset, taps, value, gate, out_value, out_gate, first, count):
     n = taps.shape[0]
-
-    def fill(i, carry):
-        r = pl.multiple_of(i * 64, 64)
-        for h in range(2):
-            ext[h, pl.ds(r, 64), :] = grad[h, pl.ds(r, 64), :]
-        return carry
-
-    lax.fori_loop(0, rows // 64, fill, 0)
-    for h in range(2):
-        ext[h, rows : rows + PAD, :] = after[h]
+    for h in range(2):
         weights = [jnp.broadcast_to(taps[k : k + 1, lanes(h)], (8, LANES)) for k in range(n)]
 
         def step(i, carry, h=h, weights=weights):
             tiles = []
-            for u in range(2):
-                r = i * 16 + u * 8
+            for u in range(4):
+                r = offset + i * 32 + u * 8
                 parts = [None, None]
                 for k in range(n):
-                    term = weights[k] * ext[h, pl.ds(r + n - 1 - k, 8), :]
+                    term = weights[k] * source[h, pl.ds(r + n - 1 - k, 8), :]
                     parts[k % 2] = term if parts[k % 2] is None else parts[k % 2] + term
                 tiles.append(parts[0] + parts[1])
-            at = pl.ds(pl.multiple_of(i * 16, 16), 16)
-            dglu = jnp.concatenate(tiles, axis=0)
+            at = pl.ds(pl.multiple_of(first + i * 32, 32), 32)
             sig = jax.nn.sigmoid(gate[at, lanes(h)].astype(F32))
-            got = dglu * sig
-            value_grad[at, lanes(h)] = got.astype(BF16)
-            gate_grad[at, lanes(h)] = (got * value[at, lanes(h)].astype(F32) * (1.0 - sig)).astype(BF16)
+            got = jnp.concatenate(tiles, axis=0) * sig
+            out_value[at, lanes(h)] = got.astype(BF16)
+            out_gate[at, lanes(h)] = (got * value[at, lanes(h)].astype(F32) * (1.0 - sig)).astype(BF16)
             return carry
 
-        lax.fori_loop(0, rows // 16, step, 0)
+        lax.fori_loop(0, count // 32, step, 0)
+
+
+def glu_head_body(
+    value_in, gate_in, grad, taps, value_grad, gate_grad, value, gate, out_value, out_gate, sems
+):
+    count = value.shape[0]
+    at = pl.ds(0, count)
+    for copy in moves(((value_in.at[at], value), (gate_in.at[at], gate)), sems):
+        copy.wait()
+    glu_grad_rows(grad, 0, taps, value, gate, out_value, out_gate, 0, count)
+    for copy in moves(((out_value, value_grad.at[at]), (out_gate, gate_grad.at[at])), sems):
+        copy.wait()
+
+
+def glu_tail_body(
+    value_in, gate_in, value_part, gate_part, grad, after, taps, value_grad, gate_grad,
+    value, gate, out_value, out_gate, ext, sems,
+):
+    count = value.shape[0]
+    rows = grad.shape[1]
+    at = pl.ds(rows - count, count)
+    loads = moves(((value_in.at[at], value), (gate_in.at[at], gate)), sems)
+    for h in range(2):
+        ext[h, 0:PAD, :] = grad[h, rows - PAD :, :]
+        ext[h, PAD : 2 * PAD, :] = after[h]
+    for load in loads:
+        load.wait()
+    glu_grad_rows(grad, rows - count, taps, value, gate, out_value, out_gate, 0, count - PAD)
+    glu_grad_rows(ext, 0, taps, value, gate, out_value, out_gate, count - PAD, PAD)
+    for copy in moves(((out_value, value_grad.at[at]), (out_gate, gate_grad.at[at])), sems):
+        copy.wait()
 
 
 def act_body(grad_in, weight_in, act, out_grad, weight, sems):
@@ -378,24 +413,40 @@
         act[at] = lax.dot_general(out_grad[at], weight[...], NT, preferred_element_type=F32)
 
 
-def proj_body(me, activ_in, grad_in, kept, sent, activ, out_grad, sems):
-    load_activ = pltpu.make_async_copy(activ_in, activ, sems.at[0])
-    load_grad = pltpu.make_async_copy(grad_in, out_grad, sems.at[1])
-    load_activ.start()
-    load_grad.start()
+def proj_body(me, activ_in, grad_in, kept_out, sent_out, activ, out_grad, kept, sent, sems):
+    chunks = 4
+    outs = out_grad.shape[1]
+    size = outs // chunks
     width = activ.shape[1]
     half = width // 2
+    load_activ = pltpu.make_async_copy(activ_in, activ, sems.at[chunks])
+    load_activ.start()
+    loads = []
+    for c in range(chunks):
+        at = pl.ds(c * size, size)
+        loads.append(pltpu.make_async_copy(grad_in.at[:, at], out_grad.at[:, at], sems.at[c]))
+        loads[c].start()
     row = lax.broadcasted_iota(jnp.int32, (width, width), 0)
     col = lax.broadcasted_iota(jnp.int32, (width, width), 1)
-    low = jnp.bitwise_and(col, half - 1)
-    high = jnp.bitwise_xor(jnp.right_shift(col, 7), me[0])
-    source = jnp.left_shift(jnp.right_shift(low, 1), 2) + 2 * high + jnp.bitwise_and(col, 1)
-    order = (row == source).astype(F32).astype(BF16)
+    low = jnp.bitwise_and(row, half - 1)
+    high = jnp.bitwise_xor(jnp.right_shift(row, 7), me[0])
+    source = jnp.left_shift(jnp.right_shift(low, 1), 2) + 2 * high + jnp.bitwise_and(row, 1)
+    order = (col == source).astype(F32).astype(BF16)
     load_activ.wait()
-    placed = jnp.dot(activ[...], order, preferred_element_type=F32).astype(BF16)
-    load_grad.wait()
-    sent[...] = lax.dot_general(placed[:, half:], out_grad[...], TN, preferred_element_type=F32)
-    kept[...] = lax.dot_general(placed[:, :half], out_grad[...], TN, preferred_element_type=F32)
+    placed = lax.dot_general(order, activ[...], NT, preferred_element_type=F32).astype(BF16)
+    stores = []
+    for c in range(chunks):
+        loads[c].wait()
+        at = pl.ds(c * size, size)
+        got = jnp.dot(placed, out_grad[:, at], preferred_element_type=F32)
+        kept[:, at] = got[:half]
+        sent[:, at] = got[half:]
+        stores.append(pltpu.make_async_copy(sent.at[:, at], sent_out.at[:, at], sems.at[c]))
+        stores.append(pltpu.make_async_copy(kept.at[:, at], kept_out.at[:, at], sems.at[chunks + 1 + c]))
+        stores[2 * c].start()
+        stores[2 * c + 1].start()
+    for store in stores:
+        store.wait()
 
 
 def over_tp(array):
@@ -451,73 +502,66 @@
         scratch=[((rows, outs), BF16), ((width, outs), BF16), dma((5,))],
     )
     stats, act_grad = lax.optimization_barrier((stats, act_grad))
-    activ, xhat, scaled, sums, rstd, gain_sum = kernel(
+    spreading = [((2, rows), F32), ((LANES, LANES), F32), ((2, rows, LANES), F32)]
+    activ, xhat, scaled, sums, gain_sum = kernel(
         norm_body,
-        [
-            (*tall, "far"),
-            kept_wide(rows),
-            wide(rows),
-            stat,
-            ((1, rows), F32, "near"),
-            wide(8),
-        ],
+        [(*tall, "far"), kept_wide(rows), wide(rows), stat, wide(8)],
         (near(stats), near(conv), near(act_grad), channel_gain[None]),
-        out_specs=[HBM] * 2 + [VMEM] * 4,
-        scratch=[((2, rows), F32), tall, wide(rows)[:2], dma((2, rows // LANES))],
+        out_specs=[HBM] * 2 + [VMEM] * 3,
+        scratch=[*spreading, tall, wide(rows)[:2], dma((2, 4))],
     )
     sums = over_tp(sums)
+    share = ((width // 2, outs), F32)
     kept, sent = kernel(
         proj_body,
-        [((width // 2, outs), F32, "far")] * 2,
+        [(*share, "far")] * 2,
         (lax.axis_index("core")[None], far(activ), far(out_grad)),
         ins=[SMEM, HBM, HBM],
-        scratch=[tall, ((rows, outs), BF16), dma((2,))],
-    )
+        out_specs=[HBM] * 2,
+        scratch=[tall, ((rows, outs), BF16), share, share, dma((9,))],
+    )
+    sums, sent, kept = lax.optimization_barrier((sums, sent, kept))
     received = swapped(sent)
-    sums, received = lax.optimization_barrier((sums, received))
-    payload = ((8, 16, outs + 512), BF16, "far")
-    share = ((width // 2, outs), F32)
-    grad, small, first = kernel(
+    grad, small = kernel(
         taps_body,
-        [wide(rows), ((n + 1, width), F32, "near"), payload],
-        (
-            far(kept), far(xhat), far(saved), near(received), near(sums), near(rstd),
-            near(scaled), near(gain_sum),
-        ),
-        ins=[HBM] * 3,
-        out_specs=[VMEM, VMEM, HBM],
-        scratch=[
-            ((2, rows), F32),
-            ((2, rows, LANES), F32),
-            share,
-            wide(rows)[:2],
-            wide(rows + PAD)[:2],
-            ((8, 16, outs), BF16),
-            dma((4,)),
-        ],
+        [wide(rows), ((n + 1, width), F32, "near")],
+        (far(xhat), far(saved), near(sums), near(scaled), near(gain_sum)),
+        ins=[HBM] * 2,
+        scratch=[*spreading, wide(rows)[:2], wide(rows + PAD)[:2], dma((5,))],
     )
     other = swapped(small)
     (first,) = kernel(
         pack_body,
-        [payload],
-        (far(first), near(small), near(other)),
-        ins=[HBM],
-        out_specs=[HBM],
-        aliases={0: 0},
-        scratch=[((8, 16, 512), BF16), dma],
+        [((8, 16, outs + 512), BF16, "any")],
+        (near(kept), near(received), near(small), near(other)),
     )
     first = lax.all_to_all(first, "z", 0, 0, tiled=True)
     after = shifted(grad[:, :PAD], -1)
-    first, after = lax.optimization_barrier((first, after))
+    gates = [((rows // 2, width), BF16)] * 4
+    value_grad, gate_grad = kernel(
+        glu_head_body,
+        [(*tall, "far")] * 2,
+        (far(glu_value), far(glu_gate), near(grad), conv_taps),
+        ins=[HBM] * 2,
+        out_specs=[HBM] * 2,
+        scratch=[*gates, dma((2,))],
+    )
+    first, after, value_grad, gate_grad = lax.optimization_barrier((first, after, value_grad, gate_grad))
     (second,) = kernel(
         relay_body, [((8, 8, 1280), F32, "any")], (near(first),), scratch=[((16, outs), F32)]
     )
     second = lax.all_to_all(second, "y", 0, 0, tiled=True)
     value_grad, gate_grad = kernel(
-        glu_grad_body,
-        [((rows, width), BF16, "any")] * 2,
-        (near(grad), near(after), conv_taps, glu_value, glu_gate),
-        scratch=[((2, rows + PAD, LANES), F32)],
+        glu_tail_body,
+        [(*tall, "far")] * 2,
+        (
+            far(glu_value), far(glu_gate), far(value_grad), far(gate_grad), near(grad),
+            near(after), conv_taps,
+        ),
+        ins=[HBM] * 4,
+        out_specs=[HBM] * 2,
+        aliases={2: 0, 3: 1},
+        scratch=[*gates, ((2, 2 * PAD, LANES), F32), dma((2,))],
     )
     second, value_grad, gate_grad = lax.optimization_barrier((second, value_grad, gate_grad))
     proj_grad, taps_grad, gain_grad = kernel(

time: 93.7 us -> 91.4 us (0.975)
  blocking collectives: 6.65 us -> 0 us
  Pallas kernels: 28 us -> 31 us
  starting transfers between devices: 33.7 us -> 36.6 us
  waiting for transfers between devices: 23.9 us -> 22.3 us
    all_to_all x1 -> x0, blocking collectives: 6.65 us -> none  [over_tp(): return lax.all_to_all(array, 'tp', 0, 0, tiled=True)]
    all_to_all x1 -> x2, starting transfers between devices: 3.28 us -> 6.55 us  [over_tp(): return lax.all_to_all(array, 'tp', 0, 0, tiled=True)]
    ppermute x2, waiting for transfers between devices: 4.2 us -> 1.22 us  [shifted(): return lax.ppermute(block, SP, route)]
    pallas_call x11 -> x12, Pallas kernels: 28 us -> 31 us  [kernel(): pl.pallas_call(body, out_shape=[shapes[where](s, d) for s, d, where in ou...]
    all_to_all x1, waiting for transfers between devices: 8.03 us -> 9.27 us  [per_device(): second = lax.all_to_all(second, 'y', 0, 0, tiled=True)]
  transfers between devices with their start and end apart: 7 -> 8, of which waited for: 6 -> 6; matrix products, arithmetic and copies ran while one was open for 0% -> 0% of each run, Pallas kernels for 12% -> 24%
where the time goes in v4:
time: 91.4 us; the launch traced here: 90.7 us
  starting transfers between devices  36.6 us (40%)
  Pallas kernels  31 us (34%)
  waiting for transfers between devices  22.3 us (24%)
    pallas_call x12, Pallas kernels, kernel(): pl.pallas_call(body, out_shape=[shapes[where](s, d) for s, d, where in ou...  31 us
    all_to_all x1, starting transfers between devices, per_device(): first = lax.all_to_all(first, 'z', 0, 0, tiled=True)  9.95 us
    all_to_all x1, waiting for transfers between devices, per_device(): second = lax.all_to_all(second, 'y', 0, 0, tiled=True)  9.27 us
    all_to_all x1, waiting for transfers between devices, per_device(): first = lax.all_to_all(first, 'z', 0, 0, tiled=True)  9.04 us
    ppermute x2, starting transfers between devices, swapped(): return lax.ppermute(block, 'core', [(0, 1), (1, 0)])  8.46 us
    ppermute x2, starting transfers between devices, shifted(): return lax.ppermute(block, SP, route)  6.93 us
    all_to_all x2, starting transfers between devices, over_tp(): return lax.all_to_all(array, 'tp', 0, 0, tiled=True)  6.55 us
    all_to_all x1, starting transfers between devices, per_device(): second = lax.all_to_all(second, 'y', 0, 0, tiled=True)  4.74 us
  transfers between devices with their start and end apart: 8, of which 6 were waited for; matrix products, arithmetic and copies ran while one was open for 0% of the time, Pallas kernels for 24%

profile of v4, /device:TPU:1, one launch (start us, length us, event | category | flops | bytes accessed | tf_op | source)
XLA Modules:
  0.0 90.7 jit_solution(13024227865539531507)
XLA Ops:
  0.6 1.5 %shard_map.101 = (f32[2,1056,128]{2,1,0:T(8,128)S(1)}, f32[2,32,128]{2,1,0:T(8,128)S(1)}, f32[31,256]{1,0:T(8,128)S(1)}) custom-call(bf16[1024,256]{1,0:T(8,128)(2,1)} %value_in.5, bf16[1024,256]{1,0:T(8,128)(2,1)} %gate_in.5, f32[31,256]{1,0:T(8,128)} %taps.3), custom_call_target="tpu_custom_call" | custom-call | tf_op jit(solution)/shard_map/pallas_call | solution.py:46
  2.1 4.6 %collective-permute-start = (f32[2,32,128]{2,1,0:T(8,128)S(1)}, f32[2,32,128]{2,1,0:T(8,128)S(1)}, u32[]{:S(2)}, u32[]{:S(2)}) collective-permute-start(f32[2,32,128]{2,1,0:T(8,128)S(1)} %get-tuple-element.45), channel_id=1, source_target_pairs={{0,4},{4,8},{8,12},{12,16},{16,20},{20,24},{24,28},{28,32},{32,36}... | collective-permute-start | bytes 98312 | tf_op jit(solution)/shard_map/ppermute | solution.py:22
  6.7 3.0 %shard_map.102 = (f32[2,1024,128]{2,1,0:T(8,128)S(1)}, f32[8,1024]{1,0:T(8,128)S(1)}, f32[2,1056,128]{2,1,0:T(8,128)}) custom-call(f32[2,1056,128]{2,1,0:T(8,128)S(1)} %get-tuple-element.42.glu.glu_in, f32[31,256]{1,0:T(8,128)S(1)} %get-tuple-element.43.taps), custom_call_target="tpu_custom_call" | custom-call | tf_op jit(solution)/shard_map/pallas_call | solution.py:46
  9.7 1.2 %collective-permute-done.edge = f32[2,32,128]{2,1,0:T(8,128)S(1)} collective-permute-done((f32[2,32,128]{2,1,0:T(8,128)S(1)}, f32[2,32,128]{2,1,0:T(8,128)S(1)}, u32[]{:S(2)}, u32[]{:S(2)}) %collective-permute-start) | collective-permute-done | bytes 32800 | tf_op jit(solution)/shard_map/ppermute | solution.py:22
  10.9 1.6 %shard_map.103 = (f32[2,1056,128]{2,1,0:T(8,128)}, f32[2,1056,128]{2,1,0:T(8,128)S(1)}, f32[2,1024,128]{2,1,0:T(8,128)S(1)}, f32[4,2,1024]{2,1,0:T(2,128)}) custom-call(f32[2,1056,128]{2,1,0:T(8,128)} %get-tuple-element.44.saved_in, f32[2,32,128]{2,1,0:T(8,128)S(1)} %collective-permute-done.edge, ...), custom_call_target="tpu_custom_call", output_to_operand_aliasing={{0}: (0, {}), {1}: (2, {}), {2}: (4, {})} | custom-call | tf_op jit(solution)/shard_map/pallas_call | solution.py:46
  12.6 3.3 %all-to-all-start = ((f32[4,2,1024]{2,1,0:T(2,128)}), f32[4,2,1024]{2,1,0:T(2,128)S(1)}, u32[]{:S(2)}, u32[]{:S(2)}) async-start(f32[4,2,1024]{2,1,0:T(2,128)} %get-tuple-element.48), calls=%async_computation | async-start | bytes 65536 | tf_op jit(solution)/shard_map/all_to_all | solution.py:453
  15.8 0.0 copy-start.2
  15.9 3.1 %shard_map.104.act_grad = f32[1024,256]{1,0:T(8,128)S(1)} custom-call(bf16[1024,1024]{1,0:T(8,128)(2,1)} %grad_in.3, bf16[256,1024]{1,0:T(8,128)(2,1)} %weight_in.1), custom_call_target="tpu_custom_call" | custom-call | tf_op jit(solution)/shard_map/pallas_call | solution.py:46
  18.9 1.2 %all-to-all-done.stats = f32[4,2,1024]{2,1,0:T(2,128)S(1)} async-done(((f32[4,2,1024]{2,1,0:T(2,128)}), f32[4,2,1024]{2,1,0:T(2,128)S(1)}, u32[]{:S(2)}, u32[]{:S(2)}) %all-to-all-start) | async-done | bytes 32800 | tf_op jit(solution)/shard_map/all_to_all | solution.py:453
  20.1 0.0 copy-done.2
  20.1 3.7 %shard_map.105 = (bf16[1024,256]{1,0:T(8,128)(2,1)}, f32[2,1024,128]{2,1,0:T(8,128)}, f32[2,1024,128]{2,1,0:T(8,128)S(1)}, f32[4,2,1024]{2,1,0:T(2,128)}, f32[2,8,128]{2,1,0:T(8,128)S(1)}) custom-call(f32[4,2,1024]{2,1,0:T(2,128)S(1)} %all-to-all-done.stats, f32[2,1024,128]{2,1,0:T(8,128)S(1)} %get-tuple-element.50.conv, ...), custom_call_target="tpu_custom_call" | custom-call | tf_op jit(solution)/shard_map/pallas_call | solution.py:46
  23.8 3.3 %all-to-all-start.1 = ((f32[4,2,1024]{2,1,0:T(2,128)}), f32[4,2,1024]{2,1,0:T(2,128)S(1)}, u32[]{:S(2)}, u32[]{:S(2)}) async-start(f32[4,2,1024]{2,1,0:T(2,128)} %get-tuple-element.52), calls=%async_computation.1 | async-start | bytes 65536 | tf_op jit(solution)/shard_map/all_to_all | solution.py:453
  27.1 3.8 %shard_map.106 = (f32[128,1024]{1,0:T(8,128)}, f32[128,1024]{1,0:T(8,128)}) custom-call(s32[1]{0:T(128)} %bitcast.1.me, bf16[1024,256]{1,0:T(8,128)(2,1)} %get-tuple-element.53.activ_in, bf16[1024,1024]{1,0:T(8,128)(2,1)} %grad_in.3), custom_call_target="tpu_custom_call" | custom-call | tf_op jit(solution)/shard_map/pallas_call | solution.py:46
  31.0 0.4 all-to-all-done.1.sums
  31.4 6.5 %collective-permute-start.1 = (f32[128,1024]{1,0:T(8,128)}, f32[128,1024]{1,0:T(8,128)S(1)}, u32[]{:S(2)}, u32[]{:S(2)}) collective-permute-start(f32[128,1024]{1,0:T(8,128)} %get-tuple-element.57), channel_id=1, source_target_pairs={{0,4},{4,0},{1,5},{5,1},{2,6},{6,2},{3,7},{7,3},{8,12},{12,8},{9,1... | collective-permute-start | bytes 1572872 | tf_op jit(solution)/shard_map/ppermute | solution.py:26
  37.9 0.0 copy-start
  37.9 4.6 %shard_map.107 = (f32[2,1024,128]{2,1,0:T(8,128)S(1)}, f32[32,256]{1,0:T(8,128)S(1)}) custom-call(f32[2,1024,128]{2,1,0:T(8,128)} %get-tuple-element.58.xhat_in, f32[2,1056,128]{2,1,0:T(8,128)} %get-tuple-element.59.glu_in, f32[4,2,1024]{2,1,0:T(2,128)S(1)} %all-to-all-done.1.sums, f32[2,1024,128]{2,1,0:T(8,128)S(1)} %get-tuple-element.61.scaled, ...), custom_call_target="tpu_custom_call" | custom-call | tf_op jit(solution)/shard_map/pallas_call | solution.py:46
  42.5 0.0 copy-start.1
  42.5 1.9 %collective-permute-start.2 = (f32[32,256]{1,0:T(8,128)S(1)}, f32[32,256]{1,0:T(8,128)S(1)}, u32[]{:S(2)}, u32[]{:S(2)}) collective-permute-start(f32[32,256]{1,0:T(8,128)S(1)} %get-tuple-element.63.small), channel_id=1, source_target_pairs={{0,4},{4,0},{1,5},{5,1},{2,6},{6,2},{3,7},{7,3},{8,12},{12,8},{9,1... | collective-permute-start | bytes 98312 | tf_op jit(solution)/shard_map/ppermute | solution.py:26
  44.4 1.2 %collective-permute-done.2.other = f32[32,256]{1,0:T(8,128)S(1)} collective-permute-done((f32[32,256]{1,0:T(8,128)S(1)}, f32[32,256]{1,0:T(8,128)S(1)}, u32[]{:S(2)}, u32[]{:S(2)}) %collective-permute-start.2) | collective-permute-done | bytes 32800 | tf_op jit(solution)/shard_map/ppermute | solution.py:26
  45.6 0.0 collective-permute-done.1.received
  45.6 0.8 shard_map.108
  46.4 9.9 %all-to-all-start.2 = ((bf16[8,16,1536]{2,1,0:T(8,128)(2,1)}), bf16[8,16,1536]{2,1,0:T(8,128)(2,1)S(1)}, u32[]{:S(2)}, u32[]{:S(2)}) async-start(bf16[8,16,1536]{2,1,0:T(8,128)(2,1)} %shard_map.108), calls=%async_computation.2 | async-start | bytes 786432 | tf_op jit(solution)/shard_map/all_to_all | solution.py:538
  56.4 2.4 %collective-permute-start.3 = (f32[2,32,128]{2,1,0:T(8,128)S(1)}, f32[2,32,128]{2,1,0:T(8,128)S(1)}, u32[]{:S(2)}, u32[]{:S(2)}) collective-permute-start(f32[2,32,128]{2,1,0:T(8,128)S(1)} %slice.3), channel_id=1, source_target_pairs={{4,0},{8,4},{12,8},{16,12},{20,16},{24,20},{28,24},{32,28},{36,32}... | collective-permute-start | bytes 98312 | tf_op jit(solution)/shard_map/ppermute | solution.py:22
  58.8 3.7 %shard_map.109 = (bf16[1024,256]{1,0:T(8,128)(2,1)}, bf16[1024,256]{1,0:T(8,128)(2,1)}) custom-call(bf16[1024,256]{1,0:T(8,128)(2,1)} %value_in.5, bf16[1024,256]{1,0:T(8,128)(2,1)} %gate_in.5, f32[2,1024,128]{2,1,0:T(8,128)S(1)} %get-tuple-element.64.grad, f32[31,256]{1,0:T(8,128)S(1)} %copy-done.1), custom_call_target="tpu_custom_call" | custom-call | tf_op jit(solution)/shard_map/pallas_call | solution.py:46
  62.5 0.0 collective-permute-done.3.after
  62.5 9.0 %all-to-all-done.2.got = bf16[8,16,1536]{2,1,0:T(8,128)(2,1)S(1)} async-done(((bf16[8,16,1536]{2,1,0:T(8,128)(2,1)}), bf16[8,16,1536]{2,1,0:T(8,128)(2,1)S(1)}, u32[]{:S(2)}, u32[]{:S(2)}) %all-to-all-start.2) | async-done | bytes 393248 | tf_op jit(solution)/shard_map/all_to_all | solution.py:538
  71.5 0.8 shard_map.110
  72.3 4.7 %all-to-all-start.3 = ((f32[8,8,1280]{2,1,0:T(8,128)}), f32[8,8,1280]{2,1,0:T(8,128)S(1)}, u32[]{:S(2)}, u32[]{:S(2)}) async-start(f32[8,8,1280]{2,1,0:T(8,128)} %shard_map.110), calls=%async_computation.3 | async-start | bytes 655360 | tf_op jit(solution)/shard_map/all_to_all | solution.py:553
  77.1 3.7 %shard_map.111 = (bf16[1024,256]{1,0:T(8,128)(2,1)}, bf16[1024,256]{1,0:T(8,128)(2,1)}) custom-call(bf16[1024,256]{1,0:T(8,128)(2,1)} %value_in.5, bf16[1024,256]{1,0:T(8,128)(2,1)} %gate_in.5, bf16[1024,256]{1,0:T(8,128)(2,1)} %get-tuple-element.68.value_part, ...), custom_call_target="tpu_custom_call", output_to_operand_aliasing={{0}: (2, {}), {1}: (3, {})} | custom-call | tf_op jit(solution)/shard_map/pallas_call | solution.py:46
  80.8 9.3 %all-to-all-done.3.refs_0_ = f32[8,8,1280]{2,1,0:T(8,128)S(1)} async-done(((f32[8,8,1280]{2,1,0:T(8,128)}), f32[8,8,1280]{2,1,0:T(8,128)S(1)}, u32[]{:S(2)}, u32[]{:S(2)}) %all-to-all-start.3) | async-done | bytes 327712 | tf_op jit(solution)/shard_map/all_to_all | solution.py:553
  90.1 0.6 shard_map.112
  (3 shorter events, 0.0 us)
Async XLA Ops:
  2.1 8.8 %collective-permute-start = (f32[2,32,128]{2,1,0:T(8,128)S(1)}, f32[2,32,128]{2,1,0:T(8,128)S(1)}, u32[]{:S(2)}, u32[]{:S(2)}) collective-permute-start(f32[2,32,128]{2,1,0:T(8,128)S(1)} %get-tuple-element.45), channel_id=1, source_target_pairs={{0,4},{4,8},{8,12},{12,16},{16,20},{20,24},{24,28},{28,32},{32,36}... | collective-permute-start | bytes 98312 | tf_op jit(solution)/shard_map/ppermute | solution.py:22
  12.6 7.5 %all-to-all-start = ((f32[4,2,1024]{2,1,0:T(2,128)}), f32[4,2,1024]{2,1,0:T(2,128)S(1)}, u32[]{:S(2)}, u32[]{:S(2)}) async-start(f32[4,2,1024]{2,1,0:T(2,128)} %get-tuple-element.48), calls=%async_computation | async-start | bytes 65536 | tf_op jit(solution)/shard_map/all_to_all | solution.py:453
  15.8 4.3 %copy-start.2 = (f32[256]{0:T(256)S(1)}, f32[256]{0:T(256)}, u32[]{:S(2)}) copy-start(f32[256]{0:T(256)} %param.9) | copy-start | bytes 3076
  23.8 7.5 %all-to-all-start.1 = ((f32[4,2,1024]{2,1,0:T(2,128)}), f32[4,2,1024]{2,1,0:T(2,128)S(1)}, u32[]{:S(2)}, u32[]{:S(2)}) async-start(f32[4,2,1024]{2,1,0:T(2,128)} %get-tuple-element.52), calls=%async_computation.1 | async-start | bytes 65536 | tf_op jit(solution)/shard_map/all_to_all | solution.py:453
  31.4 14.2 %collective-permute-start.1 = (f32[128,1024]{1,0:T(8,128)}, f32[128,1024]{1,0:T(8,128)S(1)}, u32[]{:S(2)}, u32[]{:S(2)}) collective-permute-start(f32[128,1024]{1,0:T(8,128)} %get-tuple-element.57), channel_id=1, source_target_pairs={{0,4},{4,0},{1,5},{5,1},{2,6},{6,2},{3,7},{7,3},{8,12},{12,8},{9,1... | collective-permute-start | bytes 1572872 | tf_op jit(solution)/shard_map/ppermute | solution.py:26
  37.9 7.7 %copy-start = (f32[128,1024]{1,0:T(8,128)S(1)}, f32[128,1024]{1,0:T(8,128)}, u32[]{:S(2)}) copy-start(f32[128,1024]{1,0:T(8,128)} %get-tuple-element.56.kept) | copy-start | bytes 1572868
  42.5 16.2 %copy-start.1 = (f32[31,256]{1,0:T(8,128)S(1)}, f32[31,256]{1,0:T(8,128)}, u32[]{:S(2)}) copy-start(f32[31,256]{1,0:T(8,128)} %taps.3) | copy-start | bytes 95236
  42.5 3.1 %collective-permute-start.2 = (f32[32,256]{1,0:T(8,128)S(1)}, f32[32,256]{1,0:T(8,128)S(1)}, u32[]{:S(2)}, u32[]{:S(2)}) collective-permute-start(f32[32,256]{1,0:T(8,128)S(1)} %get-tuple-element.63.small), channel_id=1, source_target_pairs={{0,4},{4,0},{1,5},{5,1},{2,6},{6,2},{3,7},{7,3},{8,12},{12,8},{9,1... | collective-permute-start | bytes 98312 | tf_op jit(solution)/shard_map/ppermute | solution.py:26
  46.4 25.1 %all-to-all-start.2 = ((bf16[8,16,1536]{2,1,0:T(8,128)(2,1)}), bf16[8,16,1536]{2,1,0:T(8,128)(2,1)S(1)}, u32[]{:S(2)}, u32[]{:S(2)}) async-start(bf16[8,16,1536]{2,1,0:T(8,128)(2,1)} %shard_map.108), calls=%async_computation.2 | async-start | bytes 786432 | tf_op jit(solution)/shard_map/all_to_all | solution.py:538
  56.4 6.1 %collective-permute-start.3 = (f32[2,32,128]{2,1,0:T(8,128)S(1)}, f32[2,32,128]{2,1,0:T(8,128)S(1)}, u32[]{:S(2)}, u32[]{:S(2)}) collective-permute-start(f32[2,32,128]{2,1,0:T(8,128)S(1)} %slice.3), channel_id=1, source_target_pairs={{4,0},{8,4},{12,8},{16,12},{20,16},{24,20},{28,24},{32,28},{36,32}... | collective-permute-start | bytes 98312 | tf_op jit(solution)/shard_map/ppermute | solution.py:22
  72.3 17.7 %all-to-all-start.3 = ((f32[8,8,1280]{2,1,0:T(8,128)}), f32[8,8,1280]{2,1,0:T(8,128)S(1)}, u32[]{:S(2)}, u32[]{:S(2)}) async-start(f32[8,8,1280]{2,1,0:T(8,128)} %shard_map.110), calls=%async_computation.3 | async-start | bytes 655360 | tf_op jit(solution)/shard_map/all_to_all | solution.py:553

commit v5 on v4

--- a/solution.py
+++ b/solution.py
@@ -243,8 +243,8 @@
 
 
 def taps_body(
-    xhat_in, glu_in, sums, scaled, gain_sum, grad, small,
-    rows_in, stack, columns, xhat, glu, sems,
+    taps_count, xhat_in, glu_in, sent_in, sums, scaled, gain_sum, grad, sent,
+    rows_in, stack, columns, xhat, glu, small, sems,
 ):
     rows = grad.shape[1]
     size = 256
@@ -256,7 +256,7 @@
     load_glu = pltpu.make_async_copy(glu_in, glu, sems.at[rows // size])
     load_glu.start()
     peers = sums.shape[0]
-    n = small.shape[0] - 1
+    n = taps_count
     total = sums[0]
     for p in range(1, peers):
         total = total + sums[p]
@@ -290,17 +290,19 @@
             for k in range(lo, hi):
                 small[k : k + 1, lanes(h)] = jnp.sum(acc[k - lo], axis=0, keepdims=True)
         small[n : n + 1, lanes(h)] = jnp.sum(gain_sum[h], axis=0, keepdims=True)
-
-
-def pack_body(kept, received, small, other, out):
-    outs = kept.shape[1]
-    total = small[...] + other[...]
-    low, high = total[0:16].astype(BF16), total[16:32].astype(BF16)
+    top = sent.shape[0] - 8
+    for q in range(4):
+        sent[top:, 256 * q : 256 * q + 256] = small[8 * q : 8 * q + 8]
+
+
+def pack_body(kept, sent, received, out):
+    rows, outs = kept.shape
+    total = sent[rows:] + received[rows:]
+    small = jnp.concatenate([total[:, 0:512], total[:, 512:1024]], axis=0).astype(BF16)
     for p in range(out.shape[0]):
         at = slice(p * 16, (p + 1) * 16)
         out[p, :, 0:outs] = (kept[at] + received[at]).astype(BF16)
-        out[p, :, outs : outs + 256] = low
-        out[p, :, outs + 256 : outs + 512] = high
+        out[p, :, outs:] = small
 
 
 def relay_body(got, out, held):
@@ -325,8 +327,8 @@
         total = total + got[p]
     total = total * factor
     taps[0:8] = total[:, 0:256]
-    taps[16:24] = total[:, 256:512]
-    taps[8:16] = total[:, 512:768]
+    taps[8:16] = total[:, 256:512]
+    taps[16:24] = total[:, 512:768]
     taps[24:31] = total[0:7, 768:1024]
     gain[...] = total[7:8, 768:1024]
     for i in range(2):
@@ -413,7 +415,7 @@
         act[at] = lax.dot_general(out_grad[at], weight[...], NT, preferred_element_type=F32)
 
 
-def proj_body(me, activ_in, grad_in, kept_out, sent_out, activ, out_grad, kept, sent, sems):
+def proj_body(me, activ_in, grad_in, kept_out, sent, activ, out_grad, kept, sems):
     chunks = 4
     outs = out_grad.shape[1]
     size = outs // chunks
@@ -440,11 +442,9 @@
         at = pl.ds(c * size, size)
         got = jnp.dot(placed, out_grad[:, at], preferred_element_type=F32)
         kept[:, at] = got[:half]
-        sent[:, at] = got[half:]
-        stores.append(pltpu.make_async_copy(sent.at[:, at], sent_out.at[:, at], sems.at[c]))
+        sent[0:half, at] = got[half:]
         stores.append(pltpu.make_async_copy(kept.at[:, at], kept_out.at[:, at], sems.at[chunks + 1 + c]))
-        stores[2 * c].start()
-        stores[2 * c + 1].start()
+        stores[c].start()
     for store in stores:
         store.wait()
 
@@ -512,28 +512,27 @@
     )
     sums = over_tp(sums)
     share = ((width // 2, outs), F32)
+    joint = ((width // 2 + 8, outs), F32, "near")
     kept, sent = kernel(
         proj_body,
-        [(*share, "far")] * 2,
+        [(*share, "far"), joint],
         (lax.axis_index("core")[None], far(activ), far(out_grad)),
         ins=[SMEM, HBM, HBM],
-        out_specs=[HBM] * 2,
-        scratch=[tall, ((rows, outs), BF16), share, share, dma((9,))],
+        out_specs=[HBM, VMEM],
+        scratch=[tall, ((rows, outs), BF16), share, dma((9,))],
     )
     sums, sent, kept = lax.optimization_barrier((sums, sent, kept))
+    grad, sent = kernel(
+        lambda *refs: taps_body(n, *refs),
+        [wide(rows), joint],
+        (far(xhat), far(saved), near(sent), near(sums), near(scaled), near(gain_sum)),
+        ins=[HBM] * 2,
+        aliases={2: 1},
+        scratch=[*spreading, wide(rows)[:2], wide(rows + PAD)[:2], ((32, width), F32), dma((5,))],
+    )
     received = swapped(sent)
-    grad, small = kernel(
-        taps_body,
-        [wide(rows), ((n + 1, width), F32, "near")],
-        (far(xhat), far(saved), near(sums), near(scaled), near(gain_sum)),
-        ins=[HBM] * 2,
-        scratch=[*spreading, wide(rows)[:2], wide(rows + PAD)[:2], dma((5,))],
-    )
-    other = swapped(small)
     (first,) = kernel(
-        pack_body,
-        [((8, 16, outs + 512), BF16, "any")],
-        (near(kept), near(received), near(small), near(other)),
+        pack_body, [((8, 16, outs + 512), BF16, "any")], (near(kept), near(sent), near(received))
     )
     first = lax.all_to_all(first, "z", 0, 0, tiled=True)
     after = shifted(grad[:, :PAD], -1)

time: 91.4 us -> 89.9 us (0.984)
  starting transfers between devices: 36.6 us -> 34.9 us
    ppermute x2 -> x1, starting transfers between devices: 8.46 us -> 6.55 us  [swapped(): return lax.ppermute(block, 'core', [(0, 1), (1, 0)])]
  transfers between devices with their start and end apart: 8 -> 7, of which waited for: 6 -> 6; matrix products, arithmetic and copies ran while one was open for 0% -> 0% of each run, Pallas kernels for 24% -> 19%
where the time goes in v5:
time: 89.9 us; the launch traced here: 89.2 us
  starting transfers between devices  34.9 us (39%)
  Pallas kernels  30.9 us (34%)
  waiting for transfers between devices  22.5 us (25%)
    pallas_call x12, Pallas kernels, kernel(): pl.pallas_call(body, out_shape=[shapes[where](s, d) for s, d, where in ou...  30.9 us
    all_to_all x1, starting transfers between devices, per_device(): first = lax.all_to_all(first, 'z', 0, 0, tiled=True)  9.95 us
    all_to_all x1, waiting for transfers between devices, per_device(): second = lax.all_to_all(second, 'y', 0, 0, tiled=True)  9.25 us
    all_to_all x1, waiting for transfers between devices, per_device(): first = lax.all_to_all(first, 'z', 0, 0, tiled=True)  8.82 us
    ppermute x2, starting transfers between devices, shifted(): return lax.ppermute(block, SP, route)  7.15 us
    ppermute x1, starting transfers between devices, swapped(): return lax.ppermute(block, 'core', [(0, 1), (1, 0)])  6.55 us
    all_to_all x2, starting transfers between devices, over_tp(): return lax.all_to_all(array, 'tp', 0, 0, tiled=True)  6.55 us
    all_to_all x1, starting transfers between devices, per_device(): second = lax.all_to_all(second, 'y', 0, 0, tiled=True)  4.74 us
  transfers between devices with their start and end apart: 7, of which 6 were waited for; matrix products, arithmetic and copies ran while one was open for 0% of the time, Pallas kernels for 19%

profile of v5, /device:TPU:1, one launch (start us, length us, event | category | flops | bytes accessed | tf_op | source)
XLA Modules:
  0.0 89.2 jit_solution(12982861647891278152)
XLA Ops:
  0.6 1.5 %shard_map.101 = (f32[2,1056,128]{2,1,0:T(8,128)S(1)}, f32[2,32,128]{2,1,0:T(8,128)S(1)}, f32[31,256]{1,0:T(8,128)S(1)}) custom-call(bf16[1024,256]{1,0:T(8,128)(2,1)} %value_in.5, bf16[1024,256]{1,0:T(8,128)(2,1)} %gate_in.5, f32[31,256]{1,0:T(8,128)} %taps.3), custom_call_target="tpu_custom_call" | custom-call | tf_op jit(solution)/shard_map/pallas_call | solution.py:46
  2.1 4.6 %collective-permute-start = (f32[2,32,128]{2,1,0:T(8,128)S(1)}, f32[2,32,128]{2,1,0:T(8,128)S(1)}, u32[]{:S(2)}, u32[]{:S(2)}) collective-permute-start(f32[2,32,128]{2,1,0:T(8,128)S(1)} %get-tuple-element.45), channel_id=1, source_target_pairs={{0,4},{4,8},{8,12},{12,16},{16,20},{20,24},{24,28},{28,32},{32,36}... | collective-permute-start | bytes 98312 | tf_op jit(solution)/shard_map/ppermute | solution.py:22
  6.7 3.0 %shard_map.102 = (f32[2,1024,128]{2,1,0:T(8,128)S(1)}, f32[8,1024]{1,0:T(8,128)S(1)}, f32[2,1056,128]{2,1,0:T(8,128)}) custom-call(f32[2,1056,128]{2,1,0:T(8,128)S(1)} %get-tuple-element.42.glu.glu_in, f32[31,256]{1,0:T(8,128)S(1)} %get-tuple-element.43.taps), custom_call_target="tpu_custom_call" | custom-call | tf_op jit(solution)/shard_map/pallas_call | solution.py:46
  9.7 1.2 %collective-permute-done.edge = f32[2,32,128]{2,1,0:T(8,128)S(1)} collective-permute-done((f32[2,32,128]{2,1,0:T(8,128)S(1)}, f32[2,32,128]{2,1,0:T(8,128)S(1)}, u32[]{:S(2)}, u32[]{:S(2)}) %collective-permute-start) | collective-permute-done | bytes 32800 | tf_op jit(solution)/shard_map/ppermute | solution.py:22
  10.9 1.6 %shard_map.103 = (f32[2,1056,128]{2,1,0:T(8,128)}, f32[2,1056,128]{2,1,0:T(8,128)S(1)}, f32[2,1024,128]{2,1,0:T(8,128)S(1)}, f32[4,2,1024]{2,1,0:T(2,128)}) custom-call(f32[2,1056,128]{2,1,0:T(8,128)} %get-tuple-element.44.saved_in, f32[2,32,128]{2,1,0:T(8,128)S(1)} %collective-permute-done.edge, ...), custom_call_target="tpu_custom_call", output_to_operand_aliasing={{0}: (0, {}), {1}: (2, {}), {2}: (4, {})} | custom-call | tf_op jit(solution)/shard_map/pallas_call | solution.py:46
  12.6 3.3 %all-to-all-start = ((f32[4,2,1024]{2,1,0:T(2,128)}), f32[4,2,1024]{2,1,0:T(2,128)S(1)}, u32[]{:S(2)}, u32[]{:S(2)}) async-start(f32[4,2,1024]{2,1,0:T(2,128)} %get-tuple-element.48), calls=%async_computation | async-start | bytes 65536 | tf_op jit(solution)/shard_map/all_to_all | solution.py:453
  15.8 0.0 copy-start.2
  15.9 3.1 %shard_map.104.act_grad = f32[1024,256]{1,0:T(8,128)S(1)} custom-call(bf16[1024,1024]{1,0:T(8,128)(2,1)} %grad_in.3, bf16[256,1024]{1,0:T(8,128)(2,1)} %weight_in.1), custom_call_target="tpu_custom_call" | custom-call | tf_op jit(solution)/shard_map/pallas_call | solution.py:46
  18.9 1.2 %all-to-all-done.stats = f32[4,2,1024]{2,1,0:T(2,128)S(1)} async-done(((f32[4,2,1024]{2,1,0:T(2,128)}), f32[4,2,1024]{2,1,0:T(2,128)S(1)}, u32[]{:S(2)}, u32[]{:S(2)}) %all-to-all-start) | async-done | bytes 32800 | tf_op jit(solution)/shard_map/all_to_all | solution.py:453
  20.1 0.0 copy-done.2
  20.1 3.7 %shard_map.105 = (bf16[1024,256]{1,0:T(8,128)(2,1)}, f32[2,1024,128]{2,1,0:T(8,128)}, f32[2,1024,128]{2,1,0:T(8,128)S(1)}, f32[4,2,1024]{2,1,0:T(2,128)}, f32[2,8,128]{2,1,0:T(8,128)S(1)}) custom-call(f32[4,2,1024]{2,1,0:T(2,128)S(1)} %all-to-all-done.stats, f32[2,1024,128]{2,1,0:T(8,128)S(1)} %get-tuple-element.50.conv, ...), custom_call_target="tpu_custom_call" | custom-call | tf_op jit(solution)/shard_map/pallas_call | solution.py:46
  23.8 3.3 %all-to-all-start.1 = ((f32[4,2,1024]{2,1,0:T(2,128)}), f32[4,2,1024]{2,1,0:T(2,128)S(1)}, u32[]{:S(2)}, u32[]{:S(2)}) async-start(f32[4,2,1024]{2,1,0:T(2,128)} %get-tuple-element.52), calls=%async_computation.1 | async-start | bytes 65536 | tf_op jit(solution)/shard_map/all_to_all | solution.py:453
  27.1 3.8 %shard_map.106 = (f32[128,1024]{1,0:T(8,128)}, f32[136,1024]{1,0:T(8,128)S(1)}) custom-call(s32[1]{0:T(128)} %bitcast.1.me, bf16[1024,256]{1,0:T(8,128)(2,1)} %get-tuple-element.53.activ_in, bf16[1024,1024]{1,0:T(8,128)(2,1)} %grad_in.3), custom_call_target="tpu_custom_call" | custom-call | tf_op jit(solution)/shard_map/pallas_call | solution.py:46
  30.9 0.5 all-to-all-done.1.refs_3_
  31.4 0.0 copy-start
  31.4 4.6 %shard_map.107 = (f32[2,1024,128]{2,1,0:T(8,128)S(1)}, f32[136,1024]{1,0:T(8,128)S(1)}) custom-call(f32[2,1024,128]{2,1,0:T(8,128)} %get-tuple-element.57.refs_0_, f32[2,1056,128]{2,1,0:T(8,128)} %get-tuple-element.58.refs_1_, f32[136,1024]{1,0:T(8,128)S(1)} %get-tuple-element.59.refs_2_, ...), custom_call_target="tpu_custom_call", output_to_operand_aliasing={{1}: (2, {})} | custom-call | tf_op jit(solution)/shard_map/pallas_call | solution.py:46
  36.0 0.0 copy-start.1
  36.0 6.6 %collective-permute-start.1 = (f32[136,1024]{1,0:T(8,128)S(1)}, f32[136,1024]{1,0:T(8,128)S(1)}, u32[]{:S(2)}, u32[]{:S(2)}) collective-permute-start(f32[136,1024]{1,0:T(8,128)S(1)} %get-tuple-element.63.sent), channel_id=1, source_target_pairs={{0,4},{4,0},{1,5},{5,1},{2,6},{6,2},{3,7},{7,3},{8,12},{12,8},{9,1... | collective-permute-start | bytes 1671176 | tf_op jit(solution)/shard_map/ppermute | solution.py:26
  42.5 1.6 %collective-permute-done.1.received = f32[136,1024]{1,0:T(8,128)S(1)} collective-permute-done((f32[136,1024]{1,0:T(8,128)S(1)}, f32[136,1024]{1,0:T(8,128)S(1)}, u32[]{:S(2)}, u32[]{:S(2)}) %collective-permute-start.1) | collective-permute-done | bytes 557088 | tf_op jit(solution)/shard_map/ppermute | solution.py:26
  44.1 0.0 copy-done
  44.1 0.8 shard_map.108
  44.9 9.9 %all-to-all-start.2 = ((bf16[8,16,1536]{2,1,0:T(8,128)(2,1)}), bf16[8,16,1536]{2,1,0:T(8,128)(2,1)S(1)}, u32[]{:S(2)}, u32[]{:S(2)}) async-start(bf16[8,16,1536]{2,1,0:T(8,128)(2,1)} %shard_map.108), calls=%async_computation.2 | async-start | bytes 786432 | tf_op jit(solution)/shard_map/all_to_all | solution.py:537
  54.9 2.6 %collective-permute-start.2 = (f32[2,32,128]{2,1,0:T(8,128)S(1)}, f32[2,32,128]{2,1,0:T(8,128)S(1)}, u32[]{:S(2)}, u32[]{:S(2)}) collective-permute-start(f32[2,32,128]{2,1,0:T(8,128)S(1)} %slice.3), channel_id=1, source_target_pairs={{4,0},{8,4},{12,8},{16,12},{20,16},{24,20},{28,24},{32,28},{36,32}... | collective-permute-start | bytes 98312 | tf_op jit(solution)/shard_map/ppermute | solution.py:22
  57.4 0.0 copy-done.1
  57.4 3.7 %shard_map.109 = (bf16[1024,256]{1,0:T(8,128)(2,1)}, bf16[1024,256]{1,0:T(8,128)(2,1)}) custom-call(bf16[1024,256]{1,0:T(8,128)(2,1)} %value_in.5, bf16[1024,256]{1,0:T(8,128)(2,1)} %gate_in.5, f32[2,1024,128]{2,1,0:T(8,128)S(1)} %get-tuple-element.64.grad, f32[31,256]{1,0:T(8,128)S(1)} %copy-done.1), custom_call_target="tpu_custom_call" | custom-call | tf_op jit(solution)/shard_map/pallas_call | solution.py:46
  61.2 0.0 collective-permute-done.2.after
  61.2 8.8 %all-to-all-done.2.got = bf16[8,16,1536]{2,1,0:T(8,128)(2,1)S(1)} async-done(((bf16[8,16,1536]{2,1,0:T(8,128)(2,1)}), bf16[8,16,1536]{2,1,0:T(8,128)(2,1)S(1)}, u32[]{:S(2)}, u32[]{:S(2)}) %all-to-all-start.2) | async-done | bytes 393248 | tf_op jit(solution)/shard_map/all_to_all | solution.py:537
  70.0 0.8 shard_map.110
  70.8 4.7 %all-to-all-start.3 = ((f32[8,8,1280]{2,1,0:T(8,128)}), f32[8,8,1280]{2,1,0:T(8,128)S(1)}, u32[]{:S(2)}, u32[]{:S(2)}) async-start(f32[8,8,1280]{2,1,0:T(8,128)} %shard_map.110), calls=%async_computation.3 | async-start | bytes 655360 | tf_op jit(solution)/shard_map/all_to_all | solution.py:552
  75.6 3.7 %shard_map.111 = (bf16[1024,256]{1,0:T(8,128)(2,1)}, bf16[1024,256]{1,0:T(8,128)(2,1)}) custom-call(bf16[1024,256]{1,0:T(8,128)(2,1)} %value_in.5, bf16[1024,256]{1,0:T(8,128)(2,1)} %gate_in.5, bf16[1024,256]{1,0:T(8,128)(2,1)} %get-tuple-element.68.value_part, ...), custom_call_target="tpu_custom_call", output_to_operand_aliasing={{0}: (2, {}), {1}: (3, {})} | custom-call | tf_op jit(solution)/shard_map/pallas_call | solution.py:46
  79.3 9.3 %all-to-all-done.3.refs_0_ = f32[8,8,1280]{2,1,0:T(8,128)S(1)} async-done(((f32[8,8,1280]{2,1,0:T(8,128)}), f32[8,8,1280]{2,1,0:T(8,128)S(1)}, u32[]{:S(2)}, u32[]{:S(2)}) %all-to-all-start.3) | async-done | bytes 327712 | tf_op jit(solution)/shard_map/all_to_all | solution.py:552
  88.5 0.6 shard_map.112
  (1 shorter events, 0.0 us)
Async XLA Ops:
  2.1 8.8 %collective-permute-start = (f32[2,32,128]{2,1,0:T(8,128)S(1)}, f32[2,32,128]{2,1,0:T(8,128)S(1)}, u32[]{:S(2)}, u32[]{:S(2)}) collective-permute-start(f32[2,32,128]{2,1,0:T(8,128)S(1)} %get-tuple-element.45), channel_id=1, source_target_pairs={{0,4},{4,8},{8,12},{12,16},{16,20},{20,24},{24,28},{28,32},{32,36}... | collective-permute-start | bytes 98312 | tf_op jit(solution)/shard_map/ppermute | solution.py:22
  12.6 7.5 %all-to-all-start = ((f32[4,2,1024]{2,1,0:T(2,128)}), f32[4,2,1024]{2,1,0:T(2,128)S(1)}, u32[]{:S(2)}, u32[]{:S(2)}) async-start(f32[4,2,1024]{2,1,0:T(2,128)} %get-tuple-element.48), calls=%async_computation | async-start | bytes 65536 | tf_op jit(solution)/shard_map/all_to_all | solution.py:453
  15.8 4.3 %copy-start.2 = (f32[256]{0:T(256)S(1)}, f32[256]{0:T(256)}, u32[]{:S(2)}) copy-start(f32[256]{0:T(256)} %param.9) | copy-start | bytes 3076
  23.8 7.5 %all-to-all-start.1 = ((f32[4,2,1024]{2,1,0:T(2,128)}), f32[4,2,1024]{2,1,0:T(2,128)S(1)}, u32[]{:S(2)}, u32[]{:S(2)}) async-start(f32[4,2,1024]{2,1,0:T(2,128)} %get-tuple-element.52), calls=%async_computation.1 | async-start | bytes 65536 | tf_op jit(solution)/shard_map/all_to_all | solution.py:453
  31.4 12.7 %copy-start = (f32[128,1024]{1,0:T(8,128)S(1)}, f32[128,1024]{1,0:T(8,128)}, u32[]{:S(2)}) copy-start(f32[128,1024]{1,0:T(8,128)} %get-tuple-element.56.kept) | copy-start | bytes 1572868
  36.0 21.5 %copy-start.1 = (f32[31,256]{1,0:T(8,128)S(1)}, f32[31,256]{1,0:T(8,128)}, u32[]{:S(2)}) copy-start(f32[31,256]{1,0:T(8,128)} %taps.3) | copy-start | bytes 95236
  36.0 8.1 %collective-permute-start.1 = (f32[136,1024]{1,0:T(8,128)S(1)}, f32[136,1024]{1,0:T(8,128)S(1)}, u32[]{:S(2)}, u32[]{:S(2)}) collective-permute-start(f32[136,1024]{1,0:T(8,128)S(1)} %get-tuple-element.63.sent), channel_id=1, source_target_pairs={{0,4},{4,0},{1,5},{5,1},{2,6},{6,2},{3,7},{7,3},{8,12},{12,8},{9,1... | collective-permute-start | bytes 1671176 | tf_op jit(solution)/shard_map/ppermute | solution.py:26
  44.9 25.1 %all-to-all-start.2 = ((bf16[8,16,1536]{2,1,0:T(8,128)(2,1)}), bf16[8,16,1536]{2,1,0:T(8,128)(2,1)S(1)}, u32[]{:S(2)}, u32[]{:S(2)}) async-start(bf16[8,16,1536]{2,1,0:T(8,128)(2,1)} %shard_map.108), calls=%async_computation.2 | async-start | bytes 786432 | tf_op jit(solution)/shard_map/all_to_all | solution.py:537
  54.9 6.3 %collective-permute-start.2 = (f32[2,32,128]{2,1,0:T(8,128)S(1)}, f32[2,32,128]{2,1,0:T(8,128)S(1)}, u32[]{:S(2)}, u32[]{:S(2)}) collective-permute-start(f32[2,32,128]{2,1,0:T(8,128)S(1)} %slice.3), channel_id=1, source_target_pairs={{4,0},{8,4},{12,8},{16,12},{20,16},{24,20},{28,24},{32,28},{36,32}... | collective-permute-start | bytes 98312 | tf_op jit(solution)/shard_map/ppermute | solution.py:22
  70.8 17.7 %all-to-all-start.3 = ((f32[8,8,1280]{2,1,0:T(8,128)}), f32[8,8,1280]{2,1,0:T(8,128)S(1)}, u32[]{:S(2)}, u32[]{:S(2)}) async-start(f32[8,8,1280]{2,1,0:T(8,128)} %shard_map.110), calls=%async_computation.3 | async-start | bytes 655360 | tf_op jit(solution)/shard_map/all_to_all | solution.py:552

commit v6 on v5

--- a/solution.py
+++ b/solution.py
@@ -89,19 +89,26 @@
     load_taps.wait()
 
 
+def weighted(source, h, base, weights):
+    parts = [[None, None] for _ in range(4)]
+    for k, weight in enumerate(weights):
+        for u in range(4):
+            term = weight * source[h, pl.ds(base + k + u * 8, 8), :]
+            old = parts[u][k % 2]
+            parts[u][k % 2] = term if old is None else old + term
+    return [p[0] + p[1] for p in parts]
+
+
 def conv_rows(glu, taps, conv, start, count):
     n = taps.shape[0]
     for h in range(2):
         weights = [jnp.broadcast_to(taps[k : k + 1, lanes(h)], (8, LANES)) for k in range(n)]
 
         def step(i, carry, h=h, weights=weights):
+            r = start + i * 32
+            tiles = weighted(glu, h, r + PAD + 1 - n, weights)
             for u in range(4):
-                r = start + i * 32 + u * 8
-                parts = [None, None]
-                for k in range(n):
-                    term = weights[k] * glu[h, pl.ds(r + PAD + 1 - n + k, 8), :]
-                    parts[k % 2] = term if parts[k % 2] is None else parts[k % 2] + term
-                conv[h, pl.ds(pl.multiple_of(r, 8), 8), :] = parts[0] + parts[1]
+                conv[h, pl.ds(pl.multiple_of(r + u * 8, 8), 8), :] = tiles[u]
             return carry
 
         lax.fori_loop(0, count // 32, step, 0)
@@ -140,29 +147,21 @@
     lax.fori_loop(0, count // 256, step, 0)
 
 
-def conv_body(glu, taps, conv, stats, saved, sem):
+def conv_body(glu, taps, conv, stats):
     rows = conv.shape[1]
-    store = pltpu.make_async_copy(
-        glu.at[:, pl.ds(PAD, rows)], saved.at[:, pl.ds(PAD, rows)], sem
-    )
-    store.start()
-    conv_rows(glu, taps, conv, 256, rows - 256)
+    conv_rows(glu, taps, conv, PAD, rows - PAD)
     conv_stats(conv, stats, 256, rows - 256)
-    store.wait()
-
-
-def head_body(saved_in, edge, glu_in, taps, conv_in, stats_in, saved, glu, conv, sent, stats, sem):
-    store = pltpu.make_async_copy(edge, saved.at[:, pl.ds(0, PAD)], sem)
-    store.start()
+
+
+def head_body(edge, glu_in, taps, conv_in, stats_in, glu, conv, sent, stats):
     for h in range(2):
         glu[h, 0:PAD, :] = edge[h]
-    conv_rows(glu, taps, conv, 0, 256)
+    conv_rows(glu, taps, conv, 0, PAD)
     conv_stats(conv, stats, 0, 256)
     rows = conv.shape[1]
     for p in range(sent.shape[0]):
         sent[p, :, 0:256] = stats[0:2]
         sent[p, :, 256:rows] = stats_in[0:2, 256:rows]
-    store.wait()
 
 
 def spread(rows, stack, columns):
@@ -182,8 +181,7 @@
 
 
 def norm_body(
-    stats, conv, act_grad, gain, activ_out, xhat_out, scaled, sums, gain_sum,
-    rows_in, stack, columns, activ, xhats, sems,
+    stats, conv, act_grad, gain, activ, xhats, scaled, sums, gain_sum, rows_in, stack, columns
 ):
     peers = stats.shape[0]
     rows = conv.shape[1]
@@ -198,13 +196,6 @@
     for h in range(2):
         gain_sum[h] = jnp.zeros((8, LANES), F32)
     size = 256
-
-    def store(i):
-        at = pl.ds(pl.multiple_of(i * size, size), size)
-        return (
-            pltpu.make_async_copy(activ.at[at], activ_out.at[at], sems.at[0, i]),
-            pltpu.make_async_copy(xhats.at[:, at], xhat_out.at[:, at], sems.at[1, i]),
-        )
 
     def block(i, carry):
         def step(j, carry):
@@ -224,8 +215,6 @@
             return carry
 
         lax.fori_loop(0, size // 32, step, 0)
-        for copy in store(i):
-            copy.start()
         at = pl.ds(pl.multiple_of(i * size, size), size)
         pairs = []
         for h in range(2):
@@ -237,52 +226,37 @@
         return carry
 
     lax.fori_loop(0, rows // size, block, 0)
-    for i in range(rows // size):
-        for copy in store(i):
-            copy.wait()
 
 
 def taps_body(
-    taps_count, xhat_in, glu_in, sent_in, sums, scaled, gain_sum, grad, sent,
-    rows_in, stack, columns, xhat, glu, small, sems,
+    n, sent_in, sums, scaled, xhat, glu, gain_sum, grad, sent, rows_in, stack, columns, small
 ):
     rows = grad.shape[1]
-    size = 256
-    loads = []
-    for i in range(rows // size):
-        at = pl.ds(i * size, size)
-        loads.append(pltpu.make_async_copy(xhat_in.at[:, at], xhat.at[:, at], sems.at[i]))
-        loads[i].start()
-    load_glu = pltpu.make_async_copy(glu_in, glu, sems.at[rows // size])
-    load_glu.start()
     peers = sums.shape[0]
-    n = taps_count
     total = sums[0]
     for p in range(1, peers):
         total = total + sums[p]
     rows_in[...] = total * (1.0 / (2 * LANES * peers))
     spread(rows_in, stack, columns)
-    for i in range(rows // size):
-        loads[i].wait()
-
-        def step(j, carry, i=i):
-            at = pl.ds(pl.multiple_of(i * size + j * 64, 64), 64)
-            for h in range(2):
-                grad[h, at, :] = scaled[h, at, :] - columns[0, at] - xhat[h, at, :] * columns[1, at]
-            return carry
-
-        lax.fori_loop(0, size // 64, step, 0)
-    load_glu.wait()
+
+    def step(j, carry):
+        at = pl.ds(pl.multiple_of(j * 64, 64), 64)
+        for h in range(2):
+            grad[h, at, :] = scaled[h, at, :] - columns[0, at] - xhat[h, at, :] * columns[1, at]
+        return carry
+
+    lax.fori_loop(0, rows // 64, step, 0)
     for h in range(2):
         for lo, hi in ((0, 16), (16, n)):
 
             def tile(i, acc, h=h, lo=lo, hi=hi):
                 acc = list(acc)
+                r = pl.multiple_of(i * 32, 32)
+                c = [grad[h, pl.ds(r + u * 8, 8), :] for u in range(4)]
                 for u in range(4):
-                    r = pl.multiple_of(i * 32 + u * 8, 8)
-                    c = grad[h, pl.ds(r, 8), :]
                     for k in range(lo, hi):
-                        acc[k - lo] = acc[k - lo] + c * glu[h, pl.ds(r + PAD + 1 - n + k, 8), :]
+                        base = r + PAD + 1 - n + k
+                        acc[k - lo] = acc[k - lo] + c[u] * glu[h, pl.ds(base + u * 8, 8), :]
                 return tuple(acc)
 
             zero = tuple(jnp.zeros((8, LANES), F32) for _ in range(lo, hi))
@@ -349,14 +323,7 @@
         weights = [jnp.broadcast_to(taps[k : k + 1, lanes(h)], (8, LANES)) for k in range(n)]
 
         def step(i, carry, h=h, weights=weights):
-            tiles = []
-            for u in range(4):
-                r = offset + i * 32 + u * 8
-                parts = [None, None]
-                for k in range(n):
-                    term = weights[k] * source[h, pl.ds(r + n - 1 - k, 8), :]
-                    parts[k % 2] = term if parts[k % 2] is None else parts[k % 2] + term
-                tiles.append(parts[0] + parts[1])
+            tiles = weighted(source, h, offset + i * 32, weights[::-1])
             at = pl.ds(pl.multiple_of(first + i * 32, 32), 32)
             sig = jax.nn.sigmoid(gate[at, lanes(h)].astype(F32))
             got = jnp.concatenate(tiles, axis=0) * sig
@@ -392,61 +359,29 @@
         ext[h, PAD : 2 * PAD, :] = after[h]
     for load in loads:
         load.wait()
-    glu_grad_rows(grad, rows - count, taps, value, gate, out_value, out_gate, 0, count - PAD)
+    if count > PAD:
+        glu_grad_rows(grad, rows - count, taps, value, gate, out_value, out_gate, 0, count - PAD)
     glu_grad_rows(ext, 0, taps, value, gate, out_value, out_gate, count - PAD, PAD)
     for copy in moves(((out_value, value_grad.at[at]), (out_gate, gate_grad.at[at])), sems):
         copy.wait()
 
 
-def act_body(grad_in, weight_in, act, out_grad, weight, sems):
-    rows = out_grad.shape[0]
-    size = rows // 4
-    load_weight = pltpu.make_async_copy(weight_in, weight, sems.at[4])
-    load_weight.start()
-    loads = []
-    for c in range(4):
-        at = pl.ds(c * size, size)
-        loads.append(pltpu.make_async_copy(grad_in.at[at], out_grad.at[at], sems.at[c]))
-        loads[c].start()
-    load_weight.wait()
-    for c in range(4):
-        loads[c].wait()
-        at = pl.ds(c * size, size)
-        act[at] = lax.dot_general(out_grad[at], weight[...], NT, preferred_element_type=F32)
-
-
-def proj_body(me, activ_in, grad_in, kept_out, sent, activ, out_grad, kept, sems):
-    chunks = 4
-    outs = out_grad.shape[1]
-    size = outs // chunks
+def act_body(out_grad, weight, act):
+    act[...] = lax.dot_general(out_grad[...], weight[...], NT, preferred_element_type=F32)
+
+
+def proj_body(me, activ, out_grad, kept, sent):
     width = activ.shape[1]
     half = width // 2
-    load_activ = pltpu.make_async_copy(activ_in, activ, sems.at[chunks])
-    load_activ.start()
-    loads = []
-    for c in range(chunks):
-        at = pl.ds(c * size, size)
-        loads.append(pltpu.make_async_copy(grad_in.at[:, at], out_grad.at[:, at], sems.at[c]))
-        loads[c].start()
     row = lax.broadcasted_iota(jnp.int32, (width, width), 0)
     col = lax.broadcasted_iota(jnp.int32, (width, width), 1)
     low = jnp.bitwise_and(row, half - 1)
     high = jnp.bitwise_xor(jnp.right_shift(row, 7), me[0])
     source = jnp.left_shift(jnp.right_shift(low, 1), 2) + 2 * high + jnp.bitwise_and(row, 1)
     order = (col == source).astype(F32).astype(BF16)
-    load_activ.wait()
     placed = lax.dot_general(order, activ[...], NT, preferred_element_type=F32).astype(BF16)
-    stores = []
-    for c in range(chunks):
-        loads[c].wait()
-        at = pl.ds(c * size, size)
-        got = jnp.dot(placed, out_grad[:, at], preferred_element_type=F32)
-        kept[:, at] = got[:half]
-        sent[0:half, at] = got[half:]
-        stores.append(pltpu.make_async_copy(kept.at[:, at], kept_out.at[:, at], sems.at[chunks + 1 + c]))
-        stores[c].start()
-    for store in stores:
-        store.wait()
+    kept[...] = jnp.dot(placed[:half], out_grad[...], preferred_element_type=F32)
+    sent[0:half] = jnp.dot(placed[half:], out_grad[...], preferred_element_type=F32)
 
 
 def over_tp(array):
@@ -463,10 +398,7 @@
     def wide(length):
         return ((2, length, LANES), F32, "near")
 
-    def kept_wide(length):
-        return ((2, length, LANES), F32, "far")
-
-    stat = ((peers, 2, rows), F32, "any")
+    stat = ((peers, 2, rows), F32, "near")
     dma = pltpu.SemaphoreType.DMA
     tall = ((rows, width), BF16)
     glu, edge, taps = kernel(
@@ -477,58 +409,43 @@
         scratch=[tall, tall, dma((2, 5))],
     )
     edge = shifted(edge, 1)
-    conv, stats, saved = kernel(
-        conv_body,
-        [wide(rows), ((8, rows), F32, "near"), kept_wide(rows + PAD)],
-        (near(glu), near(taps)),
-        out_specs=[VMEM, VMEM, HBM],
-        scratch=[dma],
-    )
-    saved, _, conv, stats = kernel(
+    conv, stats = kernel(conv_body, [wide(rows), ((8, rows), F32, "near")], (near(glu), near(taps)))
+    out_grad, stats = lax.optimization_barrier((near(out_grad), stats))
+    (act_grad,) = kernel(
+        act_body, [((rows, width), F32, "near")], (near(out_grad), near(proj_weight))
+    )
+    me = lax.axis_index("core")[None]
+    edge, act_grad, me = lax.optimization_barrier((edge, act_grad, me))
+    glu, conv, stats = kernel(
         head_body,
-        [kept_wide(rows + PAD), wide(rows + PAD), wide(rows), stat],
-        (far(saved), near(edge), near(glu), near(taps), near(conv), near(stats)),
-        ins=[HBM],
-        out_specs=[HBM, VMEM, VMEM, VMEM],
-        aliases={0: 0, 2: 1, 4: 2},
-        scratch=[((8, 256), F32), dma],
+        [wide(rows + PAD), wide(rows), stat],
+        (near(edge), near(glu), near(taps), near(conv), near(stats)),
+        aliases={1: 0, 3: 1},
+        scratch=[((8, 256), F32)],
     )
     stats = over_tp(stats)
-    (act_grad,) = kernel(
-        act_body,
-        [((rows, width), F32, "near")],
-        (far(out_grad), far(proj_weight)),
-        ins=[HBM] * 2,
-        scratch=[((rows, outs), BF16), ((width, outs), BF16), dma((5,))],
-    )
-    stats, act_grad = lax.optimization_barrier((stats, act_grad))
     spreading = [((2, rows), F32), ((LANES, LANES), F32), ((2, rows, LANES), F32)]
     activ, xhat, scaled, sums, gain_sum = kernel(
         norm_body,
-        [(*tall, "far"), kept_wide(rows), wide(rows), stat, wide(8)],
+        [(*tall, "near"), wide(rows), wide(rows), stat, wide(8)],
         (near(stats), near(conv), near(act_grad), channel_gain[None]),
-        out_specs=[HBM] * 2 + [VMEM] * 3,
-        scratch=[*spreading, tall, wide(rows)[:2], dma((2, 4))],
+        scratch=spreading,
     )
     sums = over_tp(sums)
-    share = ((width // 2, outs), F32)
+    sums, activ = lax.optimization_barrier((sums, activ))
     joint = ((width // 2 + 8, outs), F32, "near")
     kept, sent = kernel(
         proj_body,
-        [(*share, "far"), joint],
-        (lax.axis_index("core")[None], far(activ), far(out_grad)),
-        ins=[SMEM, HBM, HBM],
-        out_specs=[HBM, VMEM],
-        scratch=[tall, ((rows, outs), BF16), share, dma((9,))],
-    )
-    sums, sent, kept = lax.optimization_barrier((sums, sent, kept))
+        [((width // 2, outs), F32, "near"), joint],
+        (me, near(activ), near(out_grad)),
+        ins=[SMEM],
+    )
     grad, sent = kernel(
         lambda *refs: taps_body(n, *refs),
         [wide(rows), joint],
-        (far(xhat), far(saved), near(sent), near(sums), near(scaled), near(gain_sum)),
-        ins=[HBM] * 2,
-        aliases={2: 1},
-        scratch=[*spreading, wide(rows)[:2], wide(rows + PAD)[:2], ((32, width), F32), dma((5,))],
+        (near(sent), near(sums), near(scaled), near(xhat), near(glu), near(gain_sum)),
+        aliases={0: 1},
+        scratch=[*spreading, ((32, width), F32)],
     )
     received = swapped(sent)
     (first,) = kernel(
@@ -536,20 +453,19 @@
     )
     first = lax.all_to_all(first, "z", 0, 0, tiled=True)
     after = shifted(grad[:, :PAD], -1)
-    gates = [((rows // 2, width), BF16)] * 4
+
+    def gates(length):
+        return [((length, width), BF16)] * 4
+
     value_grad, gate_grad = kernel(
         glu_head_body,
         [(*tall, "far")] * 2,
         (far(glu_value), far(glu_gate), near(grad), conv_taps),
         ins=[HBM] * 2,
         out_specs=[HBM] * 2,
-        scratch=[*gates, dma((2,))],
-    )
-    first, after, value_grad, gate_grad = lax.optimization_barrier((first, after, value_grad, gate_grad))
-    (second,) = kernel(
-        relay_body, [((8, 8, 1280), F32, "any")], (near(first),), scratch=[((16, outs), F32)]
-    )
-    second = lax.all_to_all(second, "y", 0, 0, tiled=True)
+        scratch=[*gates(rows - PAD), dma((2,))],
+    )
+    after, value_grad, gate_grad = lax.optimization_barrier((after, value_grad, gate_grad))
     value_grad, gate_grad = kernel(
         glu_tail_body,
         [(*tall, "far")] * 2,
@@ -560,9 +476,13 @@
         ins=[HBM] * 4,
         out_specs=[HBM] * 2,
         aliases={2: 0, 3: 1},
-        scratch=[*gates, ((2, 2 * PAD, LANES), F32), dma((2,))],
-    )
-    second, value_grad, gate_grad = lax.optimization_barrier((second, value_grad, gate_grad))
+        scratch=[*gates(PAD), ((2, 2 * PAD, LANES), F32), dma((2,))],
+    )
+    first, value_grad, gate_grad = lax.optimization_barrier((first, value_grad, gate_grad))
+    (second,) = kernel(
+        relay_body, [((8, 8, 1280), F32, "near")], (near(first),), scratch=[((16, outs), F32)]
+    )
+    second = lax.all_to_all(second, "y", 0, 0, tiled=True)
     proj_grad, taps_grad, gain_grad = kernel(
         lambda *refs: final_body(factor, *refs),
         [((2, outs), F32, "any"), ((n, width), F32, "any"), ((1, width), F32, "any")],

time: 89.9 us -> 86.9 us (0.967)
  blocking collectives: 0 us -> 33.9 us
  waiting for transfers between devices: 22.5 us -> 7.56 us
  starting transfers between devices: 34.9 us -> 20.7 us
  Pallas kernels: 30.9 us -> 20.9 us
  local copies, waits for them, and re-layouts: 0.02 us -> 2.53 us
    all_to_all x0 -> x3, blocking collectives: none -> 33.9 us  [the longest x1 19.1 us: per_device(): second = lax.all_to_all(second, 'y', 0, 0, tiled=True)]
    all_to_all x3 -> x0, starting transfers between devices: 11.3 us -> none  [the longest x2 6.55 us: over_tp(): return lax.all_to_all(array, 'tp', 0, 0, tiled=True)]
    all_to_all x3 -> x0, waiting for transfers between devices: 10.9 us -> none  [the longest x1 9.25 us: per_device(): second = lax.all_to_all(second, 'y', 0, 0, tiled=True)]
    pallas_call x12, Pallas kernels: 30.9 us -> 20.9 us  [kernel(): pl.pallas_call(body, out_shape=[shapes[where](s, d) for s, d, where in ou...]
    all_to_all x1, waiting for transfers between devices: 8.82 us -> 5.99 us  [per_device(): first = lax.all_to_all(first, 'z', 0, 0, tiled=True)]
    all_to_all x1, starting transfers between devices: 9.95 us -> 7.23 us  [per_device(): first = lax.all_to_all(first, 'z', 0, 0, tiled=True)]
    unnamed x6 -> x12, local copies, waits for them, and re-layouts: 0.02 us -> 2.52 us
    ppermute x2, waiting for transfers between devices: 1.22 us -> 0.01 us  [shifted(): return lax.ppermute(block, SP, route)]
  transfers between devices with their start and end apart: 7 -> 4, of which waited for: 6 -> 2; matrix products, arithmetic and copies ran while one was open for 0% -> 0% of each run, Pallas kernels for 19% -> 12%
where the time goes in v6:
time: 86.9 us; the launch traced here: 86.3 us
  blocking collectives  33.9 us (39%)
  Pallas kernels  20.9 us (24%)
  starting transfers between devices  20.7 us (24%)
  waiting for transfers between devices  7.56 us (9%)
  local copies, waits for them, and re-layouts  2.53 us (3%)
    pallas_call x12, Pallas kernels, kernel(): pl.pallas_call(body, out_shape=[shapes[where](s, d) for s, d, where in ou...  20.9 us
    all_to_all x1, blocking collectives, per_device(): second = lax.all_to_all(second, 'y', 0, 0, tiled=True)  19.1 us
    all_to_all x2, blocking collectives, over_tp(): return lax.all_to_all(array, 'tp', 0, 0, tiled=True)  14.8 us
    all_to_all x1, starting transfers between devices, per_device(): first = lax.all_to_all(first, 'z', 0, 0, tiled=True)  7.23 us
    ppermute x2, starting transfers between devices, shifted(): return lax.ppermute(block, SP, route)  7.15 us
    ppermute x1, starting transfers between devices, swapped(): return lax.ppermute(block, 'core', [(0, 1), (1, 0)])  6.29 us
    all_to_all x1, waiting for transfers between devices, per_device(): first = lax.all_to_all(first, 'z', 0, 0, tiled=True)  5.99 us
    unnamed x12, local copies, waits for them, and re-layouts  2.52 us
  transfers between devices with their start and end apart: 4, of which 2 were waited for; matrix products, arithmetic and copies ran while one was open for 0% of the time, Pallas kernels for 12%

profile of v6, /device:TPU:1, one launch (start us, length us, event | category | flops | bytes accessed | tf_op | source)
XLA Modules:
  0.0 86.3 jit_solution(6713786686041477996)
XLA Ops:
  0.6 0.0 copy-start
  0.6 1.6 %shard_map.101 = (f32[2,1056,128]{2,1,0:T(8,128)S(1)}, f32[2,32,128]{2,1,0:T(8,128)S(1)}, f32[31,256]{1,0:T(8,128)S(1)}) custom-call(bf16[1024,256]{1,0:T(8,128)(2,1)} %value_in.5, bf16[1024,256]{1,0:T(8,128)(2,1)} %gate_in.5, f32[31,256]{1,0:T(8,128)} %taps.3), custom_call_target="tpu_custom_call" | custom-call | tf_op jit(solution)/shard_map/pallas_call | solution.py:46
  2.2 4.6 %collective-permute-start = (f32[2,32,128]{2,1,0:T(8,128)S(1)}, f32[2,32,128]{2,1,0:T(8,128)S(1)}, u32[]{:S(2)}, u32[]{:S(2)}) collective-permute-start(f32[2,32,128]{2,1,0:T(8,128)S(1)} %get-tuple-element.42), channel_id=1, source_target_pairs={{0,4},{4,8},{8,12},{12,16},{16,20},{20,24},{24,28},{28,32},{32,36}... | collective-permute-start | bytes 98312 | tf_op jit(solution)/shard_map/ppermute | solution.py:22
  6.8 3.2 %shard_map.102 = (f32[2,1024,128]{2,1,0:T(8,128)S(1)}, f32[8,1024]{1,0:T(8,128)S(1)}) custom-call(f32[2,1056,128]{2,1,0:T(8,128)S(1)} %get-tuple-element.43.glu.glu_in, f32[31,256]{1,0:T(8,128)S(1)} %get-tuple-element.44.taps), custom_call_target="tpu_custom_call" | custom-call | tf_op jit(solution)/shard_map/pallas_call | solution.py:46
  10.0 1.0 %copy-done.1 = f32[2,1024,128]{2,1,0:T(8,128)} copy-done((f32[2,1024,128]{2,1,0:T(8,128)}, f32[2,1024,128]{2,1,0:T(8,128)S(1)}, u32[]{:S(2)}) %copy-start.1) | copy-done | bytes 1048600
  11.0 0.0 copy-done
  11.0 0.0 copy-start.3
  11.0 1.0 %copy-done.3 = bf16[256,1024]{1,0:T(8,128)(2,1)S(1)} copy-done((bf16[256,1024]{1,0:T(8,128)(2,1)S(1)}, bf16[256,1024]{1,0:T(8,128)(2,1)}, u32[]{:S(2)}) %copy-start.3) | copy-done | bytes 524312
  12.0 0.0 copy-start.2
  12.0 0.7 shard_map.103.act_grad
  12.8 0.0 collective-permute-done.edge
  12.8 0.5 copy-done.2
  13.3 0.3 shard_map.104
  13.6 8.1 %all_to_all.20.stats = f32[4,2,1024]{2,1,0:T(2,128)S(1)} all-to-all(f32[4,2,1024]{2,1,0:T(2,128)S(1)} %get-tuple-element.51), channel_id=1, replica_groups=mesh['z'=8,'y'=8,'core'=2,'tp'=4] {'tp'}, dimensions={0} | all-to-all | bytes 65536 | tf_op jit(solution)/shard_map/all_to_all | solution.py:388
  21.7 0.0 copy-done.5
  21.7 2.5 %shard_map.105 = (bf16[1024,256]{1,0:T(8,128)(2,1)S(1)}, f32[2,1024,128]{2,1,0:T(8,128)S(1)}, f32[2,1024,128]{2,1,0:T(8,128)S(1)}, f32[4,2,1024]{2,1,0:T(2,128)S(1)}, f32[2,8,128]{2,1,0:T(8,128)S(1)}) custom-call(f32[4,2,1024]{2,1,0:T(2,128)S(1)} %all_to_all.20.stats, f32[2,1024,128]{2,1,0:T(8,128)S(1)} %get-tuple-element.52.conv, ...), custom_call_target="tpu_custom_call" | custom-call | tf_op jit(solution)/shard_map/pallas_call | solution.py:46
  24.2 6.7 %all_to_all.21.refs_1_ = f32[4,2,1024]{2,1,0:T(2,128)S(1)} all-to-all(f32[4,2,1024]{2,1,0:T(2,128)S(1)} %get-tuple-element.54), channel_id=1, replica_groups=mesh['z'=8,'y'=8,'core'=2,'tp'=4] {'tp'}, dimensions={0} | all-to-all | bytes 65536 | tf_op jit(solution)/shard_map/all_to_all | solution.py:388
  30.9 0.9 %shard_map.106 = (f32[128,1024]{1,0:T(8,128)S(1)}, f32[136,1024]{1,0:T(8,128)S(1)}) custom-call(s32[1]{0:T(128)} %bitcast.me, bf16[1024,256]{1,0:T(8,128)(2,1)S(1)} %get-tuple-element.56.activ, bf16[1024,1024]{1,0:T(8,128)(2,1)S(1)} %copy-done), custom_call_target="tpu_custom_call" | custom-call | tf_op jit(solution)/shard_map/pallas_call | solution.py:46
  31.8 3.7 %shard_map.107 = (f32[2,1024,128]{2,1,0:T(8,128)S(1)}, f32[136,1024]{1,0:T(8,128)S(1)}) custom-call(f32[136,1024]{1,0:T(8,128)S(1)} %get-tuple-element.58.refs_0_, f32[4,2,1024]{2,1,0:T(2,128)S(1)} %all_to_all.21.refs_1_, f32[2,1024,128]{2,1,0:T(8,128)S(1)} %get-tuple-element.60.refs_2_, ...), custom_call_target="tpu_custom_call", output_to_operand_aliasing={{1}: (0, {})} | custom-call | tf_op jit(solution)/shard_map/pallas_call | solution.py:46
  35.5 6.3 %collective-permute-start.1 = (f32[136,1024]{1,0:T(8,128)S(1)}, f32[136,1024]{1,0:T(8,128)S(1)}, u32[]{:S(2)}, u32[]{:S(2)}) collective-permute-start(f32[136,1024]{1,0:T(8,128)S(1)} %get-tuple-element.64.sent), channel_id=1, source_target_pairs={{0,4},{4,0},{1,5},{5,1},{2,6},{6,2},{3,7},{7,3},{8,12},{12,8},{9,1... | collective-permute-start | bytes 1671176 | tf_op jit(solution)/shard_map/ppermute | solution.py:26
  41.8 1.6 %collective-permute-done.1.received = f32[136,1024]{1,0:T(8,128)S(1)} collective-permute-done((f32[136,1024]{1,0:T(8,128)S(1)}, f32[136,1024]{1,0:T(8,128)S(1)}, u32[]{:S(2)}, u32[]{:S(2)}) %collective-permute-start.1) | collective-permute-done | bytes 557088 | tf_op jit(solution)/shard_map/ppermute | solution.py:26
  43.3 0.8 shard_map.108
  44.1 7.2 %all-to-all-start.2 = ((bf16[8,16,1536]{2,1,0:T(8,128)(2,1)}), bf16[8,16,1536]{2,1,0:T(8,128)(2,1)S(1)}, u32[]{:S(2)}, u32[]{:S(2)}) async-start(bf16[8,16,1536]{2,1,0:T(8,128)(2,1)} %shard_map.108), calls=%async_computation.2 | async-start | bytes 786432 | tf_op jit(solution)/shard_map/all_to_all | solution.py:454
  51.4 2.6 %collective-permute-start.2 = (f32[2,32,128]{2,1,0:T(8,128)S(1)}, f32[2,32,128]{2,1,0:T(8,128)S(1)}, u32[]{:S(2)}, u32[]{:S(2)}) collective-permute-start(f32[2,32,128]{2,1,0:T(8,128)S(1)} %slice.3), channel_id=1, source_target_pairs={{4,0},{8,4},{12,8},{16,12},{20,16},{24,20},{28,24},{32,28},{36,32}... | collective-permute-start | bytes 98312 | tf_op jit(solution)/shard_map/ppermute | solution.py:22
  53.9 0.0 copy-done.4
  53.9 5.1 %shard_map.109 = (bf16[1024,256]{1,0:T(8,128)(2,1)}, bf16[1024,256]{1,0:T(8,128)(2,1)}) custom-call(bf16[1024,256]{1,0:T(8,128)(2,1)} %value_in.5, bf16[1024,256]{1,0:T(8,128)(2,1)} %gate_in.5, f32[2,1024,128]{2,1,0:T(8,128)S(1)} %get-tuple-element.65.grad, f32[31,256]{1,0:T(8,128)S(1)} %copy-done.4), custom_call_target="tpu_custom_call" | custom-call | tf_op jit(solution)/shard_map/pallas_call | solution.py:46
  59.0 0.0 collective-permute-done.2.after
  59.1 1.4 %shard_map.110 = (bf16[1024,256]{1,0:T(8,128)(2,1)}, bf16[1024,256]{1,0:T(8,128)(2,1)}) custom-call(bf16[1024,256]{1,0:T(8,128)(2,1)} %value_in.5, bf16[1024,256]{1,0:T(8,128)(2,1)} %gate_in.5, bf16[1024,256]{1,0:T(8,128)(2,1)} %get-tuple-element.68.value_part, ...), custom_call_target="tpu_custom_call", output_to_operand_aliasing={{0}: (2, {}), {1}: (3, {})} | custom-call | tf_op jit(solution)/shard_map/pallas_call | solution.py:46
  60.5 6.0 %all-to-all-done.2.got = bf16[8,16,1536]{2,1,0:T(8,128)(2,1)S(1)} async-done(((bf16[8,16,1536]{2,1,0:T(8,128)(2,1)}), bf16[8,16,1536]{2,1,0:T(8,128)(2,1)S(1)}, u32[]{:S(2)}, u32[]{:S(2)}) %all-to-all-start.2) | async-done | bytes 393248 | tf_op jit(solution)/shard_map/all_to_all | solution.py:454
  66.5 0.1 shard_map.111
  66.6 19.1 %all_to_all.22.refs_0_ = f32[8,8,1280]{2,1,0:T(8,128)S(1)} all-to-all(f32[8,8,1280]{2,1,0:T(8,128)S(1)} %shard_map.111), channel_id=1, replica_groups=mesh['z'=8,'y'=8,'core'=2,'tp'=4] {'y'}, dimensions={0} | all-to-all | bytes 655360 | tf_op jit(solution)/shard_map/all_to_all | solution.py:485
  85.7 0.6 shard_map.112
  (4 shorter events, 0.0 us)
Async XLA Ops:
  0.6 10.4 %copy-start = (bf16[1024,1024]{1,0:T(8,128)(2,1)S(1)}, bf16[1024,1024]{1,0:T(8,128)(2,1)}, u32[]{:S(2)}) copy-start(bf16[1024,1024]{1,0:T(8,128)(2,1)} %out_grad.1) | copy-start | bytes 6291460
  2.2 10.5 %collective-permute-start = (f32[2,32,128]{2,1,0:T(8,128)S(1)}, f32[2,32,128]{2,1,0:T(8,128)S(1)}, u32[]{:S(2)}, u32[]{:S(2)}) collective-permute-start(f32[2,32,128]{2,1,0:T(8,128)S(1)} %get-tuple-element.42), channel_id=1, source_target_pairs={{0,4},{4,8},{8,12},{12,16},{16,20},{20,24},{24,28},{28,32},{32,36}... | collective-permute-start | bytes 98312 | tf_op jit(solution)/shard_map/ppermute | solution.py:22
  10.0 1.0 %copy-start.1 = (f32[2,1024,128]{2,1,0:T(8,128)}, f32[2,1024,128]{2,1,0:T(8,128)S(1)}, u32[]{:S(2)}) copy-start(f32[2,1024,128]{2,1,0:T(8,128)S(1)} %get-tuple-element.49.conv_in) | copy-start | bytes 3145732
  11.0 1.0 %copy-start.3 = (bf16[256,1024]{1,0:T(8,128)(2,1)S(1)}, bf16[256,1024]{1,0:T(8,128)(2,1)}, u32[]{:S(2)}) copy-start(bf16[256,1024]{1,0:T(8,128)(2,1)} %weight.1) | copy-start | bytes 1572868
  12.0 1.2 %copy-start.2 = (f32[2,1024,128]{2,1,0:T(8,128)S(1)}, f32[2,1024,128]{2,1,0:T(8,128)}, u32[]{:S(2)}) copy-start(f32[2,1024,128]{2,1,0:T(8,128)} %copy-done.1) | copy-start | bytes 3145732
  13.3 8.4 %copy-start.5 = (f32[256]{0:T(256)S(1)}, f32[256]{0:T(256)}, u32[]{:S(2)}) copy-start(f32[256]{0:T(256)} %param.9) | copy-start | bytes 3076
  35.5 7.9 %collective-permute-start.1 = (f32[136,1024]{1,0:T(8,128)S(1)}, f32[136,1024]{1,0:T(8,128)S(1)}, u32[]{:S(2)}, u32[]{:S(2)}) collective-permute-start(f32[136,1024]{1,0:T(8,128)S(1)} %get-tuple-element.64.sent), channel_id=1, source_target_pairs={{0,4},{4,0},{1,5},{5,1},{2,6},{6,2},{3,7},{7,3},{8,12},{12,8},{9,1... | collective-permute-start | bytes 1671176 | tf_op jit(solution)/shard_map/ppermute | solution.py:26
  43.3 10.6 %copy-start.4 = (f32[31,256]{1,0:T(8,128)S(1)}, f32[31,256]{1,0:T(8,128)}, u32[]{:S(2)}) copy-start(f32[31,256]{1,0:T(8,128)} %taps.3) | copy-start | bytes 95236
  44.1 22.4 %all-to-all-start.2 = ((bf16[8,16,1536]{2,1,0:T(8,128)(2,1)}), bf16[8,16,1536]{2,1,0:T(8,128)(2,1)S(1)}, u32[]{:S(2)}, u32[]{:S(2)}) async-start(bf16[8,16,1536]{2,1,0:T(8,128)(2,1)} %shard_map.108), calls=%async_computation.2 | async-start | bytes 786432 | tf_op jit(solution)/shard_map/all_to_all | solution.py:454
  51.4 7.7 %collective-permute-start.2 = (f32[2,32,128]{2,1,0:T(8,128)S(1)}, f32[2,32,128]{2,1,0:T(8,128)S(1)}, u32[]{:S(2)}, u32[]{:S(2)}) collective-permute-start(f32[2,32,128]{2,1,0:T(8,128)S(1)} %slice.3), channel_id=1, source_target_pairs={{4,0},{8,4},{12,8},{16,12},{20,16},{24,20},{28,24},{32,28},{36,32}... | collective-permute-start | bytes 98312 | tf_op jit(solution)/shard_map/ppermute | solution.py:22

commit v7 on v6

--- a/solution.py
+++ b/solution.py
@@ -147,10 +147,13 @@
     lax.fori_loop(0, count // 256, step, 0)
 
 
-def conv_body(glu, taps, conv, stats):
+def conv_body(grad_in, weight_in, glu, taps, conv, stats, out_grad, weight, sems):
     rows = conv.shape[1]
+    loads = moves(((weight_in, weight), (grad_in, out_grad)), sems)
     conv_rows(glu, taps, conv, PAD, rows - PAD)
     conv_stats(conv, stats, 256, rows - 256)
+    for load in loads:
+        load.wait()
 
 
 def head_body(edge, glu_in, taps, conv_in, stats_in, glu, conv, sent, stats):
@@ -409,11 +412,19 @@
         scratch=[tall, tall, dma((2, 5))],
     )
     edge = shifted(edge, 1)
-    conv, stats = kernel(conv_body, [wide(rows), ((8, rows), F32, "near")], (near(glu), near(taps)))
-    out_grad, stats = lax.optimization_barrier((near(out_grad), stats))
-    (act_grad,) = kernel(
-        act_body, [((rows, width), F32, "near")], (near(out_grad), near(proj_weight))
-    )
+    conv, stats, out_grad, weight = kernel(
+        conv_body,
+        [
+            wide(rows),
+            ((8, rows), F32, "near"),
+            (out_grad.shape, BF16, "near"),
+            (proj_weight.shape, BF16, "near"),
+        ],
+        (far(out_grad), far(proj_weight), near(glu), near(taps)),
+        ins=[HBM] * 2,
+        scratch=[dma((2,))],
+    )
+    (act_grad,) = kernel(act_body, [((rows, width), F32, "near")], (near(out_grad), near(weight)))
     me = lax.axis_index("core")[None]
     edge, act_grad, me = lax.optimization_barrier((edge, act_grad, me))
     glu, conv, stats = kernel(
@@ -463,9 +474,13 @@
         (far(glu_value), far(glu_gate), near(grad), conv_taps),
         ins=[HBM] * 2,
         out_specs=[HBM] * 2,
-        scratch=[*gates(rows - PAD), dma((2,))],
-    )
-    after, value_grad, gate_grad = lax.optimization_barrier((after, value_grad, gate_grad))
+        scratch=[*gates(rows // 2), dma((2,))],
+    )
+    first, after, value_grad, gate_grad = lax.optimization_barrier((first, after, value_grad, gate_grad))
+    (second,) = kernel(
+        relay_body, [((8, 8, 1280), F32, "any")], (near(first),), scratch=[((16, outs), F32)]
+    )
+    second = lax.all_to_all(second, "y", 0, 0, tiled=True)
     value_grad, gate_grad = kernel(
         glu_tail_body,
         [(*tall, "far")] * 2,
@@ -476,13 +491,9 @@
         ins=[HBM] * 4,
         out_specs=[HBM] * 2,
         aliases={2: 0, 3: 1},
-        scratch=[*gates(PAD), ((2, 2 * PAD, LANES), F32), dma((2,))],
-    )
-    first, value_grad, gate_grad = lax.optimization_barrier((first, value_grad, gate_grad))
-    (second,) = kernel(
-        relay_body, [((8, 8, 1280), F32, "near")], (near(first),), scratch=[((16, outs), F32)]
-    )
-    second = lax.all_to_all(second, "y", 0, 0, tiled=True)
+        scratch=[*gates(rows // 2), ((2, 2 * PAD, LANES), F32), dma((2,))],
+    )
+    second, value_grad, gate_grad = lax.optimization_barrier((second, value_grad, gate_grad))
     proj_grad, taps_grad, gain_grad = kernel(
         lambda *refs: final_body(factor, *refs),
         [((2, outs), F32, "any"), ((n, width), F32, "any"), ((1, width), F32, "any")],

time: 86.9 us -> 86 us (0.990)
  blocking collectives: 33.9 us -> 14.6 us
  waiting for transfers between devices: 7.56 us -> 20.6 us
  starting transfers between devices: 20.7 us -> 27.9 us
  local copies, waits for them, and re-layouts: 2.53 us -> 0.02 us
    all_to_all x1 -> x0, blocking collectives: 19.1 us -> none  [per_device(): second = lax.all_to_all(second, 'y', 0, 0, tiled=True)]
    all_to_all x0 -> x1, waiting for transfers between devices: none -> 9.62 us  [per_device(): second = lax.all_to_all(second, 'y', 0, 0, tiled=True)]
    all_to_all x0 -> x1, starting transfers between devices: none -> 4.74 us  [per_device(): second = lax.all_to_all(second, 'y', 0, 0, tiled=True)]
    all_to_all x1, waiting for transfers between devices: 5.99 us -> 9.19 us  [per_device(): first = lax.all_to_all(first, 'z', 0, 0, tiled=True)]
    unnamed x12 -> x4, local copies, waits for them, and re-layouts: 2.52 us -> 0.01 us
    all_to_all x1, starting transfers between devices: 7.23 us -> 9.67 us  [per_device(): first = lax.all_to_all(first, 'z', 0, 0, tiled=True)]
  transfers between devices with their start and end apart: 4 -> 5, of which waited for: 2 -> 4; matrix products, arithmetic and copies ran while one was open for 0% -> 0% of each run, Pallas kernels for 12% -> 12%
where the time goes in v7:
time: 86 us; the launch traced here: 85.5 us
  starting transfers between devices  27.9 us (32%)
  Pallas kernels  21.7 us (25%)
  waiting for transfers between devices  20.6 us (24%)
  blocking collectives  14.6 us (17%)
    pallas_call x12, Pallas kernels, kernel(): pl.pallas_call(body, out_shape=[shapes[where](s, d) for s, d, where in ou...  21.7 us
    all_to_all x2, blocking collectives, over_tp(): return lax.all_to_all(array, 'tp', 0, 0, tiled=True)  14.6 us
    all_to_all x1, starting transfers between devices, per_device(): first = lax.all_to_all(first, 'z', 0, 0, tiled=True)  9.67 us
    all_to_all x1, waiting for transfers between devices, per_device(): second = lax.all_to_all(second, 'y', 0, 0, tiled=True)  9.62 us
    all_to_all x1, waiting for transfers between devices, per_device(): first = lax.all_to_all(first, 'z', 0, 0, tiled=True)  9.19 us
    ppermute x2, starting transfers between devices, shifted(): return lax.ppermute(block, SP, route)  7.15 us
    ppermute x1, starting transfers between devices, swapped(): return lax.ppermute(block, 'core', [(0, 1), (1, 0)])  6.29 us
    all_to_all x1, starting transfers between devices, per_device(): second = lax.all_to_all(second, 'y', 0, 0, tiled=True)  4.74 us
  transfers between devices with their start and end apart: 5, of which 4 were waited for; matrix products, arithmetic and copies ran while one was open for 0% of the time, Pallas kernels for 12%

profile of v7, /device:TPU:1, one launch (start us, length us, event | category | flops | bytes accessed | tf_op | source)
XLA Modules:
  0.0 85.5 jit_solution(605073783171349081)
XLA Ops:
  0.6 1.5 %shard_map.101 = (f32[2,1056,128]{2,1,0:T(8,128)S(1)}, f32[2,32,128]{2,1,0:T(8,128)S(1)}, f32[31,256]{1,0:T(8,128)S(1)}) custom-call(bf16[1024,256]{1,0:T(8,128)(2,1)} %value_in.5, bf16[1024,256]{1,0:T(8,128)(2,1)} %gate_in.5, f32[31,256]{1,0:T(8,128)} %taps.3), custom_call_target="tpu_custom_call" | custom-call | tf_op jit(solution)/shard_map/pallas_call | solution.py:46
  2.1 4.6 %collective-permute-start = (f32[2,32,128]{2,1,0:T(8,128)S(1)}, f32[2,32,128]{2,1,0:T(8,128)S(1)}, u32[]{:S(2)}, u32[]{:S(2)}) collective-permute-start(f32[2,32,128]{2,1,0:T(8,128)S(1)} %get-tuple-element.43), channel_id=1, source_target_pairs={{0,4},{4,8},{8,12},{12,16},{16,20},{20,24},{24,28},{28,32},{32,36}... | collective-permute-start | bytes 98312 | tf_op jit(solution)/shard_map/ppermute | solution.py:22
  6.7 3.2 %shard_map.102 = (f32[2,1024,128]{2,1,0:T(8,128)S(1)}, f32[8,1024]{1,0:T(8,128)S(1)}, bf16[1024,1024]{1,0:T(8,128)(2,1)S(1)}, bf16[256,1024]{1,0:T(8,128)(2,1)S(1)}) custom-call(bf16[1024,1024]{1,0:T(8,128)(2,1)} %grad_in.1, bf16[256,1024]{1,0:T(8,128)(2,1)} %weight_in.1, f32[2,1056,128]{2,1,0:T(8,128)S(1)} %get-tuple-element.44.glu.glu_in, ...), custom_call_target="tpu_custom_call" | custom-call | tf_op jit(solution)/shard_map/pallas_call | solution.py:46
  9.9 0.0 copy-start.1
  9.9 0.7 shard_map.103.act_grad
  10.7 0.3 collective-permute-done.edge
  10.9 0.3 shard_map.104
  11.2 7.9 %all_to_all.20.stats = f32[4,2,1024]{2,1,0:T(2,128)S(1)} all-to-all(f32[4,2,1024]{2,1,0:T(2,128)S(1)} %get-tuple-element.52), channel_id=1, replica_groups=mesh['z'=8,'y'=8,'core'=2,'tp'=4] {'tp'}, dimensions={0} | all-to-all | bytes 65536 | tf_op jit(solution)/shard_map/all_to_all | solution.py:391
  19.1 0.0 copy-done.1
  19.1 2.5 %shard_map.105 = (bf16[1024,256]{1,0:T(8,128)(2,1)S(1)}, f32[2,1024,128]{2,1,0:T(8,128)S(1)}, f32[2,1024,128]{2,1,0:T(8,128)S(1)}, f32[4,2,1024]{2,1,0:T(2,128)S(1)}, f32[2,8,128]{2,1,0:T(8,128)S(1)}) custom-call(f32[4,2,1024]{2,1,0:T(2,128)S(1)} %all_to_all.20.stats, f32[2,1024,128]{2,1,0:T(8,128)S(1)} %get-tuple-element.53.conv, ...), custom_call_target="tpu_custom_call" | custom-call | tf_op jit(solution)/shard_map/pallas_call | solution.py:46
  21.6 6.7 %all_to_all.21.refs_1_ = f32[4,2,1024]{2,1,0:T(2,128)S(1)} all-to-all(f32[4,2,1024]{2,1,0:T(2,128)S(1)} %get-tuple-element.55), channel_id=1, replica_groups=mesh['z'=8,'y'=8,'core'=2,'tp'=4] {'tp'}, dimensions={0} | all-to-all | bytes 65536 | tf_op jit(solution)/shard_map/all_to_all | solution.py:391
  28.3 0.9 %shard_map.106 = (f32[128,1024]{1,0:T(8,128)S(1)}, f32[136,1024]{1,0:T(8,128)S(1)}) custom-call(s32[1]{0:T(128)} %bitcast.me, bf16[1024,256]{1,0:T(8,128)(2,1)S(1)} %get-tuple-element.57.activ, bf16[1024,1024]{1,0:T(8,128)(2,1)S(1)} %get-tuple-element.46.out_grad), custom_call_target="tpu_custom_call" | custom-call | tf_op jit(solution)/shard_map/pallas_call | solution.py:46
  29.2 3.7 %shard_map.107 = (f32[2,1024,128]{2,1,0:T(8,128)S(1)}, f32[136,1024]{1,0:T(8,128)S(1)}) custom-call(f32[136,1024]{1,0:T(8,128)S(1)} %get-tuple-element.59.refs_0_, f32[4,2,1024]{2,1,0:T(2,128)S(1)} %all_to_all.21.refs_1_, f32[2,1024,128]{2,1,0:T(8,128)S(1)} %get-tuple-element.61.refs_2_, ...), custom_call_target="tpu_custom_call", output_to_operand_aliasing={{1}: (0, {})} | custom-call | tf_op jit(solution)/shard_map/pallas_call | solution.py:46
  32.8 0.0 copy-start
  32.9 6.3 %collective-permute-start.1 = (f32[136,1024]{1,0:T(8,128)S(1)}, f32[136,1024]{1,0:T(8,128)S(1)}, u32[]{:S(2)}, u32[]{:S(2)}) collective-permute-start(f32[136,1024]{1,0:T(8,128)S(1)} %get-tuple-element.65.sent), channel_id=1, source_target_pairs={{0,4},{4,0},{1,5},{5,1},{2,6},{6,2},{3,7},{7,3},{8,12},{12,8},{9,1... | collective-permute-start | bytes 1671176 | tf_op jit(solution)/shard_map/ppermute | solution.py:26
  39.2 1.6 %collective-permute-done.1.received = f32[136,1024]{1,0:T(8,128)S(1)} collective-permute-done((f32[136,1024]{1,0:T(8,128)S(1)}, f32[136,1024]{1,0:T(8,128)S(1)}, u32[]{:S(2)}, u32[]{:S(2)}) %collective-permute-start.1) | collective-permute-done | bytes 557088 | tf_op jit(solution)/shard_map/ppermute | solution.py:26
  40.7 0.8 shard_map.108
  41.5 9.7 %all-to-all-start.2 = ((bf16[8,16,1536]{2,1,0:T(8,128)(2,1)}), bf16[8,16,1536]{2,1,0:T(8,128)(2,1)S(1)}, u32[]{:S(2)}, u32[]{:S(2)}) async-start(bf16[8,16,1536]{2,1,0:T(8,128)(2,1)} %shard_map.108), calls=%async_computation.2 | async-start | bytes 786432 | tf_op jit(solution)/shard_map/all_to_all | solution.py:465
  51.2 2.6 %collective-permute-start.2 = (f32[2,32,128]{2,1,0:T(8,128)S(1)}, f32[2,32,128]{2,1,0:T(8,128)S(1)}, u32[]{:S(2)}, u32[]{:S(2)}) collective-permute-start(f32[2,32,128]{2,1,0:T(8,128)S(1)} %slice.3), channel_id=1, source_target_pairs={{4,0},{8,4},{12,8},{16,12},{20,16},{24,20},{28,24},{32,28},{36,32}... | collective-permute-start | bytes 98312 | tf_op jit(solution)/shard_map/ppermute | solution.py:22
  53.8 0.0 copy-done
  53.8 3.4 %shard_map.109 = (bf16[1024,256]{1,0:T(8,128)(2,1)}, bf16[1024,256]{1,0:T(8,128)(2,1)}) custom-call(bf16[1024,256]{1,0:T(8,128)(2,1)} %value_in.5, bf16[1024,256]{1,0:T(8,128)(2,1)} %gate_in.5, f32[2,1024,128]{2,1,0:T(8,128)S(1)} %get-tuple-element.66.grad, f32[31,256]{1,0:T(8,128)S(1)} %copy-done), custom_call_target="tpu_custom_call" | custom-call | tf_op jit(solution)/shard_map/pallas_call | solution.py:46
  57.2 0.0 collective-permute-done.2.after
  57.2 9.2 %all-to-all-done.2.got = bf16[8,16,1536]{2,1,0:T(8,128)(2,1)S(1)} async-done(((bf16[8,16,1536]{2,1,0:T(8,128)(2,1)}), bf16[8,16,1536]{2,1,0:T(8,128)(2,1)S(1)}, u32[]{:S(2)}, u32[]{:S(2)}) %all-to-all-start.2) | async-done | bytes 393248 | tf_op jit(solution)/shard_map/all_to_all | solution.py:465
  66.3 0.8 shard_map.110
  67.2 4.7 %all-to-all-start.3 = ((f32[8,8,1280]{2,1,0:T(8,128)}), f32[8,8,1280]{2,1,0:T(8,128)S(1)}, u32[]{:S(2)}, u32[]{:S(2)}) async-start(f32[8,8,1280]{2,1,0:T(8,128)} %shard_map.110), calls=%async_computation.3 | async-start | bytes 655360 | tf_op jit(solution)/shard_map/all_to_all | solution.py:483
  71.9 3.3 %shard_map.111 = (bf16[1024,256]{1,0:T(8,128)(2,1)}, bf16[1024,256]{1,0:T(8,128)(2,1)}) custom-call(bf16[1024,256]{1,0:T(8,128)(2,1)} %value_in.5, bf16[1024,256]{1,0:T(8,128)(2,1)} %gate_in.5, bf16[1024,256]{1,0:T(8,128)(2,1)} %get-tuple-element.70.value_part, ...), custom_call_target="tpu_custom_call", output_to_operand_aliasing={{0}: (2, {}), {1}: (3, {})} | custom-call | tf_op jit(solution)/shard_map/pallas_call | solution.py:46
  75.3 9.6 %all-to-all-done.3.refs_0_ = f32[8,8,1280]{2,1,0:T(8,128)S(1)} async-done(((f32[8,8,1280]{2,1,0:T(8,128)}), f32[8,8,1280]{2,1,0:T(8,128)S(1)}, u32[]{:S(2)}, u32[]{:S(2)}) %all-to-all-start.3) | async-done | bytes 327712 | tf_op jit(solution)/shard_map/all_to_all | solution.py:483
  84.9 0.6 shard_map.112
  (1 shorter events, 0.0 us)
Async XLA Ops:
  2.1 8.8 %collective-permute-start = (f32[2,32,128]{2,1,0:T(8,128)S(1)}, f32[2,32,128]{2,1,0:T(8,128)S(1)}, u32[]{:S(2)}, u32[]{:S(2)}) collective-permute-start(f32[2,32,128]{2,1,0:T(8,128)S(1)} %get-tuple-element.43), channel_id=1, source_target_pairs={{0,4},{4,8},{8,12},{12,16},{16,20},{20,24},{24,28},{28,32},{32,36}... | collective-permute-start | bytes 98312 | tf_op jit(solution)/shard_map/ppermute | solution.py:22
  9.9 9.2 %copy-start.1 = (f32[256]{0:T(256)S(1)}, f32[256]{0:T(256)}, u32[]{:S(2)}) copy-start(f32[256]{0:T(256)} %param.9) | copy-start | bytes 3076
  32.8 20.9 %copy-start = (f32[31,256]{1,0:T(8,128)S(1)}, f32[31,256]{1,0:T(8,128)}, u32[]{:S(2)}) copy-start(f32[31,256]{1,0:T(8,128)} %taps.3) | copy-start | bytes 95236
  32.9 7.9 %collective-permute-start.1 = (f32[136,1024]{1,0:T(8,128)S(1)}, f32[136,1024]{1,0:T(8,128)S(1)}, u32[]{:S(2)}, u32[]{:S(2)}) collective-permute-start(f32[136,1024]{1,0:T(8,128)S(1)} %get-tuple-element.65.sent), channel_id=1, source_target_pairs={{0,4},{4,0},{1,5},{5,1},{2,6},{6,2},{3,7},{7,3},{8,12},{12,8},{9,1... | collective-permute-start | bytes 1671176 | tf_op jit(solution)/shard_map/ppermute | solution.py:26
  41.5 24.8 %all-to-all-start.2 = ((bf16[8,16,1536]{2,1,0:T(8,128)(2,1)}), bf16[8,16,1536]{2,1,0:T(8,128)(2,1)S(1)}, u32[]{:S(2)}, u32[]{:S(2)}) async-start(bf16[8,16,1536]{2,1,0:T(8,128)(2,1)} %shard_map.108), calls=%async_computation.2 | async-start | bytes 786432 | tf_op jit(solution)/shard_map/all_to_all | solution.py:465
  51.2 5.9 %collective-permute-start.2 = (f32[2,32,128]{2,1,0:T(8,128)S(1)}, f32[2,32,128]{2,1,0:T(8,128)S(1)}, u32[]{:S(2)}, u32[]{:S(2)}) collective-permute-start(f32[2,32,128]{2,1,0:T(8,128)S(1)} %slice.3), channel_id=1, source_target_pairs={{4,0},{8,4},{12,8},{16,12},{20,16},{24,20},{28,24},{32,28},{36,32}... | collective-permute-start | bytes 98312 | tf_op jit(solution)/shard_map/ppermute | solution.py:22
  67.2 17.7 %all-to-all-start.3 = ((f32[8,8,1280]{2,1,0:T(8,128)}), f32[8,8,1280]{2,1,0:T(8,128)S(1)}, u32[]{:S(2)}, u32[]{:S(2)}) async-start(f32[8,8,1280]{2,1,0:T(8,128)} %shard_map.110), calls=%async_computation.3 | async-start | bytes 655360 | tf_op jit(solution)/shard_map/all_to_all | solution.py:483

commit v8 on v7

--- a/solution.py
+++ b/solution.py
@@ -135,16 +135,12 @@
 
 
 def conv_stats(conv, stats, start, count):
-    def step(i, carry):
-        r = pl.multiple_of(start + i * 256, 256)
+    for r in range(start, start + count, 256):
         pairs = []
         for h in range(2):
-            c = conv[h, pl.ds(r, 256), :]
+            c = conv[h, r : r + 256, :]
             pairs += [(0, c), (1, c * c)]
-        stats[:, pl.ds(r, 256)] = row_sums(pairs)
-        return carry
-
-    lax.fori_loop(0, count // 256, step, 0)
+        stats[:, r : r + 256] = row_sums(pairs)
 
 
 def conv_body(grad_in, weight_in, glu, taps, conv, stats, out_grad, weight, sems):
@@ -200,35 +196,31 @@
         gain_sum[h] = jnp.zeros((8, LANES), F32)
     size = 256
 
-    def block(i, carry):
-        def step(j, carry):
-            at = pl.ds(pl.multiple_of(i * size + j * 32, 32), 32)
-            rs, mu = columns[0, at], columns[1, at]
-            for h in range(2):
-                g = gain[0:1, lanes(h)]
-                xhat = (conv[h, at, :] - mu) * rs
-                normed = xhat * g
-                sig = jax.nn.sigmoid(normed)
-                act = normed * sig
-                activ[at, lanes(h)] = act.astype(BF16)
-                ng = act_grad[at, lanes(h)] * (sig + act * (1.0 - sig))
-                gain_sum[h] += jnp.sum((ng * xhat).reshape(4, 8, LANES), axis=0)
-                xhats[h, at, :] = xhat
-                scaled[h, at, :] = ng * g * rs
-            return carry
-
-        lax.fori_loop(0, size // 32, step, 0)
-        at = pl.ds(pl.multiple_of(i * size, size), size)
+    def step(j, carry):
+        at = pl.ds(pl.multiple_of(j * 128, 128), 128)
+        rs, mu = columns[0, at], columns[1, at]
+        for h in range(2):
+            g = gain[0:1, lanes(h)]
+            xhat = (conv[h, at, :] - mu) * rs
+            normed = xhat * g
+            sig = jax.nn.sigmoid(normed)
+            act = normed * sig
+            activ[at, lanes(h)] = act.astype(BF16)
+            ng = act_grad[at, lanes(h)] * (sig + act * (1.0 - sig))
+            gain_sum[h] += jnp.sum((ng * xhat).reshape(16, 8, LANES), axis=0)
+            xhats[h, at, :] = xhat
+            scaled[h, at, :] = ng * g * rs
+        return carry
+
+    lax.fori_loop(0, rows // 128, step, 0)
+    for r in range(0, rows, size):
         pairs = []
         for h in range(2):
-            x = scaled[h, at, :]
-            pairs += [(0, x), (1, x * xhats[h, at, :])]
+            x = scaled[h, r : r + size, :]
+            pairs += [(0, x), (1, x * xhats[h, r : r + size, :])]
         out = row_sums(pairs)
         for p in range(peers):
-            sums[p, :, at] = out[0:2]
-        return carry
-
-    lax.fori_loop(0, rows // size, block, 0)
+            sums[p, :, r : r + size] = out[0:2]
 
 
 def taps_body(
@@ -254,16 +246,16 @@
 
             def tile(i, acc, h=h, lo=lo, hi=hi):
                 acc = list(acc)
-                r = pl.multiple_of(i * 32, 32)
-                c = [grad[h, pl.ds(r + u * 8, 8), :] for u in range(4)]
-                for u in range(4):
+                r = pl.multiple_of(i * 64, 64)
+                c = [grad[h, pl.ds(r + u * 8, 8), :] for u in range(8)]
+                for u in range(8):
                     for k in range(lo, hi):
                         base = r + PAD + 1 - n + k
                         acc[k - lo] = acc[k - lo] + c[u] * glu[h, pl.ds(base + u * 8, 8), :]
                 return tuple(acc)
 
             zero = tuple(jnp.zeros((8, LANES), F32) for _ in range(lo, hi))
-            acc = lax.fori_loop(0, rows // 32, tile, zero)
+            acc = lax.fori_loop(0, rows // 64, tile, zero)
             for k in range(lo, hi):
                 small[k : k + 1, lanes(h)] = jnp.sum(acc[k - lo], axis=0, keepdims=True)
         small[n : n + 1, lanes(h)] = jnp.sum(gain_sum[h], axis=0, keepdims=True)

time: 86 us -> 84.9 us (0.987)
  Pallas kernels: 21.7 us -> 20.3 us
    pallas_call x12, Pallas kernels: 21.7 us -> 20.3 us  [kernel(): pl.pallas_call(body, out_shape=[shapes[where](s, d) for s, d, where in ou...]
where the time goes in v8:
time: 84.9 us; the launch traced here: 84.4 us
  starting transfers between devices  28.1 us (33%)
  waiting for transfers between devices  20.9 us (25%)
  Pallas kernels  20.3 us (24%)
  blocking collectives  14.3 us (17%)
    pallas_call x12, Pallas kernels, kernel(): pl.pallas_call(body, out_shape=[shapes[where](s, d) for s, d, where in ou...  20.3 us
    all_to_all x2, blocking collectives, over_tp(): return lax.all_to_all(array, 'tp', 0, 0, tiled=True)  14.3 us
    all_to_all x1, starting transfers between devices, per_device(): first = lax.all_to_all(first, 'z', 0, 0, tiled=True)  9.94 us
    all_to_all x1, waiting for transfers between devices, per_device(): second = lax.all_to_all(second, 'y', 0, 0, tiled=True)  9.62 us
    all_to_all x1, waiting for transfers between devices, per_device(): first = lax.all_to_all(first, 'z', 0, 0, tiled=True)  9.19 us
    ppermute x2, starting transfers between devices, shifted(): return lax.ppermute(block, SP, route)  7.15 us
    ppermute x1, starting transfers between devices, swapped(): return lax.ppermute(block, 'core', [(0, 1), (1, 0)])  6.29 us
    all_to_all x1, starting transfers between devices, per_device(): second = lax.all_to_all(second, 'y', 0, 0, tiled=True)  4.75 us
  transfers between devices with their start and end apart: 5, of which 4 were waited for; matrix products, arithmetic and copies ran while one was open for 0% of the time, Pallas kernels for 12%

profile of v8, /device:TPU:1, one launch (start us, length us, event | category | flops | bytes accessed | tf_op | source)
XLA Modules:
  0.0 84.4 jit_solution(3455974827676470492)
XLA Ops:
  0.6 1.5 %shard_map.101 = (f32[2,1056,128]{2,1,0:T(8,128)S(1)}, f32[2,32,128]{2,1,0:T(8,128)S(1)}, f32[31,256]{1,0:T(8,128)S(1)}) custom-call(bf16[1024,256]{1,0:T(8,128)(2,1)} %value_in.5, bf16[1024,256]{1,0:T(8,128)(2,1)} %gate_in.5, f32[31,256]{1,0:T(8,128)} %taps.3), custom_call_target="tpu_custom_call" | custom-call | tf_op jit(solution)/shard_map/pallas_call | solution.py:46
  2.1 4.6 %collective-permute-start = (f32[2,32,128]{2,1,0:T(8,128)S(1)}, f32[2,32,128]{2,1,0:T(8,128)S(1)}, u32[]{:S(2)}, u32[]{:S(2)}) collective-permute-start(f32[2,32,128]{2,1,0:T(8,128)S(1)} %get-tuple-element.43), channel_id=1, source_target_pairs={{0,4},{4,8},{8,12},{12,16},{16,20},{20,24},{24,28},{28,32},{32,36}... | collective-permute-start | bytes 98312 | tf_op jit(solution)/shard_map/ppermute | solution.py:22
  6.7 2.9 %shard_map.102 = (f32[2,1024,128]{2,1,0:T(8,128)S(1)}, f32[8,1024]{1,0:T(8,128)S(1)}, bf16[1024,1024]{1,0:T(8,128)(2,1)S(1)}, bf16[256,1024]{1,0:T(8,128)(2,1)S(1)}) custom-call(bf16[1024,1024]{1,0:T(8,128)(2,1)} %grad_in.1, bf16[256,1024]{1,0:T(8,128)(2,1)} %weight_in.1, f32[2,1056,128]{2,1,0:T(8,128)S(1)} %get-tuple-element.44.glu.glu_in, ...), custom_call_target="tpu_custom_call" | custom-call | tf_op jit(solution)/shard_map/pallas_call | solution.py:46
  9.6 0.0 copy-start.1
  9.6 0.7 shard_map.103.act_grad
  10.4 0.5 collective-permute-done.edge
  10.9 0.3 shard_map.104
  11.2 7.6 %all_to_all.20.stats = f32[4,2,1024]{2,1,0:T(2,128)S(1)} all-to-all(f32[4,2,1024]{2,1,0:T(2,128)S(1)} %get-tuple-element.52), channel_id=1, replica_groups=mesh['z'=8,'y'=8,'core'=2,'tp'=4] {'tp'}, dimensions={0} | all-to-all | bytes 65536 | tf_op jit(solution)/shard_map/all_to_all | solution.py:383
  18.8 0.0 copy-done.1
  18.8 1.8 %shard_map.105 = (bf16[1024,256]{1,0:T(8,128)(2,1)S(1)}, f32[2,1024,128]{2,1,0:T(8,128)S(1)}, f32[2,1024,128]{2,1,0:T(8,128)S(1)}, f32[4,2,1024]{2,1,0:T(2,128)S(1)}, f32[2,8,128]{2,1,0:T(8,128)S(1)}) custom-call(f32[4,2,1024]{2,1,0:T(2,128)S(1)} %all_to_all.20.stats, f32[2,1024,128]{2,1,0:T(8,128)S(1)} %get-tuple-element.53.conv, ...), custom_call_target="tpu_custom_call" | custom-call | tf_op jit(solution)/shard_map/pallas_call | solution.py:46
  20.6 6.7 %all_to_all.21.refs_1_ = f32[4,2,1024]{2,1,0:T(2,128)S(1)} all-to-all(f32[4,2,1024]{2,1,0:T(2,128)S(1)} %get-tuple-element.55), channel_id=1, replica_groups=mesh['z'=8,'y'=8,'core'=2,'tp'=4] {'tp'}, dimensions={0} | all-to-all | bytes 65536 | tf_op jit(solution)/shard_map/all_to_all | solution.py:383
  27.3 0.9 %shard_map.106 = (f32[128,1024]{1,0:T(8,128)S(1)}, f32[136,1024]{1,0:T(8,128)S(1)}) custom-call(s32[1]{0:T(128)} %bitcast.me, bf16[1024,256]{1,0:T(8,128)(2,1)S(1)} %get-tuple-element.57.activ, bf16[1024,1024]{1,0:T(8,128)(2,1)S(1)} %get-tuple-element.46.out_grad), custom_call_target="tpu_custom_call" | custom-call | tf_op jit(solution)/shard_map/pallas_call | solution.py:46
  28.2 3.3 %shard_map.107 = (f32[2,1024,128]{2,1,0:T(8,128)S(1)}, f32[136,1024]{1,0:T(8,128)S(1)}) custom-call(f32[136,1024]{1,0:T(8,128)S(1)} %get-tuple-element.59.refs_0_, f32[4,2,1024]{2,1,0:T(2,128)S(1)} %all_to_all.21.refs_1_, f32[2,1024,128]{2,1,0:T(8,128)S(1)} %get-tuple-element.61.refs_2_, ...), custom_call_target="tpu_custom_call", output_to_operand_aliasing={{1}: (0, {})} | custom-call | tf_op jit(solution)/shard_map/pallas_call | solution.py:46
  31.4 0.0 copy-start
  31.5 6.3 %collective-permute-start.1 = (f32[136,1024]{1,0:T(8,128)S(1)}, f32[136,1024]{1,0:T(8,128)S(1)}, u32[]{:S(2)}, u32[]{:S(2)}) collective-permute-start(f32[136,1024]{1,0:T(8,128)S(1)} %get-tuple-element.65.sent), channel_id=1, source_target_pairs={{0,4},{4,0},{1,5},{5,1},{2,6},{6,2},{3,7},{7,3},{8,12},{12,8},{9,1... | collective-permute-start | bytes 1671176 | tf_op jit(solution)/shard_map/ppermute | solution.py:26
  37.8 1.6 %collective-permute-done.1.received = f32[136,1024]{1,0:T(8,128)S(1)} collective-permute-done((f32[136,1024]{1,0:T(8,128)S(1)}, f32[136,1024]{1,0:T(8,128)S(1)}, u32[]{:S(2)}, u32[]{:S(2)}) %collective-permute-start.1) | collective-permute-done | bytes 557088 | tf_op jit(solution)/shard_map/ppermute | solution.py:26
  39.3 0.8 shard_map.108
  40.1 9.9 %all-to-all-start.2 = ((bf16[8,16,1536]{2,1,0:T(8,128)(2,1)}), bf16[8,16,1536]{2,1,0:T(8,128)(2,1)S(1)}, u32[]{:S(2)}, u32[]{:S(2)}) async-start(bf16[8,16,1536]{2,1,0:T(8,128)(2,1)} %shard_map.108), calls=%async_computation.2 | async-start | bytes 786432 | tf_op jit(solution)/shard_map/all_to_all | solution.py:457
  50.1 2.6 %collective-permute-start.2 = (f32[2,32,128]{2,1,0:T(8,128)S(1)}, f32[2,32,128]{2,1,0:T(8,128)S(1)}, u32[]{:S(2)}, u32[]{:S(2)}) collective-permute-start(f32[2,32,128]{2,1,0:T(8,128)S(1)} %slice.3), channel_id=1, source_target_pairs={{4,0},{8,4},{12,8},{16,12},{20,16},{24,20},{28,24},{32,28},{36,32}... | collective-permute-start | bytes 98312 | tf_op jit(solution)/shard_map/ppermute | solution.py:22
  52.6 0.0 copy-done
  52.7 3.4 %shard_map.109 = (bf16[1024,256]{1,0:T(8,128)(2,1)}, bf16[1024,256]{1,0:T(8,128)(2,1)}) custom-call(bf16[1024,256]{1,0:T(8,128)(2,1)} %value_in.5, bf16[1024,256]{1,0:T(8,128)(2,1)} %gate_in.5, f32[2,1024,128]{2,1,0:T(8,128)S(1)} %get-tuple-element.66.grad, f32[31,256]{1,0:T(8,128)S(1)} %copy-done), custom_call_target="tpu_custom_call" | custom-call | tf_op jit(solution)/shard_map/pallas_call | solution.py:46
  56.0 0.0 collective-permute-done.2.after
  56.0 9.2 %all-to-all-done.2.got = bf16[8,16,1536]{2,1,0:T(8,128)(2,1)S(1)} async-done(((bf16[8,16,1536]{2,1,0:T(8,128)(2,1)}), bf16[8,16,1536]{2,1,0:T(8,128)(2,1)S(1)}, u32[]{:S(2)}, u32[]{:S(2)}) %all-to-all-start.2) | async-done | bytes 393248 | tf_op jit(solution)/shard_map/all_to_all | solution.py:457
  65.2 0.8 shard_map.110
  66.0 4.7 %all-to-all-start.3 = ((f32[8,8,1280]{2,1,0:T(8,128)}), f32[8,8,1280]{2,1,0:T(8,128)S(1)}, u32[]{:S(2)}, u32[]{:S(2)}) async-start(f32[8,8,1280]{2,1,0:T(8,128)} %shard_map.110), calls=%async_computation.3 | async-start | bytes 655360 | tf_op jit(solution)/shard_map/all_to_all | solution.py:475
  70.8 3.3 %shard_map.111 = (bf16[1024,256]{1,0:T(8,128)(2,1)}, bf16[1024,256]{1,0:T(8,128)(2,1)}) custom-call(bf16[1024,256]{1,0:T(8,128)(2,1)} %value_in.5, bf16[1024,256]{1,0:T(8,128)(2,1)} %gate_in.5, bf16[1024,256]{1,0:T(8,128)(2,1)} %get-tuple-element.70.value_part, ...), custom_call_target="tpu_custom_call", output_to_operand_aliasing={{0}: (2, {}), {1}: (3, {})} | custom-call | tf_op jit(solution)/shard_map/pallas_call | solution.py:46
  74.1 9.6 %all-to-all-done.3.refs_0_ = f32[8,8,1280]{2,1,0:T(8,128)S(1)} async-done(((f32[8,8,1280]{2,1,0:T(8,128)}), f32[8,8,1280]{2,1,0:T(8,128)S(1)}, u32[]{:S(2)}, u32[]{:S(2)}) %all-to-all-start.3) | async-done | bytes 327712 | tf_op jit(solution)/shard_map/all_to_all | solution.py:475
  83.7 0.6 shard_map.112
  (1 shorter events, 0.0 us)
Async XLA Ops:
  2.1 8.8 %collective-permute-start = (f32[2,32,128]{2,1,0:T(8,128)S(1)}, f32[2,32,128]{2,1,0:T(8,128)S(1)}, u32[]{:S(2)}, u32[]{:S(2)}) collective-permute-start(f32[2,32,128]{2,1,0:T(8,128)S(1)} %get-tuple-element.43), channel_id=1, source_target_pairs={{0,4},{4,8},{8,12},{12,16},{16,20},{20,24},{24,28},{28,32},{32,36}... | collective-permute-start | bytes 98312 | tf_op jit(solution)/shard_map/ppermute | solution.py:22
  9.6 9.2 %copy-start.1 = (f32[256]{0:T(256)S(1)}, f32[256]{0:T(256)}, u32[]{:S(2)}) copy-start(f32[256]{0:T(256)} %param.9) | copy-start | bytes 3076
  31.4 21.2 %copy-start = (f32[31,256]{1,0:T(8,128)S(1)}, f32[31,256]{1,0:T(8,128)}, u32[]{:S(2)}) copy-start(f32[31,256]{1,0:T(8,128)} %taps.3) | copy-start | bytes 95236
  31.5 7.9 %collective-permute-start.1 = (f32[136,1024]{1,0:T(8,128)S(1)}, f32[136,1024]{1,0:T(8,128)S(1)}, u32[]{:S(2)}, u32[]{:S(2)}) collective-permute-start(f32[136,1024]{1,0:T(8,128)S(1)} %get-tuple-element.65.sent), channel_id=1, source_target_pairs={{0,4},{4,0},{1,5},{5,1},{2,6},{6,2},{3,7},{7,3},{8,12},{12,8},{9,1... | collective-permute-start | bytes 1671176 | tf_op jit(solution)/shard_map/ppermute | solution.py:26
  40.1 25.1 %all-to-all-start.2 = ((bf16[8,16,1536]{2,1,0:T(8,128)(2,1)}), bf16[8,16,1536]{2,1,0:T(8,128)(2,1)S(1)}, u32[]{:S(2)}, u32[]{:S(2)}) async-start(bf16[8,16,1536]{2,1,0:T(8,128)(2,1)} %shard_map.108), calls=%async_computation.2 | async-start | bytes 786432 | tf_op jit(solution)/shard_map/all_to_all | solution.py:457
  50.1 5.9 %collective-permute-start.2 = (f32[2,32,128]{2,1,0:T(8,128)S(1)}, f32[2,32,128]{2,1,0:T(8,128)S(1)}, u32[]{:S(2)}, u32[]{:S(2)}) collective-permute-start(f32[2,32,128]{2,1,0:T(8,128)S(1)} %slice.3), channel_id=1, source_target_pairs={{4,0},{8,4},{12,8},{16,12},{20,16},{24,20},{28,24},{32,28},{36,32}... | collective-permute-start | bytes 98312 | tf_op jit(solution)/shard_map/ppermute | solution.py:22
  66.0 17.7 %all-to-all-start.3 = ((f32[8,8,1280]{2,1,0:T(8,128)}), f32[8,8,1280]{2,1,0:T(8,128)S(1)}, u32[]{:S(2)}, u32[]{:S(2)}) async-start(f32[8,8,1280]{2,1,0:T(8,128)} %shard_map.110), calls=%async_computation.3 | async-start | bytes 655360 | tf_op jit(solution)/shard_map/all_to_all | solution.py:475

commit v9 on v8

--- a/solution.py
+++ b/solution.py
@@ -10,6 +10,7 @@
 
 
 SP = ("z", "y", "core")
+Y_ORDER = [4, 5, 6, 7, 0, 1, 2, 3]
 F32, BF16 = jnp.float32, jnp.bfloat16
 LANES = 128
 PAD = 32
@@ -246,16 +247,16 @@
 
             def tile(i, acc, h=h, lo=lo, hi=hi):
                 acc = list(acc)
-                r = pl.multiple_of(i * 64, 64)
-                c = [grad[h, pl.ds(r + u * 8, 8), :] for u in range(8)]
-                for u in range(8):
+                r = pl.multiple_of(i * 128, 128)
+                c = [grad[h, pl.ds(r + u * 8, 8), :] for u in range(16)]
+                for u in range(16):
                     for k in range(lo, hi):
                         base = r + PAD + 1 - n + k
                         acc[k - lo] = acc[k - lo] + c[u] * glu[h, pl.ds(base + u * 8, 8), :]
                 return tuple(acc)
 
             zero = tuple(jnp.zeros((8, LANES), F32) for _ in range(lo, hi))
-            acc = lax.fori_loop(0, rows // 64, tile, zero)
+            acc = lax.fori_loop(0, rows // 128, tile, zero)
             for k in range(lo, hi):
                 small[k : k + 1, lanes(h)] = jnp.sum(acc[k - lo], axis=0, keepdims=True)
         small[n : n + 1, lanes(h)] = jnp.sum(gain_sum[h], axis=0, keepdims=True)
@@ -286,7 +287,7 @@
         for i in range(2):
             for j in range(4):
                 out[p, 4 * i + j : 4 * i + j + 1, 1024:1280] = held[
-                    2 * p + i : 2 * p + i + 1, 256 * j : 256 * j + 256
+                    2 * Y_ORDER[p] + i : 2 * Y_ORDER[p] + i + 1, 256 * j : 256 * j + 256
                 ]
 
 
@@ -472,7 +473,7 @@
     (second,) = kernel(
         relay_body, [((8, 8, 1280), F32, "any")], (near(first),), scratch=[((16, outs), F32)]
     )
-    second = lax.all_to_all(second, "y", 0, 0, tiled=True)
+    second = lax.all_to_all(second, "y", 0, 0, tiled=True, axis_index_groups=[Y_ORDER])
     value_grad, gate_grad = kernel(
         glu_tail_body,
         [(*tall, "far")] * 2,

time: 84.9 us -> 81.4 us (0.959)
  waiting for transfers between devices: 20.9 us -> 15.4 us
  starting transfers between devices: 28.1 us -> 30.2 us
    all_to_all x1, waiting for transfers between devices: 9.62 us -> 4.15 us  [per_device(): lax.all_to_all(second, 'y', 0, 0, tiled=True, axis_index_groups=[Y_ORDER])]
    all_to_all x1, starting transfers between devices: 4.75 us -> 6.82 us  [per_device(): lax.all_to_all(second, 'y', 0, 0, tiled=True, axis_index_groups=[Y_ORDER])]
  transfers between devices with their start and end apart: 5 -> 5, of which waited for: 4 -> 4; matrix products, arithmetic and copies ran while one was open for 0% -> 0% of each run, Pallas kernels for 12% -> 13%
where the time goes in v9:
time: 81.4 us; the launch traced here: 80.8 us
  starting transfers between devices  30.2 us (37%)
  Pallas kernels  20.1 us (25%)
  waiting for transfers between devices  15.4 us (19%)
  blocking collectives  14.3 us (18%)
    pallas_call x12, Pallas kernels, kernel(): pl.pallas_call(body, out_shape=[shapes[where](s, d) for s, d, where in ou...  20.1 us
    all_to_all x2, blocking collectives, over_tp(): return lax.all_to_all(array, 'tp', 0, 0, tiled=True)  14.3 us
    all_to_all x1, starting transfers between devices, per_device(): first = lax.all_to_all(first, 'z', 0, 0, tiled=True)  9.94 us
    all_to_all x1, waiting for transfers between devices, per_device(): first = lax.all_to_all(first, 'z', 0, 0, tiled=True)  9.19 us
    ppermute x2, starting transfers between devices, shifted(): return lax.ppermute(block, SP, route)  7.15 us
    all_to_all x1, starting transfers between devices, per_device(): lax.all_to_all(second, 'y', 0, 0, tiled=True, axis_index_groups=[Y_ORDER])  6.82 us
    ppermute x1, starting transfers between devices, swapped(): return lax.ppermute(block, 'core', [(0, 1), (1, 0)])  6.29 us
    all_to_all x1, waiting for transfers between devices, per_device(): lax.all_to_all(second, 'y', 0, 0, tiled=True, axis_index_groups=[Y_ORDER])  4.15 us
  transfers between devices with their start and end apart: 5, of which 4 were waited for; matrix products, arithmetic and copies ran while one was open for 0% of the time, Pallas kernels for 13%

profile of v9, /device:TPU:1, one launch (start us, length us, event | category | flops | bytes accessed | tf_op | source)
XLA Modules:
  0.0 80.8 jit_solution(7034560921942888036)
XLA Ops:
  0.6 1.5 %shard_map.101 = (f32[2,1056,128]{2,1,0:T(8,128)S(1)}, f32[2,32,128]{2,1,0:T(8,128)S(1)}, f32[31,256]{1,0:T(8,128)S(1)}) custom-call(bf16[1024,256]{1,0:T(8,128)(2,1)} %value_in.5, bf16[1024,256]{1,0:T(8,128)(2,1)} %gate_in.5, f32[31,256]{1,0:T(8,128)} %taps.3), custom_call_target="tpu_custom_call" | custom-call | tf_op jit(solution)/shard_map/pallas_call | solution.py:47
  2.1 4.6 %collective-permute-start = (f32[2,32,128]{2,1,0:T(8,128)S(1)}, f32[2,32,128]{2,1,0:T(8,128)S(1)}, u32[]{:S(2)}, u32[]{:S(2)}) collective-permute-start(f32[2,32,128]{2,1,0:T(8,128)S(1)} %get-tuple-element.43), channel_id=1, source_target_pairs={{0,4},{4,8},{8,12},{12,16},{16,20},{20,24},{24,28},{28,32},{32,36}... | collective-permute-start | bytes 98312 | tf_op jit(solution)/shard_map/ppermute | solution.py:23
  6.7 2.9 %shard_map.102 = (f32[2,1024,128]{2,1,0:T(8,128)S(1)}, f32[8,1024]{1,0:T(8,128)S(1)}, bf16[1024,1024]{1,0:T(8,128)(2,1)S(1)}, bf16[256,1024]{1,0:T(8,128)(2,1)S(1)}) custom-call(bf16[1024,1024]{1,0:T(8,128)(2,1)} %grad_in.1, bf16[256,1024]{1,0:T(8,128)(2,1)} %weight_in.1, f32[2,1056,128]{2,1,0:T(8,128)S(1)} %get-tuple-element.44.glu.glu_in, ...), custom_call_target="tpu_custom_call" | custom-call | tf_op jit(solution)/shard_map/pallas_call | solution.py:47
  9.6 0.0 copy-start.1
  9.6 0.7 shard_map.103.act_grad
  10.4 0.5 collective-permute-done.edge
  10.9 0.3 shard_map.104
  11.2 7.6 %all_to_all.20.stats = f32[4,2,1024]{2,1,0:T(2,128)S(1)} all-to-all(f32[4,2,1024]{2,1,0:T(2,128)S(1)} %get-tuple-element.52), channel_id=1, replica_groups=mesh['z'=8,'y'=8,'core'=2,'tp'=4] {'tp'}, dimensions={0} | all-to-all | bytes 65536 | tf_op jit(solution)/shard_map/all_to_all | solution.py:384
  18.8 0.0 copy-done.1
  18.8 1.8 %shard_map.105 = (bf16[1024,256]{1,0:T(8,128)(2,1)S(1)}, f32[2,1024,128]{2,1,0:T(8,128)S(1)}, f32[2,1024,128]{2,1,0:T(8,128)S(1)}, f32[4,2,1024]{2,1,0:T(2,128)S(1)}, f32[2,8,128]{2,1,0:T(8,128)S(1)}) custom-call(f32[4,2,1024]{2,1,0:T(2,128)S(1)} %all_to_all.20.stats, f32[2,1024,128]{2,1,0:T(8,128)S(1)} %get-tuple-element.53.conv, ...), custom_call_target="tpu_custom_call" | custom-call | tf_op jit(solution)/shard_map/pallas_call | solution.py:47
  20.6 6.7 %all_to_all.21.refs_1_ = f32[4,2,1024]{2,1,0:T(2,128)S(1)} all-to-all(f32[4,2,1024]{2,1,0:T(2,128)S(1)} %get-tuple-element.55), channel_id=1, replica_groups=mesh['z'=8,'y'=8,'core'=2,'tp'=4] {'tp'}, dimensions={0} | all-to-all | bytes 65536 | tf_op jit(solution)/shard_map/all_to_all | solution.py:384
  27.3 0.9 %shard_map.106 = (f32[128,1024]{1,0:T(8,128)S(1)}, f32[136,1024]{1,0:T(8,128)S(1)}) custom-call(s32[1]{0:T(128)} %bitcast.me, bf16[1024,256]{1,0:T(8,128)(2,1)S(1)} %get-tuple-element.57.activ, bf16[1024,1024]{1,0:T(8,128)(2,1)S(1)} %get-tuple-element.46.out_grad), custom_call_target="tpu_custom_call" | custom-call | tf_op jit(solution)/shard_map/pallas_call | solution.py:47
  28.2 3.1 %shard_map.107 = (f32[2,1024,128]{2,1,0:T(8,128)S(1)}, f32[136,1024]{1,0:T(8,128)S(1)}) custom-call(f32[136,1024]{1,0:T(8,128)S(1)} %get-tuple-element.59.refs_0_, f32[4,2,1024]{2,1,0:T(2,128)S(1)} %all_to_all.21.refs_1_, f32[2,1024,128]{2,1,0:T(8,128)S(1)} %get-tuple-element.61.refs_2_, ...), custom_call_target="tpu_custom_call", output_to_operand_aliasing={{1}: (0, {})} | custom-call | tf_op jit(solution)/shard_map/pallas_call | solution.py:47
  31.3 0.0 copy-start
  31.3 6.3 %collective-permute-start.1 = (f32[136,1024]{1,0:T(8,128)S(1)}, f32[136,1024]{1,0:T(8,128)S(1)}, u32[]{:S(2)}, u32[]{:S(2)}) collective-permute-start(f32[136,1024]{1,0:T(8,128)S(1)} %get-tuple-element.65.sent), channel_id=1, source_target_pairs={{0,4},{4,0},{1,5},{5,1},{2,6},{6,2},{3,7},{7,3},{8,12},{12,8},{9,1... | collective-permute-start | bytes 1671176 | tf_op jit(solution)/shard_map/ppermute | solution.py:27
  37.6 1.6 %collective-permute-done.1.received = f32[136,1024]{1,0:T(8,128)S(1)} collective-permute-done((f32[136,1024]{1,0:T(8,128)S(1)}, f32[136,1024]{1,0:T(8,128)S(1)}, u32[]{:S(2)}, u32[]{:S(2)}) %collective-permute-start.1) | collective-permute-done | bytes 557088 | tf_op jit(solution)/shard_map/ppermute | solution.py:27
  39.1 0.8 %shard_map.108 = bf16[8,16,1536]{2,1,0:T(8,128)(2,1)} custom-call(f32[128,1024]{1,0:T(8,128)S(1)} %get-tuple-element.58.kept, f32[136,1024]{1,0:T(8,128)S(1)} %get-tuple-element.65.sent, f32[136,1024]{1,0:T(8,128)S(1)} %collective-permute-done.1.received), custom_call_target="tpu_custom_call" | custom-call | tf_op jit(solution)/shard_map/pallas_call | solution.py:47
  39.9 9.9 %all-to-all-start.2 = ((bf16[8,16,1536]{2,1,0:T(8,128)(2,1)}), bf16[8,16,1536]{2,1,0:T(8,128)(2,1)S(1)}, u32[]{:S(2)}, u32[]{:S(2)}) async-start(bf16[8,16,1536]{2,1,0:T(8,128)(2,1)} %shard_map.108), calls=%async_computation.2 | async-start | bytes 786432 | tf_op jit(solution)/shard_map/all_to_all | solution.py:458
  49.9 2.6 %collective-permute-start.2 = (f32[2,32,128]{2,1,0:T(8,128)S(1)}, f32[2,32,128]{2,1,0:T(8,128)S(1)}, u32[]{:S(2)}, u32[]{:S(2)}) collective-permute-start(f32[2,32,128]{2,1,0:T(8,128)S(1)} %slice.3), channel_id=1, source_target_pairs={{4,0},{8,4},{12,8},{16,12},{20,16},{24,20},{28,24},{32,28},{36,32}... | collective-permute-start | bytes 98312 | tf_op jit(solution)/shard_map/ppermute | solution.py:23
  52.5 0.0 copy-done
  52.5 3.4 %shard_map.109 = (bf16[1024,256]{1,0:T(8,128)(2,1)}, bf16[1024,256]{1,0:T(8,128)(2,1)}) custom-call(bf16[1024,256]{1,0:T(8,128)(2,1)} %value_in.5, bf16[1024,256]{1,0:T(8,128)(2,1)} %gate_in.5, f32[2,1024,128]{2,1,0:T(8,128)S(1)} %get-tuple-element.66.grad, f32[31,256]{1,0:T(8,128)S(1)} %copy-done), custom_call_target="tpu_custom_call" | custom-call | tf_op jit(solution)/shard_map/pallas_call | solution.py:47
  55.8 0.0 collective-permute-done.2.after
  55.8 9.2 %all-to-all-done.2.got = bf16[8,16,1536]{2,1,0:T(8,128)(2,1)S(1)} async-done(((bf16[8,16,1536]{2,1,0:T(8,128)(2,1)}), bf16[8,16,1536]{2,1,0:T(8,128)(2,1)S(1)}, u32[]{:S(2)}, u32[]{:S(2)}) %all-to-all-start.2) | async-done | bytes 393248 | tf_op jit(solution)/shard_map/all_to_all | solution.py:458
  65.0 0.8 %shard_map.110 = f32[8,8,1280]{2,1,0:T(8,128)} custom-call(bf16[8,16,1536]{2,1,0:T(8,128)(2,1)S(1)} %all-to-all-done.2.got), custom_call_target="tpu_custom_call" | custom-call | tf_op jit(solution)/shard_map/pallas_call | solution.py:47
  65.8 6.8 %all-to-all-start.3 = ((f32[8,8,1280]{2,1,0:T(8,128)}), f32[8,8,1280]{2,1,0:T(8,128)S(1)}, u32[]{:S(2)}, u32[]{:S(2)}) async-start(f32[8,8,1280]{2,1,0:T(8,128)} %shard_map.110), calls=%async_computation.3 | async-start | bytes 655360 | tf_op jit(solution)/shard_map/all_to_all | solution.py:476
  72.7 3.3 %shard_map.111 = (bf16[1024,256]{1,0:T(8,128)(2,1)}, bf16[1024,256]{1,0:T(8,128)(2,1)}) custom-call(bf16[1024,256]{1,0:T(8,128)(2,1)} %value_in.5, bf16[1024,256]{1,0:T(8,128)(2,1)} %gate_in.5, bf16[1024,256]{1,0:T(8,128)(2,1)} %get-tuple-element.70.value_part, ...), custom_call_target="tpu_custom_call", output_to_operand_aliasing={{0}: (2, {}), {1}: (3, {})} | custom-call | tf_op jit(solution)/shard_map/pallas_call | solution.py:47
  76.0 4.1 %all-to-all-done.3.refs_0_ = f32[8,8,1280]{2,1,0:T(8,128)S(1)} async-done(((f32[8,8,1280]{2,1,0:T(8,128)}), f32[8,8,1280]{2,1,0:T(8,128)S(1)}, u32[]{:S(2)}, u32[]{:S(2)}) %all-to-all-start.3) | async-done | bytes 327712 | tf_op jit(solution)/shard_map/all_to_all | solution.py:476
  80.2 0.6 shard_map.112
  (1 shorter events, 0.0 us)
Async XLA Ops:
  2.1 8.8 %collective-permute-start = (f32[2,32,128]{2,1,0:T(8,128)S(1)}, f32[2,32,128]{2,1,0:T(8,128)S(1)}, u32[]{:S(2)}, u32[]{:S(2)}) collective-permute-start(f32[2,32,128]{2,1,0:T(8,128)S(1)} %get-tuple-element.43), channel_id=1, source_target_pairs={{0,4},{4,8},{8,12},{12,16},{16,20},{20,24},{24,28},{28,32},{32,36}... | collective-permute-start | bytes 98312 | tf_op jit(solution)/shard_map/ppermute | solution.py:23
  9.6 9.2 %copy-start.1 = (f32[256]{0:T(256)S(1)}, f32[256]{0:T(256)}, u32[]{:S(2)}) copy-start(f32[256]{0:T(256)} %param.9) | copy-start | bytes 3076
  31.3 21.2 %copy-start = (f32[31,256]{1,0:T(8,128)S(1)}, f32[31,256]{1,0:T(8,128)}, u32[]{:S(2)}) copy-start(f32[31,256]{1,0:T(8,128)} %taps.3) | copy-start | bytes 95236
  31.3 7.9 %collective-permute-start.1 = (f32[136,1024]{1,0:T(8,128)S(1)}, f32[136,1024]{1,0:T(8,128)S(1)}, u32[]{:S(2)}, u32[]{:S(2)}) collective-permute-start(f32[136,1024]{1,0:T(8,128)S(1)} %get-tuple-element.65.sent), channel_id=1, source_target_pairs={{0,4},{4,0},{1,5},{5,1},{2,6},{6,2},{3,7},{7,3},{8,12},{12,8},{9,1... | collective-permute-start | bytes 1671176 | tf_op jit(solution)/shard_map/ppermute | solution.py:27
  39.9 25.1 %all-to-all-start.2 = ((bf16[8,16,1536]{2,1,0:T(8,128)(2,1)}), bf16[8,16,1536]{2,1,0:T(8,128)(2,1)S(1)}, u32[]{:S(2)}, u32[]{:S(2)}) async-start(bf16[8,16,1536]{2,1,0:T(8,128)(2,1)} %shard_map.108), calls=%async_computation.2 | async-start | bytes 786432 | tf_op jit(solution)/shard_map/all_to_all | solution.py:458
  49.9 5.9 %collective-permute-start.2 = (f32[2,32,128]{2,1,0:T(8,128)S(1)}, f32[2,32,128]{2,1,0:T(8,128)S(1)}, u32[]{:S(2)}, u32[]{:S(2)}) collective-permute-start(f32[2,32,128]{2,1,0:T(8,128)S(1)} %slice.3), channel_id=1, source_target_pairs={{4,0},{8,4},{12,8},{16,12},{20,16},{24,20},{28,24},{32,28},{36,32}... | collective-permute-start | bytes 98312 | tf_op jit(solution)/shard_map/ppermute | solution.py:23
  65.8 14.3 %all-to-all-start.3 = ((f32[8,8,1280]{2,1,0:T(8,128)}), f32[8,8,1280]{2,1,0:T(8,128)S(1)}, u32[]{:S(2)}, u32[]{:S(2)}) async-start(f32[8,8,1280]{2,1,0:T(8,128)} %shard_map.110), calls=%async_computation.3 | async-start | bytes 655360 | tf_op jit(solution)/shard_map/all_to_all | solution.py:476

commit v10 on v9

--- a/solution.py
+++ b/solution.py
@@ -10,7 +10,9 @@
 
 
 SP = ("z", "y", "core")
+X_ORDER = [3, 0, 1, 2]
 Y_ORDER = [4, 5, 6, 7, 0, 1, 2, 3]
+Z_ORDER = [4, 5, 6, 7, 0, 1, 2, 3]
 F32, BF16 = jnp.float32, jnp.bfloat16
 LANES = 128
 PAD = 32
@@ -269,8 +271,8 @@
     rows, outs = kept.shape
     total = sent[rows:] + received[rows:]
     small = jnp.concatenate([total[:, 0:512], total[:, 512:1024]], axis=0).astype(BF16)
-    for p in range(out.shape[0]):
-        at = slice(p * 16, (p + 1) * 16)
+    for p, z in enumerate(Z_ORDER):
+        at = slice(z * 16, (z + 1) * 16)
         out[p, :, 0:outs] = (kept[at] + received[at]).astype(BF16)
         out[p, :, outs:] = small
 
@@ -381,7 +383,7 @@
 
 
 def over_tp(array):
-    return lax.all_to_all(array, "tp", 0, 0, tiled=True)
+    return lax.all_to_all(array, "tp", 0, 0, tiled=True, axis_index_groups=[X_ORDER])
 
 
 def per_device(glu_value, glu_gate, conv_taps, channel_gain, proj_weight, out_grad):
@@ -455,7 +457,7 @@
     (first,) = kernel(
         pack_body, [((8, 16, outs + 512), BF16, "any")], (near(kept), near(sent), near(received))
     )
-    first = lax.all_to_all(first, "z", 0, 0, tiled=True)
+    first = lax.all_to_all(first, "z", 0, 0, tiled=True, axis_index_groups=[Z_ORDER])
     after = shifted(grad[:, :PAD], -1)
 
     def gates(length):

time: 81.4 us -> 76.9 us (0.945)
  waiting for transfers between devices: 15.4 us -> 8.56 us
  starting transfers between devices: 30.2 us -> 33.3 us
    all_to_all x1, waiting for transfers between devices: 9.19 us -> 2.64 us  [per_device(): lax.all_to_all(first, 'z', 0, 0, tiled=True, axis_index_groups=[Z_ORDER])]
    all_to_all x1, starting transfers between devices: 9.94 us -> 11.2 us  [per_device(): lax.all_to_all(first, 'z', 0, 0, tiled=True, axis_index_groups=[Z_ORDER])]
    all_to_all x1, starting transfers between devices: 6.82 us -> 8.03 us  [per_device(): lax.all_to_all(second, 'y', 0, 0, tiled=True, axis_index_groups=[Y_ORDER])]
  transfers between devices with their start and end apart: 5 -> 5, of which waited for: 4 -> 4; matrix products, arithmetic and copies ran while one was open for 0% -> 0% of each run, Pallas kernels for 13% -> 14%
where the time goes in v10:
time: 76.9 us; the launch traced here: 76.3 us
  starting transfers between devices  33.3 us (43%)
  Pallas kernels  20.1 us (26%)
  blocking collectives  13.5 us (18%)
  waiting for transfers between devices  8.56 us (11%)
    pallas_call x12, Pallas kernels, kernel(): pl.pallas_call(body, out_shape=[shapes[where](s, d) for s, d, where in ou...  20.1 us
    all_to_all x2, blocking collectives, over_tp(): lax.all_to_all(array, 'tp', 0, 0, tiled=True, axis_index_groups=[X_ORDER])  13.5 us
    all_to_all x1, starting transfers between devices, per_device(): lax.all_to_all(first, 'z', 0, 0, tiled=True, axis_index_groups=[Z_ORDER])  11.2 us
    all_to_all x1, starting transfers between devices, per_device(): lax.all_to_all(second, 'y', 0, 0, tiled=True, axis_index_groups=[Y_ORDER])  8.03 us
    ppermute x2, starting transfers between devices, shifted(): return lax.ppermute(block, SP, route)  7.13 us
    ppermute x1, starting transfers between devices, swapped(): return lax.ppermute(block, 'core', [(0, 1), (1, 0)])  6.94 us
    all_to_all x1, waiting for transfers between devices, per_device(): lax.all_to_all(second, 'y', 0, 0, tiled=True, axis_index_groups=[Y_ORDER])  3.83 us
    all_to_all x1, waiting for transfers between devices, per_device(): lax.all_to_all(first, 'z', 0, 0, tiled=True, axis_index_groups=[Z_ORDER])  2.64 us
  transfers between devices with their start and end apart: 5, of which 4 were waited for; matrix products, arithmetic and copies ran while one was open for 0% of the time, Pallas kernels for 14%

profile of v10, /device:TPU:1, one launch (start us, length us, event | category | flops | bytes accessed | tf_op | source)
XLA Modules:
  0.0 76.3 jit_solution(9227079807540297533)
XLA Ops:
  0.6 1.5 %shard_map.101 = (f32[2,1056,128]{2,1,0:T(8,128)S(1)}, f32[2,32,128]{2,1,0:T(8,128)S(1)}, f32[31,256]{1,0:T(8,128)S(1)}) custom-call(bf16[1024,256]{1,0:T(8,128)(2,1)} %value_in.5, bf16[1024,256]{1,0:T(8,128)(2,1)} %gate_in.5, f32[31,256]{1,0:T(8,128)} %taps.3), custom_call_target="tpu_custom_call" | custom-call | tf_op jit(solution)/shard_map/pallas_call | solution.py:49
  2.1 4.6 %collective-permute-start = (f32[2,32,128]{2,1,0:T(8,128)S(1)}, f32[2,32,128]{2,1,0:T(8,128)S(1)}, u32[]{:S(2)}, u32[]{:S(2)}) collective-permute-start(f32[2,32,128]{2,1,0:T(8,128)S(1)} %get-tuple-element.43), channel_id=1, source_target_pairs={{0,4},{4,8},{8,12},{12,16},{16,20},{20,24},{24,28},{28,32},{32,36}... | collective-permute-start | bytes 98312 | tf_op jit(solution)/shard_map/ppermute | solution.py:25
  6.7 2.9 %shard_map.102 = (f32[2,1024,128]{2,1,0:T(8,128)S(1)}, f32[8,1024]{1,0:T(8,128)S(1)}, bf16[1024,1024]{1,0:T(8,128)(2,1)S(1)}, bf16[256,1024]{1,0:T(8,128)(2,1)S(1)}) custom-call(bf16[1024,1024]{1,0:T(8,128)(2,1)} %grad_in.1, bf16[256,1024]{1,0:T(8,128)(2,1)} %weight_in.1, f32[2,1056,128]{2,1,0:T(8,128)S(1)} %get-tuple-element.44.glu.glu_in, ...), custom_call_target="tpu_custom_call" | custom-call | tf_op jit(solution)/shard_map/pallas_call | solution.py:49
  9.6 0.0 copy-start.1
  9.6 0.7 shard_map.103.act_grad
  10.4 0.5 collective-permute-done.edge
  10.9 0.3 shard_map.104
  11.2 6.9 %all_to_all.20.stats = f32[4,2,1024]{2,1,0:T(2,128)S(1)} all-to-all(f32[4,2,1024]{2,1,0:T(2,128)S(1)} %get-tuple-element.52), channel_id=1, replica_groups={{3,0,1,2},{7,4,5,6},{11,8,9,10},{15,12,13,14},{19,16,17,18},{23,20,21,2..., dimensions={0} | all-to-all | bytes 65536 | tf_op jit(solution)/shard_map/all_to_all | solution.py:386
  18.1 0.0 copy-done.1
  18.1 1.8 %shard_map.105 = (bf16[1024,256]{1,0:T(8,128)(2,1)S(1)}, f32[2,1024,128]{2,1,0:T(8,128)S(1)}, f32[2,1024,128]{2,1,0:T(8,128)S(1)}, f32[4,2,1024]{2,1,0:T(2,128)S(1)}, f32[2,8,128]{2,1,0:T(8,128)S(1)}) custom-call(f32[4,2,1024]{2,1,0:T(2,128)S(1)} %all_to_all.20.stats, f32[2,1024,128]{2,1,0:T(8,128)S(1)} %get-tuple-element.53.conv, ...), custom_call_target="tpu_custom_call" | custom-call | tf_op jit(solution)/shard_map/pallas_call | solution.py:49
  19.9 6.7 %all_to_all.21.refs_1_ = f32[4,2,1024]{2,1,0:T(2,128)S(1)} all-to-all(f32[4,2,1024]{2,1,0:T(2,128)S(1)} %get-tuple-element.55), channel_id=1, replica_groups={{3,0,1,2},{7,4,5,6},{11,8,9,10},{15,12,13,14},{19,16,17,18},{23,20,21,2..., dimensions={0} | all-to-all | bytes 65536 | tf_op jit(solution)/shard_map/all_to_all | solution.py:386
  26.5 0.9 %shard_map.106 = (f32[128,1024]{1,0:T(8,128)S(1)}, f32[136,1024]{1,0:T(8,128)S(1)}) custom-call(s32[1]{0:T(128)} %bitcast.me, bf16[1024,256]{1,0:T(8,128)(2,1)S(1)} %get-tuple-element.57.activ, bf16[1024,1024]{1,0:T(8,128)(2,1)S(1)} %get-tuple-element.46.out_grad), custom_call_target="tpu_custom_call" | custom-call | tf_op jit(solution)/shard_map/pallas_call | solution.py:49
  27.4 3.1 %shard_map.107 = (f32[2,1024,128]{2,1,0:T(8,128)S(1)}, f32[136,1024]{1,0:T(8,128)S(1)}) custom-call(f32[136,1024]{1,0:T(8,128)S(1)} %get-tuple-element.59.refs_0_, f32[4,2,1024]{2,1,0:T(2,128)S(1)} %all_to_all.21.refs_1_, f32[2,1024,128]{2,1,0:T(8,128)S(1)} %get-tuple-element.61.refs_2_, ...), custom_call_target="tpu_custom_call", output_to_operand_aliasing={{1}: (0, {})} | custom-call | tf_op jit(solution)/shard_map/pallas_call | solution.py:49
  30.5 0.0 copy-start
  30.5 6.9 %collective-permute-start.1 = (f32[136,1024]{1,0:T(8,128)S(1)}, f32[136,1024]{1,0:T(8,128)S(1)}, u32[]{:S(2)}, u32[]{:S(2)}) collective-permute-start(f32[136,1024]{1,0:T(8,128)S(1)} %get-tuple-element.65.sent), channel_id=1, source_target_pairs={{0,4},{4,0},{1,5},{5,1},{2,6},{6,2},{3,7},{7,3},{8,12},{12,8},{9,1... | collective-permute-start | bytes 1671176 | tf_op jit(solution)/shard_map/ppermute | solution.py:29
  37.5 1.6 %collective-permute-done.1.received = f32[136,1024]{1,0:T(8,128)S(1)} collective-permute-done((f32[136,1024]{1,0:T(8,128)S(1)}, f32[136,1024]{1,0:T(8,128)S(1)}, u32[]{:S(2)}, u32[]{:S(2)}) %collective-permute-start.1) | collective-permute-done | bytes 557088 | tf_op jit(solution)/shard_map/ppermute | solution.py:29
  39.0 0.8 %shard_map.108 = bf16[8,16,1536]{2,1,0:T(8,128)(2,1)} custom-call(f32[128,1024]{1,0:T(8,128)S(1)} %get-tuple-element.58.kept, f32[136,1024]{1,0:T(8,128)S(1)} %get-tuple-element.65.sent, f32[136,1024]{1,0:T(8,128)S(1)} %collective-permute-done.1.received), custom_call_target="tpu_custom_call" | custom-call | tf_op jit(solution)/shard_map/pallas_call | solution.py:49
  39.8 11.2 %all-to-all-start.2 = ((bf16[8,16,1536]{2,1,0:T(8,128)(2,1)}), bf16[8,16,1536]{2,1,0:T(8,128)(2,1)S(1)}, u32[]{:S(2)}, u32[]{:S(2)}) async-start(bf16[8,16,1536]{2,1,0:T(8,128)(2,1)} %shard_map.108), calls=%async_computation.2 | async-start | bytes 786432 | tf_op jit(solution)/shard_map/all_to_all | solution.py:460
  51.1 2.5 %collective-permute-start.2 = (f32[2,32,128]{2,1,0:T(8,128)S(1)}, f32[2,32,128]{2,1,0:T(8,128)S(1)}, u32[]{:S(2)}, u32[]{:S(2)}) collective-permute-start(f32[2,32,128]{2,1,0:T(8,128)S(1)} %slice.3), channel_id=1, source_target_pairs={{4,0},{8,4},{12,8},{16,12},{20,16},{24,20},{28,24},{32,28},{36,32}... | collective-permute-start | bytes 98312 | tf_op jit(solution)/shard_map/ppermute | solution.py:25
  53.6 0.0 copy-done
  53.6 3.4 %shard_map.109 = (bf16[1024,256]{1,0:T(8,128)(2,1)}, bf16[1024,256]{1,0:T(8,128)(2,1)}) custom-call(bf16[1024,256]{1,0:T(8,128)(2,1)} %value_in.5, bf16[1024,256]{1,0:T(8,128)(2,1)} %gate_in.5, f32[2,1024,128]{2,1,0:T(8,128)S(1)} %get-tuple-element.66.grad, f32[31,256]{1,0:T(8,128)S(1)} %copy-done), custom_call_target="tpu_custom_call" | custom-call | tf_op jit(solution)/shard_map/pallas_call | solution.py:49
  57.0 0.0 collective-permute-done.2.after
  57.0 2.6 %all-to-all-done.2.got = bf16[8,16,1536]{2,1,0:T(8,128)(2,1)S(1)} async-done(((bf16[8,16,1536]{2,1,0:T(8,128)(2,1)}), bf16[8,16,1536]{2,1,0:T(8,128)(2,1)S(1)}, u32[]{:S(2)}, u32[]{:S(2)}) %all-to-all-start.2) | async-done | bytes 393248 | tf_op jit(solution)/shard_map/all_to_all | solution.py:460
  59.6 0.8 %shard_map.110 = f32[8,8,1280]{2,1,0:T(8,128)} custom-call(bf16[8,16,1536]{2,1,0:T(8,128)(2,1)S(1)} %all-to-all-done.2.got), custom_call_target="tpu_custom_call" | custom-call | tf_op jit(solution)/shard_map/pallas_call | solution.py:49
  60.5 8.0 %all-to-all-start.3 = ((f32[8,8,1280]{2,1,0:T(8,128)}), f32[8,8,1280]{2,1,0:T(8,128)S(1)}, u32[]{:S(2)}, u32[]{:S(2)}) async-start(f32[8,8,1280]{2,1,0:T(8,128)} %shard_map.110), calls=%async_computation.3 | async-start | bytes 655360 | tf_op jit(solution)/shard_map/all_to_all | solution.py:478
  68.5 3.3 %shard_map.111 = (bf16[1024,256]{1,0:T(8,128)(2,1)}, bf16[1024,256]{1,0:T(8,128)(2,1)}) custom-call(bf16[1024,256]{1,0:T(8,128)(2,1)} %value_in.5, bf16[1024,256]{1,0:T(8,128)(2,1)} %gate_in.5, bf16[1024,256]{1,0:T(8,128)(2,1)} %get-tuple-element.70.value_part, ...), custom_call_target="tpu_custom_call", output_to_operand_aliasing={{0}: (2, {}), {1}: (3, {})} | custom-call | tf_op jit(solution)/shard_map/pallas_call | solution.py:49
  71.8 3.8 %all-to-all-done.3.refs_0_ = f32[8,8,1280]{2,1,0:T(8,128)S(1)} async-done(((f32[8,8,1280]{2,1,0:T(8,128)}), f32[8,8,1280]{2,1,0:T(8,128)S(1)}, u32[]{:S(2)}, u32[]{:S(2)}) %all-to-all-start.3) | async-done | bytes 327712 | tf_op jit(solution)/shard_map/all_to_all | solution.py:478
  75.7 0.6 shard_map.112
  (1 shorter events, 0.0 us)
Async XLA Ops:
  2.1 8.8 %collective-permute-start = (f32[2,32,128]{2,1,0:T(8,128)S(1)}, f32[2,32,128]{2,1,0:T(8,128)S(1)}, u32[]{:S(2)}, u32[]{:S(2)}) collective-permute-start(f32[2,32,128]{2,1,0:T(8,128)S(1)} %get-tuple-element.43), channel_id=1, source_target_pairs={{0,4},{4,8},{8,12},{12,16},{16,20},{20,24},{24,28},{28,32},{32,36}... | collective-permute-start | bytes 98312 | tf_op jit(solution)/shard_map/ppermute | solution.py:25
  9.6 8.5 %copy-start.1 = (f32[256]{0:T(256)S(1)}, f32[256]{0:T(256)}, u32[]{:S(2)}) copy-start(f32[256]{0:T(256)} %param.9) | copy-start | bytes 3076
  30.5 23.1 %copy-start = (f32[31,256]{1,0:T(8,128)S(1)}, f32[31,256]{1,0:T(8,128)}, u32[]{:S(2)}) copy-start(f32[31,256]{1,0:T(8,128)} %taps.3) | copy-start | bytes 95236
  30.5 8.5 %collective-permute-start.1 = (f32[136,1024]{1,0:T(8,128)S(1)}, f32[136,1024]{1,0:T(8,128)S(1)}, u32[]{:S(2)}, u32[]{:S(2)}) collective-permute-start(f32[136,1024]{1,0:T(8,128)S(1)} %get-tuple-element.65.sent), channel_id=1, source_target_pairs={{0,4},{4,0},{1,5},{5,1},{2,6},{6,2},{3,7},{7,3},{8,12},{12,8},{9,1... | collective-permute-start | bytes 1671176 | tf_op jit(solution)/shard_map/ppermute | solution.py:29
  39.8 19.8 %all-to-all-start.2 = ((bf16[8,16,1536]{2,1,0:T(8,128)(2,1)}), bf16[8,16,1536]{2,1,0:T(8,128)(2,1)S(1)}, u32[]{:S(2)}, u32[]{:S(2)}) async-start(bf16[8,16,1536]{2,1,0:T(8,128)(2,1)} %shard_map.108), calls=%async_computation.2 | async-start | bytes 786432 | tf_op jit(solution)/shard_map/all_to_all | solution.py:460
  51.1 5.9 %collective-permute-start.2 = (f32[2,32,128]{2,1,0:T(8,128)S(1)}, f32[2,32,128]{2,1,0:T(8,128)S(1)}, u32[]{:S(2)}, u32[]{:S(2)}) collective-permute-start(f32[2,32,128]{2,1,0:T(8,128)S(1)} %slice.3), channel_id=1, source_target_pairs={{4,0},{8,4},{12,8},{16,12},{20,16},{24,20},{28,24},{32,28},{36,32}... | collective-permute-start | bytes 98312 | tf_op jit(solution)/shard_map/ppermute | solution.py:25
  60.5 15.2 %all-to-all-start.3 = ((f32[8,8,1280]{2,1,0:T(8,128)}), f32[8,8,1280]{2,1,0:T(8,128)S(1)}, u32[]{:S(2)}, u32[]{:S(2)}) async-start(f32[8,8,1280]{2,1,0:T(8,128)} %shard_map.110), calls=%async_computation.3 | async-start | bytes 655360 | tf_op jit(solution)/shard_map/all_to_all | solution.py:478
